TPU v7x, 32 devices: a whole 2x2x4 slice. The times are simulated.
32 devices in a mesh: fs: 4 (over z), rep: 4 (over y, x), tp: 2 (over core).
Axes of the slice: x: 2, y: 2, z: 4, core: 2. Of those that a mesh axis runs over, the one named last changes fastest.
Arguments:
- saved_input: bfloat16 [16384, 2048], P(('fs', 'rep')), may hold values from -6 to 6
- cot_input: bfloat16 [16384, 1024], P(('fs', 'rep'), 'tp'), may hold values from -0.046875 to 0.046875
- cot_gate: bfloat16 [16384, 1024], P(('fs', 'rep'), 'tp'), may hold values from -0.046875 to 0.046875
- in_master: float32 [2048, 1024], P('fs', 'tp'), may hold values from -3 to 3
- gate_master: float32 [2048, 1024], P('fs', 'tp'), may hold values from -3 to 3
- in_factor: bfloat16 [2048, 256], P('fs'), may hold values from -0.125 to 0.125
- gate_factor: bfloat16 [2048, 256], P('fs'), may hold values from -0.125 to 0.125
- in_first: float32 [256, 1024], P('fs', 'tp'), may hold values from -6 to 6
- in_second: float32 [256, 1024], P('fs', 'tp'), may hold values from 0.5 to 2
- gate_first: float32 [256, 1024], P('fs', 'tp'), may hold values from -6 to 6
- gate_second: float32 [256, 1024], P('fs', 'tp'), may hold values from 0.5 to 2
Outputs:
- in_master_new: float32 [2048, 1024], P('fs', 'tp')
- gate_master_new: float32 [2048, 1024], P('fs', 'tp')
- in_update: float32 [2048, 1024], P('fs', 'tp')
- gate_update: float32 [2048, 1024], P('fs', 'tp')
- in_first_new: float32 [256, 1024], P('fs', 'tp')
- in_second_new: float32 [256, 1024], P('fs', 'tp')
- gate_first_new: float32 [256, 1024], P('fs', 'tp')
- gate_second_new: float32 [256, 1024], P('fs', 'tp')
- in_copy: bfloat16 [2048, 1024], P(None, 'tp')
- gate_copy: bfloat16 [2048, 1024], P(None, 'tp')
All inputs are finite; a program needn't handle non-finite values.
Results may differ from a plain program's by a relative error of at most 0.0065.
Values may be sent and summed in bfloat16 or wider, within the bound.
No kernel may reach another device: no remote copies, remote signals or barrier semaphores. Data moves between devices by JAX's collectives and lax.ppermute only.
A program may use at most 64 MiB of HBM per device.

v0:
```python
import functools

import jax
import jax.numpy as jnp
from jax import lax
from jax.experimental import pallas as pl
from jax.experimental.pallas import tpu as pltpu
from jax.sharding import PartitionSpec as P


F32 = jnp.float32
BF16 = jnp.bfloat16
DIRECT = 4
CONTRACT_ROWS = (((0,), (0,)), ((), ()))


def dot(left, right):
    return jnp.dot(left, right, preferred_element_type=F32)


def swap(values, axis, size, step):
    return lax.ppermute(values, axis, [(i, i ^ step) for i in range(size)])


def from_others(values, axis, size):
    if size <= DIRECT:
        return [swap(values, axis, size, k) for k in range(1, size)]
    whole = lax.all_gather(values, axis)
    order = lax.axis_index(axis) ^ jnp.arange(1, size)
    return [jnp.take(whole, order, axis=0).reshape((-1, *values.shape[1:]))]


def one_step(operands, n_outs, scratch=(), out_space=pltpu.VMEM):
    return pltpu.PrefetchScalarGridSpec(
        num_scalar_prefetch=1,
        grid=(),
        in_specs=[pl.BlockSpec(memory_space=pltpu.VMEM)] * len(operands),
        out_specs=[pl.BlockSpec(memory_space=out_space)] * n_outs,
        scratch_shapes=scratch,
    )


def grant(mib):
    return pltpu.CompilerParams(vmem_limit_bytes=mib << 20)


def struct(shape, kind):
    return jax.ShapeDtypeStruct(shape, kind)


def walk(refs, rows):
    k = 0
    for ref in refs:
        for offset in range(0, ref.shape[0], rows):
            k += 1
            yield k, ref, offset


def stage(values):
    def body(in_ref, out_ref, sem):
        copy = pltpu.make_async_copy(in_ref, out_ref, sem)
        copy.start()
        copy.wait()

    return pl.pallas_call(
        body,
        in_specs=[pl.BlockSpec(memory_space=pltpu.HBM)],
        out_specs=pl.BlockSpec(memory_space=pltpu.VMEM),
        out_shape=struct(values.shape, values.dtype),
        scratch_shapes=[pltpu.SemaphoreType.DMA],
        compiler_params=grant(10),
        name="stage",
    )(values)


def project(place, x, in_factor, gate_factor, direct, relayed, rep_size):
    tokens, model = x.shape
    rows, rank = in_factor.shape
    part = rows // rep_size
    n_direct = len(direct)

    def body(place_ref, x_ref, in_ref, gate_ref, *refs):
        pieces, (y_ref, whole_ref) = refs[:-2], refs[-2:]
        fs, rep = place_ref[0], place_ref[1]
        own = jnp.where(place_ref[2] == 0, in_ref[...], gate_ref[...])
        whole_ref[pl.ds(pl.multiple_of(fs * rows, rows), rows), :] = own
        groups = [(0, pieces[:n_direct])]
        groups += [(j + 1, [piece]) for j, piece in enumerate(pieces[n_direct:])]
        for j, group in groups:
            for k, ref, offset in walk(group, part):
                start = pl.multiple_of((fs ^ k) * rows + (rep ^ j) * part, part)
                whole_ref[pl.ds(start, part), :] = ref[offset : offset + part, :]
        y_ref[...] = dot(x_ref[...], whole_ref[...]).astype(BF16)

    operands = (x, in_factor, gate_factor, *direct, *relayed)
    return pl.pallas_call(
        body,
        grid_spec=one_step(operands, 2),
        out_shape=[struct((tokens, rank), BF16), struct((model, rank), BF16)],
        compiler_params=grant(12),
        name="project",
    )(place, *operands)


def token_sums(place, y_own, y_other, cot_input, cot_gate, fs_size):
    rank = y_own.shape[1]
    width = cot_input.shape[1]
    rows = rank // fs_size
    split = fs_size <= DIRECT

    def body(place_ref, own_ref, other_ref, ci_ref, cg_ref, *refs):
        outs, scratch = refs[:-1], refs[-1]
        first = place_ref[2] == 0
        y_in = jnp.where(first, own_ref[...], other_ref[...])
        y_gate = jnp.where(first, other_ref[...], own_ref[...])
        scratch[:, :width] = lax.dot_general(y_in, ci_ref[...], CONTRACT_ROWS, preferred_element_type=F32)
        scratch[:, width:] = lax.dot_general(y_gate, cg_ref[...], CONTRACT_ROWS, preferred_element_type=F32)
        if not split:
            outs[0][...] = scratch[...].astype(BF16)
            return
        for k, out in enumerate(outs):
            start = pl.multiple_of((place_ref[0] ^ k) * rows, rows)
            out[...] = scratch[pl.ds(start, rows), :].astype(out.dtype)

    if split:
        outs = [struct((rows, 2 * width), BF16 if k else F32) for k in range(fs_size)]
    else:
        outs = [struct((rank, 2 * width), BF16)]
    operands = (y_own, y_other, cot_input, cot_gate)
    return pl.pallas_call(
        body,
        grid_spec=one_step(operands, len(outs), [pltpu.VMEM((rank, 2 * width), F32)]),
        out_shape=outs,
        compiler_params=grant(10),
        name="token_sums",
    )(place, *operands)


def add_up(parts):
    def body(*refs):
        total = refs[0][...].astype(F32)
        for ref in refs[1:-1]:
            total = total + ref[...].astype(F32)
        refs[-1][...] = total.astype(BF16)

    return pl.pallas_call(body, out_shape=struct(parts[0].shape, BF16), compiler_params=grant(3), name="add_up")(*parts)


def tree(values):
    while len(values) > 1:
        values = [values[i] + values[i + 1] for i in range(0, len(values), 2)]
    return values[0]


def moments(parts, in_first, in_second, gate_first, gate_second):
    rows, width = in_first.shape
    count = len(parts)

    def body(*refs):
        sums, olds, outs = refs[:count], refs[count : count + 4], refs[count + 4 :]
        low = tree([ref[...].astype(F32) for ref in sums])
        for side in (0, 1):
            part = low[:, side * width : (side + 1) * width]
            first = 0.8 * olds[2 * side][...] + 0.2 * part
            second = 0.95 * olds[2 * side + 1][...] + 0.05 * part * part
            outs[2 * side][...] = first
            outs[2 * side + 1][...] = second
            outs[4][:, side * width : (side + 1) * width] = (first / jnp.sqrt(second)).astype(BF16)

    small = struct((rows, width), F32)
    return pl.pallas_call(
        body,
        out_shape=[small, small, small, small, struct((rows, 2 * width), BF16)],
        compiler_params=grant(4),
        name="moments",
    )(*parts, in_first, in_second, gate_first, gate_second)


def flat_rows(values):
    count, rows, width = values.shape
    if rows % 16:
        return values.astype(F32).reshape(count * rows, width).astype(BF16)
    return values.reshape(count * rows, width)


def gram(place, u_own, u_other):
    rank = u_own.shape[1]

    def body(place_ref, own_ref, other_ref, out_ref):
        first = place_ref[2] == 0
        own, other = own_ref[...], other_ref[...]
        for side, u in ((0, jnp.where(first, own, other)), (1, jnp.where(first, other, own))):
            products = lax.dot_general(u, u, CONTRACT_ROWS, preferred_element_type=F32)
            upper = products.astype(BF16)
            out_ref[2 * side] = upper
            out_ref[2 * side + 1] = (products - upper.astype(F32)).astype(BF16)

    operands = (u_own, u_other)
    return pl.pallas_call(
        body,
        grid_spec=one_step(operands, 1),
        out_shape=[struct((4, rank, rank), BF16)],
        compiler_params=grant(8),
        cost_estimate=pl.CostEstimate(flops=4 * u_own.shape[0] * rank * rank, bytes_accessed=0, transcendentals=0),
        name="gram",
    )(place, *operands)[0]


def squares(place, normed, others, products, fs_size):
    rows, both = normed.shape
    width = both // 2

    def body(place_ref, normed_ref, *refs):
        pieces, (gram_ref, all_ref, sum_ref) = refs[:-3], refs[-3:]
        fs = place_ref[0]
        all_ref[fs] = normed_ref[...]
        for k, ref, offset in walk(pieces, rows):
            all_ref[fs ^ k] = ref[offset : offset + rows, :]
        whole = flat_rows(all_ref[...])
        for side in (0, 1):
            part = whole[:, side * width : (side + 1) * width]
            image = dot(gram_ref[2 * side], part) + dot(gram_ref[2 * side + 1], part)
            total = jnp.sum(part.astype(F32) * image)
            sum_ref[8 * side : 8 * side + 8, :] = jnp.broadcast_to(total, (8, 128))

    operands = (normed, *others, products)
    return pl.pallas_call(
        body,
        grid_spec=one_step(operands, 2),
        out_shape=[struct((fs_size, rows, both), BF16), struct((16, 128), F32)],
        compiler_params=grant(6),
        name="squares",
    )(place, *operands)


def finish(place, sum_own, sum_other, normed, u_own, u_other, in_master, gate_master, direct, relayed, entries):
    rows, width = in_master.shape
    model = u_own.shape[0]
    fs_size = model // rows
    rep_size = 1 + len(relayed[0])
    part = rows // rep_size
    n_direct = len(direct)

    def body(place_ref, so_ref, st_ref, n_ref, uo_ref, ut_ref, im_ref, gm_ref, *refs):
        olds, refs = refs[: n_direct + 2 * (rep_size - 1)], refs[n_direct + 2 * (rep_size - 1) :]
        outs, (mine, spread, work, sems) = refs[:6], refs[6:]
        fs, rep = place_ref[0], place_ref[1]
        first = place_ref[2] == 0
        whole = flat_rows(n_ref[...])
        copies = []

        def send(source, target):
            copy = pltpu.make_async_copy(source, target, sems.at[len(copies)])
            copy.start()
            copies.append(copy)

        pieces = [None] + [(ref, offset) for _, ref, offset in walk(olds[:n_direct], 2 * part)]
        for i in range(fs_size):
            block = pl.ds(pl.multiple_of((fs ^ i) * rows, rows), rows)
            own, other = uo_ref[block, :], ut_ref[block, :]
            for side, u in ((0, jnp.where(first, own, other)), (1, jnp.where(first, other, own))):
                square = so_ref[8 * side : 8 * side + 1, :1] + st_ref[8 * side : 8 * side + 1, :1]
                scale = lax.rsqrt(square / entries + 0.1)
                update = dot(u, whole[:, side * width : (side + 1) * width]) * scale
                target = spread.at[2 * i + side]
                if i == 0:
                    old = (im_ref, gm_ref)[side][...]
                    mine[2 + side] = update
                    send(mine.at[2 + side], outs[2 + side])
                    mine[side] = old - 0.05 * update
                    send(mine.at[side], outs[side])
                    target[...] = (old.astype(BF16).astype(F32) - 0.05 * update).astype(BF16)
                else:
                    work[...] = update
                    for j in range(rep_size):
                        at = pl.ds(pl.multiple_of((rep ^ j) * part, part), part)
                        if j == 0:
                            ref, offset = pieces[i]
                            old = ref[offset + side * part : offset + (side + 1) * part, :]
                        else:
                            ref = olds[n_direct + side * (rep_size - 1) + j - 1]
                            old = ref[(i - 1) * part : i * part, :]
                        target[at, :] = (old.astype(F32) - 0.05 * work[at, :]).astype(BF16)
                send(target, outs[4 + side].at[block, :])
        for copy in copies:
            copy.wait()

    operands = (sum_own, sum_other, normed, u_own, u_other, in_master, gate_master, *direct, *relayed[0], *relayed[1])
    small, big = struct((rows, width), F32), struct((model, width), BF16)
    scratch = [
        pltpu.VMEM((4, rows, width), F32),
        pltpu.VMEM((2 * fs_size, rows, width), BF16),
        pltpu.VMEM((rows, width), F32),
        pltpu.SemaphoreType.DMA((4 + 2 * fs_size,)),
    ]
    return pl.pallas_call(
        body,
        grid_spec=one_step(operands, 6, scratch, pltpu.HBM),
        out_shape=[small, small, small, small, big, big],
        compiler_params=grant(26),
        name="finish",
    )(place, *operands)


def layer(
    sizes,
    saved_input,
    cot_input,
    cot_gate,
    in_master,
    gate_master,
    in_factor,
    gate_factor,
    in_first,
    in_second,
    gate_first,
    gate_second,
):
    fs_size, rep_size, tp_size = sizes
    rows, width = in_master.shape
    part = rows // rep_size
    fs, rep, tp = (lax.axis_index(name) for name in ("fs", "rep", "tp"))
    place = jnp.stack([fs, rep, tp]).astype(jnp.int32)

    def own_part(values):
        return lax.dynamic_slice_in_dim(values, rep * part, part, 0)

    def after(values, *others):
        return lax.optimization_barrier((values, *others))[0]

    sent = jnp.where(tp == 0, own_part(in_factor), own_part(gate_factor))
    direct = from_others(sent, "fs", fs_size)
    x = stage(saved_input)
    relayed = from_others(jnp.concatenate(direct, axis=0), "rep", rep_size)
    old = jnp.concatenate([own_part(in_master), own_part(gate_master)], axis=0).astype(BF16)
    old_direct = from_others(after(old, *direct), "fs", fs_size)

    y_own, u_own = project(place, x, in_factor, gate_factor, direct, relayed, rep_size)
    y_other = swap(y_own, "tp", tp_size, 1)
    u_other = swap(u_own, "tp", tp_size, 1)
    sums = token_sums(place, y_own, y_other, cot_input, cot_gate, fs_size)
    if fs_size <= DIRECT:
        parts = [sums[0]] + [swap(sums[k], "fs", fs_size, k) for k in range(1, fs_size)]
    else:
        parts = [lax.psum_scatter(sums[0], "fs", scatter_dimension=0, tiled=True)]
    products = gram(place, after(u_own, sums[-1]), u_other)
    partial = add_up(parts)

    def side_of(side, cue):
        ready = lax.optimization_barrier((*old_direct, cue))[:-1]
        return jnp.concatenate(
            [values.reshape(-1, 2, part, width)[:, side].reshape(-1, width) for values in ready], axis=0
        )

    old_in = from_others(side_of(0, sums[-1]), "rep", rep_size)
    parts = [partial] + from_others(partial, "rep", rep_size)
    *new, normed = moments(parts, in_first, in_second, gate_first, gate_second)
    others = from_others(normed, "fs", fs_size)
    old_gate = from_others(side_of(1, normed), "rep", rep_size)
    whole, sum_own = squares(place, normed, others, products, fs_size)
    sum_other = swap(sum_own, "tp", tp_size, 1)
    entries = float(rows * fs_size * width * tp_size)
    olds = (in_master, gate_master, old_direct, (old_in, old_gate))
    head = finish(place, sum_own, sum_other, whole, u_own, u_other, *olds, entries)
    return (*head[:4], *new, *head[4:])


def solution(mesh):
    sizes = tuple(mesh.shape[name] for name in ("fs", "rep", "tp"))
    owned, moment = P("fs", "tp"), P("fs", "tp")
    step = jax.shard_map(
        functools.partial(layer, sizes),
        mesh=mesh,
        in_specs=(
            P(("fs", "rep"), None),
            P(("fs", "rep"), "tp"),
            P(("fs", "rep"), "tp"),
            owned,
            owned,
            P("fs", None),
            P("fs", None),
            moment,
            moment,
            moment,
            moment,
        ),
        out_specs=(owned,) * 4 + (moment,) * 4 + (P(None, "tp"),) * 2,
        check_vma=False,
    )
    if max(sizes) > DIRECT:
        return step
    return step
```

profile of v0, /device:TPU:0, one launch (start us, length us, event | category | flops | bytes accessed | tf_op | source)
XLA Modules:
  0.0 115.0 jit_solution(4498578667566655421)
XLA Ops:
  1.5 3.1 %collective-permute-start = (bf16[128,256]{1,0:T(8,128)(2,1)S(1)}, bf16[128,256]{1,0:T(8,128)(2,1)S(1)}, u32[]{:S(2)}, u32[]{:S(2)}) collective-permute-start(bf16[128,256]{1,0:T(8,128)(2,1)S(1)} %dynamic-slice_select_fusion), channel_id=1, source_target_pairs={{0,8},{8,0},{16,24},{24,16},{1,9},{9,1},{17,25},{25,17},{2,10},{10... | collective-permute-start | bytes 196616 | tf_op jit(solution)/shard_map/ppermute | solution.py:22
  4.7 2.5 %collective-permute-start.2 = (bf16[128,256]{1,0:T(8,128)(2,1)S(1)}, bf16[128,256]{1,0:T(8,128)(2,1)S(1)}, u32[]{:S(2)}, u32[]{:S(2)}) collective-permute-start(bf16[128,256]{1,0:T(8,128)(2,1)S(1)} %dynamic-slice_select_fusion), channel_id=1, source_target_pairs={{0,24},{8,16},{16,8},{24,0},{1,25},{9,17},{17,9},{25,1},{2,26},{10... | collective-permute-start | bytes 196616 | tf_op jit(solution)/shard_map/ppermute | solution.py:22
  7.3 6.3 %collective-permute-done.1.refs_1_ = bf16[128,256]{1,0:T(8,128)(2,1)S(1)} collective-permute-done((bf16[128,256]{1,0:T(8,128)(2,1)S(1)}, bf16[128,256]{1,0:T(8,128)(2,1)S(1)}, u32[]{:S(2)}, u32[]{:S(2)}) %collective-permute-start.1) | collective-permute-done | bytes 65568 | tf_op jit(solution)/shard_map/ppermute | solution.py:22
  13.6 2.5 %collective-permute-start.5 = (bf16[384,256]{1,0:T(8,128)(2,1)S(1)}, bf16[384,256]{1,0:T(8,128)(2,1)S(1)}, u32[]{:S(2)}, u32[]{:S(2)}) collective-permute-start(bf16[384,256]{1,0:T(8,128)(2,1)S(1)} %constant_dynamic-update-slice_fusion), channel_id=1, source_target_pairs={{0,6},{2,4},{4,2},{6,0},{1,7},{3,5},{5,3},{7,1},{8,14},{10,12},{12... | collective-permute-start | bytes 589832 | tf_op jit(solution)/shard_map/ppermute | solution.py:22
  17.2 2.2 %copy-done = bf16[1024,2048]{1,0:T(8,128)(2,1)S(1)} copy-done((bf16[1024,2048]{1,0:T(8,128)(2,1)S(1)}, bf16[1024,2048]{1,0:T(8,128)(2,1)}, u32[]{:S(2)}) %copy-start) | copy-done | bytes 4194328
  19.8 2.6 %collective-permute-done.5.refs_5_ = bf16[384,256]{1,0:T(8,128)(2,1)S(1)} collective-permute-done((bf16[384,256]{1,0:T(8,128)(2,1)S(1)}, bf16[384,256]{1,0:T(8,128)(2,1)S(1)}, u32[]{:S(2)}, u32[]{:S(2)}) %collective-permute-start.5) | collective-permute-done | bytes 196640 | tf_op jit(solution)/shard_map/ppermute | solution.py:22
  22.4 3.2 %collective-permute-done.4.refs_4_ = bf16[384,256]{1,0:T(8,128)(2,1)S(1)} collective-permute-done((bf16[384,256]{1,0:T(8,128)(2,1)S(1)}, bf16[384,256]{1,0:T(8,128)(2,1)S(1)}, u32[]{:S(2)}, u32[]{:S(2)}) %collective-permute-start.4) | collective-permute-done | bytes 196640 | tf_op jit(solution)/shard_map/ppermute | solution.py:22
  25.7 1.9 %project.1 = (bf16[1024,256]{1,0:T(8,128)(2,1)S(1)}, bf16[2048,256]{1,0:T(8,128)(2,1)S(1)}) custom-call(s32[3]{0:T(128)S(1)} %pad_add_fusion.place_ref, bf16[1024,2048]{1,0:T(8,128)(2,1)S(1)} %stage.1.x_ref, bf16[512,256]{1,0:T(8,128)(2,1)S(1)} %copy-done.5, bf16[512,256]{1,0:T(8,128)(2,1)S(1)} %copy-done.6, ...), custom_call_target="tpu_custom_call" | custom-call | tf_op jit(solution)/shard_map/project/pallas_call | solution.py:96
  27.8 1.6 %collective-permute-start.20 = (bf16[256,512]{1,0:T(8,128)(2,1)S(1)}, bf16[256,512]{1,0:T(8,128)(2,1)S(1)}, u32[]{:S(2)}, u32[]{:S(2)}) collective-permute-start(bf16[256,512]{1,0:T(8,128)(2,1)S(1)} %pad_maximum_fusion.2), channel_id=1, source_target_pairs={{0,24},{8,16},{16,8},{24,0},{1,25},{9,17},{17,9},{25,1},{2,26},{10... | collective-permute-start | bytes 786440 | tf_op jit(solution)/shard_map/ppermute | solution.py:22
  29.4 2.9 %collective-permute-start.18 = (bf16[256,512]{1,0:T(8,128)(2,1)S(1)}, bf16[256,512]{1,0:T(8,128)(2,1)S(1)}, u32[]{:S(2)}, u32[]{:S(2)}) collective-permute-start(bf16[256,512]{1,0:T(8,128)(2,1)S(1)} %pad_maximum_fusion.2), channel_id=1, source_target_pairs={{0,8},{8,0},{16,24},{24,16},{1,9},{9,1},{17,25},{25,17},{2,10},{10... | collective-permute-start | bytes 786440 | tf_op jit(solution)/shard_map/ppermute | solution.py:22
  32.2 1.3 %token_sums.1 = (f32[64,1024]{1,0:T(8,128)S(1)}, bf16[64,1024]{1,0:T(8,128)(2,1)S(1)}, bf16[64,1024]{1,0:T(8,128)(2,1)S(1)}, bf16[64,1024]{1,0:T(8,128)(2,1)S(1)}) custom-call(s32[3]{0:T(128)S(1)} %pad_add_fusion.place_ref, bf16[1024,256]{1,0:T(8,128)(2,1)S(1)} %get-tuple-element.37.own_ref, bf16[1024,256]{1,0:T(8,128)(2,1)S(1)} %collective-permute-done.6.other_ref, ...), custom_call_target="tpu_custom_call" | custom-call | tf_op jit(solution)/shard_map/token_sums/pallas_call | solution.py:130
  33.6 1.6 %collective-permute-start.9 = (bf16[64,1024]{1,0:T(8,128)(2,1)S(1)}, bf16[64,1024]{1,0:T(8,128)(2,1)S(1)}, u32[]{:S(2)}, u32[]{:S(2)}) collective-permute-start(bf16[64,1024]{1,0:T(8,128)(2,1)S(1)} %get-tuple-element.41), channel_id=1, source_target_pairs={{0,24},{8,16},{16,8},{24,0},{1,25},{9,17},{17,9},{25,1},{2,26},{10... | collective-permute-start | bytes 393224 | tf_op jit(solution)/shard_map/ppermute | solution.py:22
  35.2 3.8 %collective-permute-done.20.refs_2_ = bf16[256,512]{1,0:T(8,128)(2,1)S(1)} collective-permute-done((bf16[256,512]{1,0:T(8,128)(2,1)S(1)}, bf16[256,512]{1,0:T(8,128)(2,1)S(1)}, u32[]{:S(2)}, u32[]{:S(2)}) %collective-permute-start.20) | collective-permute-done | bytes 262176 | tf_op jit(solution)/shard_map/ppermute | solution.py:22
  39.0 16.2 %collective-permute-done.19.refs_1_ = bf16[256,512]{1,0:T(8,128)(2,1)S(1)} collective-permute-done((bf16[256,512]{1,0:T(8,128)(2,1)S(1)}, bf16[256,512]{1,0:T(8,128)(2,1)S(1)}, u32[]{:S(2)}, u32[]{:S(2)}) %collective-permute-start.19) | collective-permute-done | bytes 262176 | tf_op jit(solution)/shard_map/ppermute | solution.py:22
  55.2 2.6 %collective-permute-start.8 = (bf16[64,1024]{1,0:T(8,128)(2,1)S(1)}, bf16[64,1024]{1,0:T(8,128)(2,1)S(1)}, u32[]{:S(2)}, u32[]{:S(2)}) collective-permute-start(bf16[64,1024]{1,0:T(8,128)(2,1)S(1)} %get-tuple-element.40), channel_id=1, source_target_pairs={{0,16},{8,24},{16,0},{24,8},{1,17},{9,25},{17,1},{25,9},{2,18},{10... | collective-permute-start | bytes 393224 | tf_op jit(solution)/shard_map/ppermute | solution.py:22
  57.8 4.2 %collective-permute-done.7.refs_1_ = bf16[64,1024]{1,0:T(8,128)(2,1)S(1)} collective-permute-done((bf16[64,1024]{1,0:T(8,128)(2,1)S(1)}, bf16[64,1024]{1,0:T(8,128)(2,1)S(1)}, u32[]{:S(2)}, u32[]{:S(2)}) %collective-permute-start.7) | collective-permute-done | bytes 131104 | tf_op jit(solution)/shard_map/ppermute | solution.py:22
  62.0 1.6 %collective-permute-done.8.refs_2_ = bf16[64,1024]{1,0:T(8,128)(2,1)S(1)} collective-permute-done((bf16[64,1024]{1,0:T(8,128)(2,1)S(1)}, bf16[64,1024]{1,0:T(8,128)(2,1)S(1)}, u32[]{:S(2)}, u32[]{:S(2)}) %collective-permute-start.8) | collective-permute-done | bytes 131104 | tf_op jit(solution)/shard_map/ppermute | solution.py:22
  63.6 1.7 %collective-permute-start.12 = (bf16[64,1024]{1,0:T(8,128)(2,1)S(1)}, bf16[64,1024]{1,0:T(8,128)(2,1)S(1)}, u32[]{:S(2)}, u32[]{:S(2)}) collective-permute-start(bf16[64,1024]{1,0:T(8,128)(2,1)S(1)} %add_up.1.refs_0_), channel_id=1, source_target_pairs={{0,6},{2,4},{4,2},{6,0},{1,7},{3,5},{5,3},{7,1},{8,14},{10,12},{12... | collective-permute-start | bytes 393224 | tf_op jit(solution)/shard_map/ppermute | solution.py:22
  67.2 1.7 %collective-permute-start.23 = (bf16[384,512]{1,0:T(8,128)(2,1)S(1)}, bf16[384,512]{1,0:T(8,128)(2,1)S(1)}, u32[]{:S(2)}, u32[]{:S(2)}) collective-permute-start(bf16[384,512]{1,0:T(8,128)(2,1)S(1)} %pad_maximum_fusion), channel_id=1, source_target_pairs={{0,6},{2,4},{4,2},{6,0},{1,7},{3,5},{5,3},{7,1},{8,14},{10,12},{12... | collective-permute-start | bytes 1179656 | tf_op jit(solution)/shard_map/ppermute | solution.py:22
  69.0 2.1 %collective-permute-done.12.refs_3_ = bf16[64,1024]{1,0:T(8,128)(2,1)S(1)} collective-permute-done((bf16[64,1024]{1,0:T(8,128)(2,1)S(1)}, bf16[64,1024]{1,0:T(8,128)(2,1)S(1)}, u32[]{:S(2)}, u32[]{:S(2)}) %collective-permute-start.12) | collective-permute-done | bytes 131104 | tf_op jit(solution)/shard_map/ppermute | solution.py:22
  71.1 2.7 %collective-permute-done.11.refs_2_ = bf16[64,1024]{1,0:T(8,128)(2,1)S(1)} collective-permute-done((bf16[64,1024]{1,0:T(8,128)(2,1)S(1)}, bf16[64,1024]{1,0:T(8,128)(2,1)S(1)}, u32[]{:S(2)}, u32[]{:S(2)}) %collective-permute-start.11) | collective-permute-done | bytes 131104 | tf_op jit(solution)/shard_map/ppermute | solution.py:22
  74.7 2.0 %collective-permute-start.15 = (bf16[64,1024]{1,0:T(8,128)(2,1)S(1)}, bf16[64,1024]{1,0:T(8,128)(2,1)S(1)}, u32[]{:S(2)}, u32[]{:S(2)}) collective-permute-start(bf16[64,1024]{1,0:T(8,128)(2,1)S(1)} %get-tuple-element.42.normed_ref), channel_id=1, source_target_pairs={{0,24},{8,16},{16,8},{24,0},{1,25},{9,17},{17,9},{25,1},{2,26},{10... | collective-permute-start | bytes 393224 | tf_op jit(solution)/shard_map/ppermute | solution.py:22
  76.7 2.4 %collective-permute-start.13 = (bf16[64,1024]{1,0:T(8,128)(2,1)S(1)}, bf16[64,1024]{1,0:T(8,128)(2,1)S(1)}, u32[]{:S(2)}, u32[]{:S(2)}) collective-permute-start(bf16[64,1024]{1,0:T(8,128)(2,1)S(1)} %get-tuple-element.42.normed_ref), channel_id=1, source_target_pairs={{0,8},{8,0},{16,24},{24,16},{1,9},{9,1},{17,25},{25,17},{2,10},{10... | collective-permute-start | bytes 393224 | tf_op jit(solution)/shard_map/ppermute | solution.py:22
  79.1 2.4 %collective-permute-done.15.refs_2_ = bf16[64,1024]{1,0:T(8,128)(2,1)S(1)} collective-permute-done((bf16[64,1024]{1,0:T(8,128)(2,1)S(1)}, bf16[64,1024]{1,0:T(8,128)(2,1)S(1)}, u32[]{:S(2)}, u32[]{:S(2)}) %collective-permute-start.15) | collective-permute-done | bytes 131104 | tf_op jit(solution)/shard_map/ppermute | solution.py:22
  81.6 1.5 %collective-permute-start.22 = (bf16[384,512]{1,0:T(8,128)(2,1)S(1)}, bf16[384,512]{1,0:T(8,128)(2,1)S(1)}, u32[]{:S(2)}, u32[]{:S(2)}) collective-permute-start(bf16[384,512]{1,0:T(8,128)(2,1)S(1)} %pad_maximum_fusion), channel_id=1, source_target_pairs={{0,4},{2,6},{4,0},{6,2},{1,5},{3,7},{5,1},{7,3},{8,12},{10,14},{12... | collective-permute-start | bytes 1179656 | tf_op jit(solution)/shard_map/ppermute | solution.py:22
  84.2 2.0 %collective-permute-start.21 = (bf16[384,512]{1,0:T(8,128)(2,1)S(1)}, bf16[384,512]{1,0:T(8,128)(2,1)S(1)}, u32[]{:S(2)}, u32[]{:S(2)}) collective-permute-start(bf16[384,512]{1,0:T(8,128)(2,1)S(1)} %pad_maximum_fusion), channel_id=1, source_target_pairs={{0,2},{2,0},{4,6},{6,4},{1,3},{3,1},{5,7},{7,5},{8,10},{10,8},{12,... | collective-permute-start | bytes 1179656 | tf_op jit(solution)/shard_map/ppermute | solution.py:22
  87.7 2.0 %collective-permute-start.24 = (bf16[384,512]{1,0:T(8,128)(2,1)S(1)}, bf16[384,512]{1,0:T(8,128)(2,1)S(1)}, u32[]{:S(2)}, u32[]{:S(2)}) collective-permute-start(bf16[384,512]{1,0:T(8,128)(2,1)S(1)} %pad_maximum_fusion.1), channel_id=1, source_target_pairs={{0,2},{2,0},{4,6},{6,4},{1,3},{3,1},{5,7},{7,5},{8,10},{10,8},{12,... | collective-permute-start | bytes 1179656 | tf_op jit(solution)/shard_map/ppermute | solution.py:22
  89.7 1.3 %gram.1.refs_3_ = bf16[4,256,256]{2,1,0:T(8,128)(2,1)S(1)} custom-call(s32[3]{0:T(128)S(1)} %pad_add_fusion.place_ref, bf16[2048,256]{1,0:T(8,128)(2,1)S(1)} %get-tuple-element.44.own_ref.uo_ref, bf16[2048,256]{1,0:T(8,128)(2,1)S(1)} %collective-permute-done.16.other_ref.ut_ref), custom_call_target="tpu_custom_call" | custom-call | flops 536870912 | tf_op jit(solution)/shard_map/gram/pallas_call | solution.py:199
  92.6 3.6 %collective-permute-done.21.refs_3_ = bf16[384,512]{1,0:T(8,128)(2,1)S(1)} collective-permute-done((bf16[384,512]{1,0:T(8,128)(2,1)S(1)}, bf16[384,512]{1,0:T(8,128)(2,1)S(1)}, u32[]{:S(2)}, u32[]{:S(2)}) %collective-permute-start.21) | collective-permute-done | bytes 393248 | tf_op jit(solution)/shard_map/ppermute | solution.py:22
  96.2 9.4 %collective-permute-done.26.refs_8_ = bf16[384,512]{1,0:T(8,128)(2,1)S(1)} collective-permute-done((bf16[384,512]{1,0:T(8,128)(2,1)S(1)}, bf16[384,512]{1,0:T(8,128)(2,1)S(1)}, u32[]{:S(2)}, u32[]{:S(2)}) %collective-permute-start.26) | collective-permute-done | bytes 393248 | tf_op jit(solution)/shard_map/ppermute | solution.py:22
  106.2 4.4 %collective-permute-done.24.refs_6_ = bf16[384,512]{1,0:T(8,128)(2,1)S(1)} collective-permute-done((bf16[384,512]{1,0:T(8,128)(2,1)S(1)}, bf16[384,512]{1,0:T(8,128)(2,1)S(1)}, u32[]{:S(2)}, u32[]{:S(2)}) %collective-permute-start.24) | collective-permute-done | bytes 393248 | tf_op jit(solution)/shard_map/ppermute | solution.py:22
  110.6 4.4 %finish.1 = (f32[512,512]{1,0:T(8,128)}, f32[512,512]{1,0:T(8,128)}, f32[512,512]{1,0:T(8,128)}, f32[512,512]{1,0:T(8,128)}, bf16[2048,512]{1,0:T(8,128)(2,1)}, /*index=5*/bf16[2048,512]{1,0:T(8,128)(2,1)}) custom-call(s32[3]{0:T(128)S(1)} %pad_add_fusion.place_ref, f32[16,128]{1,0:T(8,128)S(1)} %get-tuple-element.45.so_ref, ...), custom_call_target="tpu_custom_call" | custom-call | tf_op jit(solution)/shard_map/finish/pallas_call | solution.py:296
  (67 shorter events, 10.6 us)
Async XLA Ops:
  1.5 5.7 %collective-permute-start = (bf16[128,256]{1,0:T(8,128)(2,1)S(1)}, bf16[128,256]{1,0:T(8,128)(2,1)S(1)}, u32[]{:S(2)}, u32[]{:S(2)}) collective-permute-start(bf16[128,256]{1,0:T(8,128)(2,1)S(1)} %dynamic-slice_select_fusion), channel_id=1, source_target_pairs={{0,8},{8,0},{16,24},{24,16},{1,9},{9,1},{17,25},{25,17},{2,10},{10... | collective-permute-start | bytes 196616 | tf_op jit(solution)/shard_map/ppermute | solution.py:22
  4.7 8.9 %collective-permute-start.2 = (bf16[128,256]{1,0:T(8,128)(2,1)S(1)}, bf16[128,256]{1,0:T(8,128)(2,1)S(1)}, u32[]{:S(2)}, u32[]{:S(2)}) collective-permute-start(bf16[128,256]{1,0:T(8,128)(2,1)S(1)} %dynamic-slice_select_fusion), channel_id=1, source_target_pairs={{0,24},{8,16},{16,8},{24,0},{1,25},{9,17},{17,9},{25,1},{2,26},{10... | collective-permute-start | bytes 196616 | tf_op jit(solution)/shard_map/ppermute | solution.py:22
  7.1 6.4 %collective-permute-start.1 = (bf16[128,256]{1,0:T(8,128)(2,1)S(1)}, bf16[128,256]{1,0:T(8,128)(2,1)S(1)}, u32[]{:S(2)}, u32[]{:S(2)}) collective-permute-start(bf16[128,256]{1,0:T(8,128)(2,1)S(1)} %dynamic-slice_select_fusion), channel_id=1, source_target_pairs={{0,16},{8,24},{16,0},{24,8},{1,17},{9,25},{17,1},{25,9},{2,18},{10... | collective-permute-start | bytes 196616 | tf_op jit(solution)/shard_map/ppermute | solution.py:22
  13.6 8.8 %collective-permute-start.5 = (bf16[384,256]{1,0:T(8,128)(2,1)S(1)}, bf16[384,256]{1,0:T(8,128)(2,1)S(1)}, u32[]{:S(2)}, u32[]{:S(2)}) collective-permute-start(bf16[384,256]{1,0:T(8,128)(2,1)S(1)} %constant_dynamic-update-slice_fusion), channel_id=1, source_target_pairs={{0,6},{2,4},{4,2},{6,0},{1,7},{3,5},{5,3},{7,1},{8,14},{10,12},{12... | collective-permute-start | bytes 589832 | tf_op jit(solution)/shard_map/ppermute | solution.py:22
  16.1 9.4 %collective-permute-start.4 = (bf16[384,256]{1,0:T(8,128)(2,1)S(1)}, bf16[384,256]{1,0:T(8,128)(2,1)S(1)}, u32[]{:S(2)}, u32[]{:S(2)}) collective-permute-start(bf16[384,256]{1,0:T(8,128)(2,1)S(1)} %constant_dynamic-update-slice_fusion), channel_id=1, source_target_pairs={{0,4},{2,6},{4,0},{6,2},{1,5},{3,7},{5,1},{7,3},{8,12},{10,14},{12... | collective-permute-start | bytes 589832 | tf_op jit(solution)/shard_map/ppermute | solution.py:22
  16.6 9.0 %collective-permute-start.3 = (bf16[384,256]{1,0:T(8,128)(2,1)S(1)}, bf16[384,256]{1,0:T(8,128)(2,1)S(1)}, u32[]{:S(2)}, u32[]{:S(2)}) collective-permute-start(bf16[384,256]{1,0:T(8,128)(2,1)S(1)} %constant_dynamic-update-slice_fusion), channel_id=1, source_target_pairs={{0,2},{2,0},{4,6},{6,4},{1,3},{3,1},{5,7},{7,5},{8,10},{10,8},{12,... | collective-permute-start | bytes 589832 | tf_op jit(solution)/shard_map/ppermute | solution.py:22
  19.7 12.5 %copy-start.3 = (bf16[1024,512]{1,0:T(8,128)(2,1)S(1)}, bf16[1024,512]{1,0:T(8,128)(2,1)}, u32[]{:S(2)}) copy-start(bf16[1024,512]{1,0:T(8,128)(2,1)} %ci_ref.1) | copy-start | bytes 3145732
  27.5 46.2 %copy-start.7 = (f32[64,512]{1,0:T(8,128)S(1)}, f32[64,512]{1,0:T(8,128)}, u32[]{:S(2)}) copy-start(f32[64,512]{1,0:T(8,128)} %refs_4_.1) | copy-start | bytes 393220
  27.6 46.2 %copy-start.8 = (f32[64,512]{1,0:T(8,128)S(1)}, f32[64,512]{1,0:T(8,128)}, u32[]{:S(2)}) copy-start(f32[64,512]{1,0:T(8,128)} %refs_5_.1) | copy-start | bytes 393220
  27.6 46.2 %copy-start.9 = (f32[64,512]{1,0:T(8,128)S(1)}, f32[64,512]{1,0:T(8,128)}, u32[]{:S(2)}) copy-start(f32[64,512]{1,0:T(8,128)} %refs_6_.1) | copy-start | bytes 393220
  27.6 46.2 %copy-start.10 = (f32[64,512]{1,0:T(8,128)S(1)}, f32[64,512]{1,0:T(8,128)}, u32[]{:S(2)}) copy-start(f32[64,512]{1,0:T(8,128)} %refs_7_.1) | copy-start | bytes 393220
  27.6 4.6 %collective-permute-start.6 = (bf16[1024,256]{1,0:T(8,128)(2,1)S(1)}, bf16[1024,256]{1,0:T(8,128)(2,1)S(1)}, u32[]{:S(2)}, u32[]{:S(2)}) collective-permute-start(bf16[1024,256]{1,0:T(8,128)(2,1)S(1)} %get-tuple-element.37.own_ref), channel_id=1, source_target_pairs={{0,1},{1,0},{2,3},{3,2},{4,5},{5,4},{6,7},{7,6},{8,9},{9,8},{10,11... | collective-permute-start | bytes 1572872 | tf_op jit(solution)/shard_map/ppermute | solution.py:22
  27.8 11.2 %collective-permute-start.20 = (bf16[256,512]{1,0:T(8,128)(2,1)S(1)}, bf16[256,512]{1,0:T(8,128)(2,1)S(1)}, u32[]{:S(2)}, u32[]{:S(2)}) collective-permute-start(bf16[256,512]{1,0:T(8,128)(2,1)S(1)} %pad_maximum_fusion.2), channel_id=1, source_target_pairs={{0,24},{8,16},{16,8},{24,0},{1,25},{9,17},{17,9},{25,1},{2,26},{10... | collective-permute-start | bytes 786440 | tf_op jit(solution)/shard_map/ppermute | solution.py:22
  29.4 25.8 %collective-permute-start.19 = (bf16[256,512]{1,0:T(8,128)(2,1)S(1)}, bf16[256,512]{1,0:T(8,128)(2,1)S(1)}, u32[]{:S(2)}, u32[]{:S(2)}) collective-permute-start(bf16[256,512]{1,0:T(8,128)(2,1)S(1)} %pad_maximum_fusion.2), channel_id=1, source_target_pairs={{0,16},{8,24},{16,0},{24,8},{1,17},{9,25},{17,1},{25,9},{2,18},{10... | collective-permute-start | bytes 786440 | tf_op jit(solution)/shard_map/ppermute | solution.py:22
  29.4 25.8 %collective-permute-start.18 = (bf16[256,512]{1,0:T(8,128)(2,1)S(1)}, bf16[256,512]{1,0:T(8,128)(2,1)S(1)}, u32[]{:S(2)}, u32[]{:S(2)}) collective-permute-start(bf16[256,512]{1,0:T(8,128)(2,1)S(1)} %pad_maximum_fusion.2), channel_id=1, source_target_pairs={{0,8},{8,0},{16,24},{24,16},{1,9},{9,1},{17,25},{25,17},{2,10},{10... | collective-permute-start | bytes 786440 | tf_op jit(solution)/shard_map/ppermute | solution.py:22
  32.2 55.5 %collective-permute-start.16 = (bf16[2048,256]{1,0:T(8,128)(2,1)S(1)}, bf16[2048,256]{1,0:T(8,128)(2,1)S(1)}, u32[]{:S(2)}, u32[]{:S(2)}) collective-permute-start(bf16[2048,256]{1,0:T(8,128)(2,1)S(1)} %get-tuple-element.44.own_ref.uo_ref), channel_id=1, source_target_pairs={{0,1},{1,0},{2,3},{3,2},{4,5},{5,4},{6,7},{7,6},{8,9},{9,8},{10,11... | collective-permute-start | bytes 3145736 | tf_op jit(solution)/shard_map/ppermute | solution.py:22
  33.6 30.0 %collective-permute-start.9 = (bf16[64,1024]{1,0:T(8,128)(2,1)S(1)}, bf16[64,1024]{1,0:T(8,128)(2,1)S(1)}, u32[]{:S(2)}, u32[]{:S(2)}) collective-permute-start(bf16[64,1024]{1,0:T(8,128)(2,1)S(1)} %get-tuple-element.41), channel_id=1, source_target_pairs={{0,24},{8,16},{16,8},{24,0},{1,25},{9,17},{17,9},{25,1},{2,26},{10... | collective-permute-start | bytes 393224 | tf_op jit(solution)/shard_map/ppermute | solution.py:22
  55.1 6.9 %collective-permute-start.7 = (bf16[64,1024]{1,0:T(8,128)(2,1)S(1)}, bf16[64,1024]{1,0:T(8,128)(2,1)S(1)}, u32[]{:S(2)}, u32[]{:S(2)}) collective-permute-start(bf16[64,1024]{1,0:T(8,128)(2,1)S(1)} %get-tuple-element.39), channel_id=1, source_target_pairs={{0,8},{8,0},{16,24},{24,16},{1,9},{9,1},{17,25},{25,17},{2,10},{10... | collective-permute-start | bytes 393224 | tf_op jit(solution)/shard_map/ppermute | solution.py:22
  55.2 8.4 %collective-permute-start.8 = (bf16[64,1024]{1,0:T(8,128)(2,1)S(1)}, bf16[64,1024]{1,0:T(8,128)(2,1)S(1)}, u32[]{:S(2)}, u32[]{:S(2)}) collective-permute-start(bf16[64,1024]{1,0:T(8,128)(2,1)S(1)} %get-tuple-element.40), channel_id=1, source_target_pairs={{0,16},{8,24},{16,0},{24,8},{1,17},{9,25},{17,1},{25,9},{2,18},{10... | collective-permute-start | bytes 393224 | tf_op jit(solution)/shard_map/ppermute | solution.py:22
  63.6 7.4 %collective-permute-start.12 = (bf16[64,1024]{1,0:T(8,128)(2,1)S(1)}, bf16[64,1024]{1,0:T(8,128)(2,1)S(1)}, u32[]{:S(2)}, u32[]{:S(2)}) collective-permute-start(bf16[64,1024]{1,0:T(8,128)(2,1)S(1)} %add_up.1.refs_0_), channel_id=1, source_target_pairs={{0,6},{2,4},{4,2},{6,0},{1,7},{3,5},{5,3},{7,1},{8,14},{10,12},{12... | collective-permute-start | bytes 393224 | tf_op jit(solution)/shard_map/ppermute | solution.py:22
  65.4 8.4 %collective-permute-start.11 = (bf16[64,1024]{1,0:T(8,128)(2,1)S(1)}, bf16[64,1024]{1,0:T(8,128)(2,1)S(1)}, u32[]{:S(2)}, u32[]{:S(2)}) collective-permute-start(bf16[64,1024]{1,0:T(8,128)(2,1)S(1)} %add_up.1.refs_0_), channel_id=1, source_target_pairs={{0,4},{2,6},{4,0},{6,2},{1,5},{3,7},{5,1},{7,3},{8,12},{10,14},{12... | collective-permute-start | bytes 393224 | tf_op jit(solution)/shard_map/ppermute | solution.py:22
  66.7 7.1 %collective-permute-start.10 = (bf16[64,1024]{1,0:T(8,128)(2,1)S(1)}, bf16[64,1024]{1,0:T(8,128)(2,1)S(1)}, u32[]{:S(2)}, u32[]{:S(2)}) collective-permute-start(bf16[64,1024]{1,0:T(8,128)(2,1)S(1)} %add_up.1.refs_0_), channel_id=1, source_target_pairs={{0,2},{2,0},{4,6},{6,4},{1,3},{3,1},{5,7},{7,5},{8,10},{10,8},{12,... | collective-permute-start | bytes 393224 | tf_op jit(solution)/shard_map/ppermute | solution.py:22
  67.2 20.0 %collective-permute-start.23 = (bf16[384,512]{1,0:T(8,128)(2,1)S(1)}, bf16[384,512]{1,0:T(8,128)(2,1)S(1)}, u32[]{:S(2)}, u32[]{:S(2)}) collective-permute-start(bf16[384,512]{1,0:T(8,128)(2,1)S(1)} %pad_maximum_fusion), channel_id=1, source_target_pairs={{0,6},{2,4},{4,2},{6,0},{1,7},{3,5},{5,3},{7,1},{8,14},{10,12},{12... | collective-permute-start | bytes 1179656 | tf_op jit(solution)/shard_map/ppermute | solution.py:22
  74.7 6.9 %collective-permute-start.15 = (bf16[64,1024]{1,0:T(8,128)(2,1)S(1)}, bf16[64,1024]{1,0:T(8,128)(2,1)S(1)}, u32[]{:S(2)}, u32[]{:S(2)}) collective-permute-start(bf16[64,1024]{1,0:T(8,128)(2,1)S(1)} %get-tuple-element.42.normed_ref), channel_id=1, source_target_pairs={{0,24},{8,16},{16,8},{24,0},{1,25},{9,17},{17,9},{25,1},{2,26},{10... | collective-permute-start | bytes 393224 | tf_op jit(solution)/shard_map/ppermute | solution.py:22
  76.7 7.6 %collective-permute-start.14 = (bf16[64,1024]{1,0:T(8,128)(2,1)S(1)}, bf16[64,1024]{1,0:T(8,128)(2,1)S(1)}, u32[]{:S(2)}, u32[]{:S(2)}) collective-permute-start(bf16[64,1024]{1,0:T(8,128)(2,1)S(1)} %get-tuple-element.42.normed_ref), channel_id=1, source_target_pairs={{0,16},{8,24},{16,0},{24,8},{1,17},{9,25},{17,1},{25,9},{2,18},{10... | collective-permute-start | bytes 393224 | tf_op jit(solution)/shard_map/ppermute | solution.py:22
  76.7 9.5 %collective-permute-start.13 = (bf16[64,1024]{1,0:T(8,128)(2,1)S(1)}, bf16[64,1024]{1,0:T(8,128)(2,1)S(1)}, u32[]{:S(2)}, u32[]{:S(2)}) collective-permute-start(bf16[64,1024]{1,0:T(8,128)(2,1)S(1)} %get-tuple-element.42.normed_ref), channel_id=1, source_target_pairs={{0,8},{8,0},{16,24},{24,16},{1,9},{9,1},{17,25},{25,17},{2,10},{10... | collective-permute-start | bytes 393224 | tf_op jit(solution)/shard_map/ppermute | solution.py:22
  81.6 11.1 %collective-permute-start.22 = (bf16[384,512]{1,0:T(8,128)(2,1)S(1)}, bf16[384,512]{1,0:T(8,128)(2,1)S(1)}, u32[]{:S(2)}, u32[]{:S(2)}) collective-permute-start(bf16[384,512]{1,0:T(8,128)(2,1)S(1)} %pad_maximum_fusion), channel_id=1, source_target_pairs={{0,4},{2,6},{4,0},{6,2},{1,5},{3,7},{5,1},{7,3},{8,12},{10,14},{12... | collective-permute-start | bytes 1179656 | tf_op jit(solution)/shard_map/ppermute | solution.py:22
  84.2 12.0 %collective-permute-start.21 = (bf16[384,512]{1,0:T(8,128)(2,1)S(1)}, bf16[384,512]{1,0:T(8,128)(2,1)S(1)}, u32[]{:S(2)}, u32[]{:S(2)}) collective-permute-start(bf16[384,512]{1,0:T(8,128)(2,1)S(1)} %pad_maximum_fusion), channel_id=1, source_target_pairs={{0,2},{2,0},{4,6},{6,4},{1,3},{3,1},{5,7},{7,5},{8,10},{10,8},{12,... | collective-permute-start | bytes 1179656 | tf_op jit(solution)/shard_map/ppermute | solution.py:22
  86.2 19.4 %collective-permute-start.26 = (bf16[384,512]{1,0:T(8,128)(2,1)S(1)}, bf16[384,512]{1,0:T(8,128)(2,1)S(1)}, u32[]{:S(2)}, u32[]{:S(2)}) collective-permute-start(bf16[384,512]{1,0:T(8,128)(2,1)S(1)} %pad_maximum_fusion.1), channel_id=1, source_target_pairs={{0,6},{2,4},{4,2},{6,0},{1,7},{3,5},{5,3},{7,1},{8,14},{10,12},{12... | collective-permute-start | bytes 1179656 | tf_op jit(solution)/shard_map/ppermute | solution.py:22
  87.2 19.0 %collective-permute-start.25 = (bf16[384,512]{1,0:T(8,128)(2,1)S(1)}, bf16[384,512]{1,0:T(8,128)(2,1)S(1)}, u32[]{:S(2)}, u32[]{:S(2)}) collective-permute-start(bf16[384,512]{1,0:T(8,128)(2,1)S(1)} %pad_maximum_fusion.1), channel_id=1, source_target_pairs={{0,4},{2,6},{4,0},{6,2},{1,5},{3,7},{5,1},{7,3},{8,12},{10,14},{12... | collective-permute-start | bytes 1179656 | tf_op jit(solution)/shard_map/ppermute | solution.py:22
  87.7 22.8 %collective-permute-start.24 = (bf16[384,512]{1,0:T(8,128)(2,1)S(1)}, bf16[384,512]{1,0:T(8,128)(2,1)S(1)}, u32[]{:S(2)}, u32[]{:S(2)}) collective-permute-start(bf16[384,512]{1,0:T(8,128)(2,1)S(1)} %pad_maximum_fusion.1), channel_id=1, source_target_pairs={{0,2},{2,0},{4,6},{6,4},{1,3},{3,1},{5,7},{7,5},{8,10},{10,8},{12,... | collective-permute-start | bytes 1179656 | tf_op jit(solution)/shard_map/ppermute | solution.py:22
  92.6 3.6 %collective-permute-start.17 = (f32[16,128]{1,0:T(8,128)S(1)}, f32[16,128]{1,0:T(8,128)S(1)}, u32[]{:S(2)}, u32[]{:S(2)}) collective-permute-start(f32[16,128]{1,0:T(8,128)S(1)} %get-tuple-element.45.so_ref), channel_id=1, source_target_pairs={{0,1},{1,0},{2,3},{3,2},{4,5},{5,4},{6,7},{7,6},{8,9},{9,8},{10,11... | collective-permute-start | bytes 24584 | tf_op jit(solution)/shard_map/ppermute | solution.py:22
  (6 other events, 43.4 us)
where the time goes:
time: 115 us
  waiting for transfers between devices  64.7 us (56%)
  starting transfers between devices  34.6 us (30%)
  Pallas kernels  11.4 us (10%)
  local copies, waits for them, and re-layouts  2.36 us (2%)
    ppermute x27, waiting for transfers between devices, swap(): return lax.ppermute(values, axis, [(i, i ^ step) for i in range(size)])  64.7 us
    ppermute x27, starting transfers between devices, swap(): return lax.ppermute(values, axis, [(i, i ^ step) for i in range(size)])  34.6 us
    pallas_call x1, Pallas kernels, finish(): pl.pallas_call(body, grid_spec=one_step(operands, 6, scratch, pltpu.HBM),...  4.44 us
  transfers between devices with their start and end apart: 27, of which 17 were waited for; matrix products, arithmetic and copies ran while one was open for 0% of the time, Pallas kernels for 4%

commit v1 on v0

v1 whole, which is shorter than its diff:
```python
import functools

import jax
import jax.numpy as jnp
from jax import lax
from jax.experimental import pallas as pl
from jax.experimental.pallas import tpu as pltpu
from jax.sharding import PartitionSpec as P


F32 = jnp.float32
BF16 = jnp.bfloat16
DIRECT = 4
CONTRACT_ROWS = (((0,), (0,)), ((), ()))


def dot(left, right):
    return jnp.dot(left, right, preferred_element_type=F32)


def swap(values, axis, size, step):
    return lax.ppermute(values, axis, [(i, i ^ step) for i in range(size)])


def from_others(values, axis, size):
    if size <= DIRECT:
        return [swap(values, axis, size, k) for k in range(1, size)]
    whole = lax.all_gather(values, axis)
    order = lax.axis_index(axis) ^ jnp.arange(1, size)
    return [jnp.take(whole, order, axis=0).reshape((-1, *values.shape[1:]))]


def one_step(operands, n_outs, scratch=(), out_space=pltpu.VMEM):
    return pltpu.PrefetchScalarGridSpec(
        num_scalar_prefetch=1,
        grid=(),
        in_specs=[pl.BlockSpec(memory_space=pltpu.VMEM)] * len(operands),
        out_specs=[pl.BlockSpec(memory_space=out_space)] * n_outs,
        scratch_shapes=scratch,
    )


def grant(mib):
    return pltpu.CompilerParams(vmem_limit_bytes=mib << 20)


def struct(shape, kind):
    return jax.ShapeDtypeStruct(shape, kind)


def walk(refs, rows):
    k = 0
    for ref in refs:
        for offset in range(0, ref.shape[0], rows):
            k += 1
            yield k, ref, offset


def stage(values):
    def body(in_ref, out_ref, sem):
        copy = pltpu.make_async_copy(in_ref, out_ref, sem)
        copy.start()
        copy.wait()

    return pl.pallas_call(
        body,
        in_specs=[pl.BlockSpec(memory_space=pltpu.HBM)],
        out_specs=pl.BlockSpec(memory_space=pltpu.VMEM),
        out_shape=struct(values.shape, values.dtype),
        scratch_shapes=[pltpu.SemaphoreType.DMA],
        compiler_params=grant(10),
        name="stage",
    )(values)


def project(place, x, in_factor, gate_factor, direct, relayed, rep_size):
    tokens, model = x.shape
    rows, rank = in_factor.shape
    part = rows // rep_size
    n_direct = len(direct)

    def body(place_ref, x_ref, in_ref, gate_ref, *refs):
        pieces, (y_ref, whole_ref) = refs[:-2], refs[-2:]
        fs, rep = place_ref[0], place_ref[1]
        own = jnp.where(place_ref[2] == 0, in_ref[...], gate_ref[...])
        whole_ref[pl.ds(pl.multiple_of(fs * rows, rows), rows), :] = own
        groups = [(0, pieces[:n_direct])]
        groups += [(j + 1, [piece]) for j, piece in enumerate(pieces[n_direct:])]
        for j, group in groups:
            for k, ref, offset in walk(group, part):
                start = pl.multiple_of((fs ^ k) * rows + (rep ^ j) * part, part)
                whole_ref[pl.ds(start, part), :] = ref[offset : offset + part, :]
        y_ref[...] = dot(x_ref[...], whole_ref[...]).astype(BF16)

    operands = (x, in_factor, gate_factor, *direct, *relayed)
    return pl.pallas_call(
        body,
        grid_spec=one_step(operands, 2),
        out_shape=[struct((tokens, rank), BF16), struct((model, rank), BF16)],
        compiler_params=grant(12),
        name="project",
    )(place, *operands)


def token_sums(place, y_own, y_other, cot_input, cot_gate, rep_size):
    rank = y_own.shape[1]
    width = cot_input.shape[1]
    columns = 2 * width // rep_size

    def body(place_ref, own_ref, other_ref, ci_ref, cg_ref, *refs):
        outs, scratch = refs[:-1], refs[-1]
        first = place_ref[2] == 0
        y_in = jnp.where(first, own_ref[...], other_ref[...])
        y_gate = jnp.where(first, other_ref[...], own_ref[...])
        for side, (y, ref) in enumerate(((y_in, ci_ref), (y_gate, cg_ref))):
            sums = lax.dot_general(y, ref[...], CONTRACT_ROWS, preferred_element_type=F32)
            for q in range(rep_size // 2):
                scratch[side * (rep_size // 2) + q] = sums[:, q * columns : (q + 1) * columns]
        for j, out in enumerate(outs):
            out[...] = scratch[place_ref[1] ^ j].astype(out.dtype)

    outs = [struct((rank, columns), BF16 if j else F32) for j in range(rep_size)]
    operands = (y_own, y_other, cot_input, cot_gate)
    return pl.pallas_call(
        body,
        grid_spec=one_step(operands, len(outs), [pltpu.VMEM((rep_size, rank, columns), F32)]),
        out_shape=outs,
        compiler_params=grant(10),
        name="token_sums",
    )(place, *operands)


def add_up(place, parts, fs_size):
    rank, columns = parts[0].shape
    rows = rank // fs_size
    split = fs_size <= DIRECT

    def body(place_ref, *refs):
        sums, outs, scratch = refs[: len(parts)], refs[len(parts) : -1], refs[-1]
        total = tree([ref[...].astype(F32) for ref in sums])
        if not split:
            outs[0][...] = total.astype(BF16)
            return
        for k in range(fs_size):
            scratch[k] = total[k * rows : (k + 1) * rows, :]
        for k, out in enumerate(outs):
            out[...] = scratch[place_ref[0] ^ k].astype(out.dtype)

    outs = [struct((rank, columns), BF16)]
    if split:
        outs = [struct((rows, columns), BF16 if k else F32) for k in range(fs_size)]
    return pl.pallas_call(
        body,
        grid_spec=one_step(parts, len(outs), [pltpu.VMEM((fs_size, rows, columns), F32)]),
        out_shape=outs,
        compiler_params=grant(4),
        name="add_up",
    )(place, *parts)


def tree(values):
    while len(values) > 1:
        values = [sum(values[i : i + 2][1:], values[i]) for i in range(0, len(values), 2)]
    return values[0]


def advance(first, second, low):
    return 0.8 * first + 0.2 * low, 0.95 * second + 0.05 * low * low


def norm_block(place, parts, in_first, in_second, gate_first, gate_second):
    rows, columns = parts[0].shape
    width = in_first.shape[1]
    count = len(parts)

    def body(place_ref, *refs):
        sums, (fi, si, fg, sg, low_ref, normed_ref) = refs[:count], refs[count:]
        low = tree([ref[...].astype(F32) for ref in sums]).astype(BF16)
        low_ref[...] = low
        start = place_ref[1] * columns
        at = pl.ds(pl.multiple_of(lax.rem(start, width), columns), columns)
        is_in = start < width
        old_first = jnp.where(is_in, fi[:, at], fg[:, at])
        old_second = jnp.where(is_in, si[:, at], sg[:, at])
        first, second = advance(old_first, old_second, low.astype(F32))
        normed_ref[...] = (first / jnp.sqrt(second)).astype(BF16)

    operands = (*parts, in_first, in_second, gate_first, gate_second)
    block = struct((rows, columns), BF16)
    return pl.pallas_call(
        body,
        grid_spec=one_step(operands, 2),
        out_shape=[block, block],
        compiler_params=grant(3),
        name="norm_block",
    )(place, *operands)


def moments(place, low, others, in_first, in_second, gate_first, gate_second):
    rows, width = in_first.shape
    columns = low.shape[1]
    count = 1 + len(others)

    def body(place_ref, *refs):
        lows, olds, outs, scratch = refs[:count], refs[count : count + 4], refs[count + 4 : -1], refs[-1]
        for j, ref in enumerate(lows):
            start = (place_ref[1] ^ j) * columns
            at = pl.ds(pl.multiple_of(start, columns), columns)
            scratch[:, at] = ref[-rows:, :].astype(F32)
        for side in (0, 1):
            part = scratch[:, side * width : (side + 1) * width]
            new = advance(olds[2 * side][...], olds[2 * side + 1][...], part)
            outs[2 * side][...], outs[2 * side + 1][...] = new

    operands = (low, *others, in_first, in_second, gate_first, gate_second)
    return pl.pallas_call(
        body,
        grid_spec=one_step(operands, 4, [pltpu.VMEM((rows, 2 * width), F32)]),
        out_shape=[struct((rows, width), F32)] * 4,
        compiler_params=grant(4),
        name="moments",
    )(place, *operands)


def flat_rows(values):
    count, rows, width = values.shape
    if rows % 16:
        return values.astype(F32).reshape(count * rows, width).astype(BF16)
    return values.reshape(count * rows, width)


def gram(place, u_own, u_other):
    rank = u_own.shape[1]

    def body(place_ref, own_ref, other_ref, out_ref):
        first = place_ref[2] == 0
        own, other = own_ref[...], other_ref[...]
        for side, u in ((0, jnp.where(first, own, other)), (1, jnp.where(first, other, own))):
            products = lax.dot_general(u, u, CONTRACT_ROWS, preferred_element_type=F32)
            upper = products.astype(BF16)
            out_ref[2 * side] = upper
            out_ref[2 * side + 1] = (products - upper.astype(F32)).astype(BF16)

    operands = (u_own, u_other)
    return pl.pallas_call(
        body,
        grid_spec=one_step(operands, 1),
        out_shape=[struct((4, rank, rank), BF16)],
        compiler_params=grant(8),
        cost_estimate=pl.CostEstimate(flops=4 * u_own.shape[0] * rank * rank, bytes_accessed=0, transcendentals=0),
        name="gram",
    )(place, *operands)[0]


def squares(place, blocks, products, fs_size, width):
    total, columns = blocks[0].shape
    rows = total // (fs_size + 1)

    def body(place_ref, *refs):
        pieces, (gram_ref, all_ref, sum_ref) = refs[:-3], refs[-3:]
        fs, rep = place_ref[0], place_ref[1]
        for j, ref in enumerate(pieces):
            start = (rep ^ j) * columns
            side = start // width
            at = pl.ds(pl.multiple_of(lax.rem(start, width), columns), columns)
            for k in range(fs_size):
                all_ref[side, fs ^ k, :, at] = ref[k * rows : (k + 1) * rows, :]
        for side in (0, 1):
            part = flat_rows(all_ref[side])
            image = dot(gram_ref[2 * side], part) + dot(gram_ref[2 * side + 1], part)
            total = jnp.sum(part.astype(F32) * image)
            sum_ref[8 * side : 8 * side + 8, :] = jnp.broadcast_to(total, (8, 128))

    operands = (*blocks, products)
    return pl.pallas_call(
        body,
        grid_spec=one_step(operands, 2),
        out_shape=[struct((2, fs_size, rows, width), BF16), struct((16, 128), F32)],
        compiler_params=grant(6),
        name="squares",
    )(place, *operands)


def finish(place, sum_own, sum_other, normed, u_own, u_other, in_master, gate_master, halves, in_rest, gate_rest, rep_size, entries):
    rows, width = in_master.shape
    model = u_own.shape[0]
    fs_size = model // rows
    half = rows // 2
    count, parts = len(halves), len(in_rest)

    def body(place_ref, so_ref, st_ref, n_ref, uo_ref, ut_ref, im_ref, gm_ref, *refs):
        olds, refs = refs[: count + 2 * parts], refs[count + 2 * parts :]
        outs, (mine, spread, sems) = refs[:6], refs[6:]
        fs = place_ref[0]
        held = half_of(place_ref[1], rep_size)
        first = place_ref[2] == 0
        whole = [flat_rows(n_ref[side]) for side in (0, 1)]
        copies = []

        def send(source, target):
            copy = pltpu.make_async_copy(source, target, sems.at[len(copies)])
            copy.start()
            copies.append(copy)

        pieces = [(ref, offset) for _, ref, offset in walk(olds[:count], rows)]
        rest = [[(ref, offset) for _, ref, offset in walk(olds[count + n * parts : count + (n + 1) * parts], half)] for n in (0, 1)]
        factors = []
        for side in (0, 1):
            square = so_ref[8 * side : 8 * side + 1, :1] + st_ref[8 * side : 8 * side + 1, :1]
            factors.append(lax.rsqrt(square / entries + 0.1))

        def product(side, start, size):
            at = pl.ds(pl.multiple_of(start, size), size)
            own, other = uo_ref[at, :], ut_ref[at, :]
            u = jnp.where(first, own, other) if side == 0 else jnp.where(first, other, own)
            return dot(u, whole[side])

        for i in range(fs_size):
            start = (fs ^ i) * rows
            block = pl.ds(pl.multiple_of(start, rows), rows)
            for side in (0, 1):
                target = spread.at[2 * i + side]
                if i == 0:
                    update = product(side, start, rows) * factors[side]
                    old = (im_ref, gm_ref)[side][...]
                    step = 0.05 * update
                    mine[2 + side] = update
                    send(mine.at[2 + side], outs[2 + side])
                    mine[side] = old - step
                    send(mine.at[side], outs[side])
                    target[...] = (old.astype(BF16).astype(F32) - step).astype(BF16)
                else:
                    held_part, rest_part = pieces[i - 1], rest[side][i - 1]
                    for which, (ref, offset) in (
                        (held[side], (held_part[0], held_part[1] + side * half)),
                        (1 - held[side], rest_part),
                    ):
                        step = (0.05 * factors[side]) * product(side, start + which * half, half)
                        old = ref[offset : offset + half, :].astype(F32)
                        target[pl.ds(pl.multiple_of(which * half, half), half), :] = (old - step).astype(BF16)
                send(target, outs[4 + side].at[block, :])
        for copy in copies:
            copy.wait()

    operands = (sum_own, sum_other, normed, u_own, u_other, in_master, gate_master, *halves, *in_rest, *gate_rest)
    small, big = struct((rows, width), F32), struct((model, width), BF16)
    scratch = [
        pltpu.VMEM((4, rows, width), F32),
        pltpu.VMEM((2 * fs_size, rows, width), BF16),
        pltpu.SemaphoreType.DMA((4 + 2 * fs_size,)),
    ]
    return pl.pallas_call(
        body,
        grid_spec=one_step(operands, 6, scratch, pltpu.HBM),
        out_shape=[small, small, small, small, big, big],
        compiler_params=grant(26),
        name="finish",
    )(place, *operands)


def half_of(rep, rep_size):
    return rep & 1, (rep >> ((rep_size // 2).bit_length() - 1)) & 1


def layer(
    sizes,
    saved_input,
    cot_input,
    cot_gate,
    in_master,
    gate_master,
    in_factor,
    gate_factor,
    in_first,
    in_second,
    gate_first,
    gate_second,
):
    fs_size, rep_size, tp_size = sizes
    rows, width = in_master.shape
    part = rows // rep_size
    fs, rep, tp = (lax.axis_index(name) for name in ("fs", "rep", "tp"))
    place = jnp.stack([fs, rep, tp]).astype(jnp.int32)

    half = rows // 2

    def cut(values, index, size):
        return lax.dynamic_slice_in_dim(values, index * size, size, 0)

    def after(values, *others):
        return lax.optimization_barrier((values, *others))[0]

    sent = jnp.where(tp == 0, cut(in_factor, rep, part), cut(gate_factor, rep, part))
    direct = from_others(sent, "fs", fs_size)
    x = stage(saved_input)
    relayed = from_others(jnp.concatenate(direct, axis=0), "rep", rep_size)

    held = half_of(rep, rep_size)
    old = [cut(values, index, half) for values, index in zip((in_master, gate_master), held)]
    old = after(jnp.concatenate(old, axis=0).astype(BF16), *direct)
    if fs_size == 4:
        near = swap(old, "fs", fs_size, 1)
        far = swap(old, "fs", fs_size, 2)
        halves = [near, far]
    else:
        halves = from_others(old, "fs", fs_size)

    def rest_of(values, cue):
        ready = [piece.reshape(-1, 2, half, width) for piece in lax.optimization_barrier((*values, cue))[:-1]]
        return [
            swap(jnp.concatenate([piece[:, side].reshape(-1, width) for piece in ready]), "rep", rep_size, step)
            for side, step in ((0, 1), (1, rep_size // 2))
        ]

    y_own, u_own = project(place, x, in_factor, gate_factor, direct, relayed, rep_size)
    y_other = swap(y_own, "tp", tp_size, 1)
    u_other = swap(u_own, "tp", tp_size, 1)
    sums = token_sums(place, y_own, y_other, cot_input, cot_gate, rep_size)
    parts = [sums[0]] + [swap(sums[j], "rep", rep_size, j) for j in range(1, rep_size)]
    products = gram(place, after(u_own, sums[-1]), u_other)
    sums = add_up(place, parts, fs_size)
    if fs_size <= DIRECT:
        parts = [sums[0]] + [swap(sums[k], "fs", fs_size, k) for k in range(1, fs_size)]
    else:
        parts = [lax.psum_scatter(sums[0], "fs", scatter_dimension=0, tiled=True)]
    state = (in_first, in_second, gate_first, gate_second)
    low, normed = norm_block(place, parts, *state)
    column = jnp.concatenate([normed, *from_others(normed, "fs", fs_size), low], axis=0)
    rest = [rest_of(halves, sums[-1])]
    if fs_size == 4:
        halves.append(swap(after(far, normed), "fs", fs_size, 1))
        rest.append(rest_of(halves[2:], column))
    blocks = [column] + from_others(column, "rep", rep_size)
    whole, sum_own = squares(place, blocks, products, fs_size, width)
    sum_other = swap(sum_own, "tp", tp_size, 1)
    new = moments(place, after(blocks[0], sum_own), blocks[1:], *state)
    entries = float(rows * fs_size * width * tp_size)
    in_rest, gate_rest = zip(*rest)
    olds = (in_master, gate_master, halves, in_rest, gate_rest)
    head = finish(place, sum_own, sum_other, whole, u_own, u_other, *olds, rep_size, entries)
    return (*head[:4], *new, *head[4:])


def solution(mesh):
    sizes = tuple(mesh.shape[name] for name in ("fs", "rep", "tp"))
    owned, moment = P("fs", "tp"), P("fs", "tp")
    return jax.shard_map(
        functools.partial(layer, sizes),
        mesh=mesh,
        in_specs=(
            P(("fs", "rep"), None),
            P(("fs", "rep"), "tp"),
            P(("fs", "rep"), "tp"),
            owned,
            owned,
            P("fs", None),
            P("fs", None),
            moment,
            moment,
            moment,
            moment,
        ),
        out_specs=(owned,) * 4 + (moment,) * 4 + (P(None, "tp"),) * 2,
        check_vma=False,
    )
```

time: 115 us -> 111 us (0.965)
  waiting for transfers between devices: 64.7 us -> 47.8 us
  local copies, waits for them, and re-layouts: 2.36 us -> 10.5 us
  Pallas kernels: 11.4 us -> 14.2 us
  starting transfers between devices: 34.6 us -> 36 us
    ppermute x27 -> x28, waiting for transfers between devices: 64.7 us -> 47.8 us  [swap(): return lax.ppermute(values, axis, [(i, i ^ step) for i in range(size)])]
    unnamed x24 -> x36, local copies, waits for them, and re-layouts: 2.26 us -> 9.63 us
    pallas_call x2 -> x3, Pallas kernels: 0.92 us -> 2.64 us  [the longest x1 1.39 us: moments(): pl.pallas_call(body, grid_spec=one_step(operands, 4, [pltpu.VMEM((rows, 2...]
    ppermute x27 -> x28, starting transfers between devices: 34.6 us -> 36 us  [swap(): return lax.ppermute(values, axis, [(i, i ^ step) for i in range(size)])]
  transfers between devices with their start and end apart: 27 -> 28, of which waited for: 17 -> 14; matrix products, arithmetic and copies ran while one was open for 0% -> 2% of each run, Pallas kernels for 4% -> 6%
where the time goes in v1:
time: 111 us; the launch traced here: 110 us
  waiting for transfers between devices  47.8 us (43%)
  starting transfers between devices  36 us (32%)
  Pallas kernels  14.2 us (13%)
  local copies, waits for them, and re-layouts  10.5 us (9%)
    ppermute x28, waiting for transfers between devices, swap(): return lax.ppermute(values, axis, [(i, i ^ step) for i in range(size)])  47.8 us
    ppermute x28, starting transfers between devices, swap(): return lax.ppermute(values, axis, [(i, i ^ step) for i in range(size)])  36 us
    unnamed x36, local copies, waits for them, and re-layouts  9.63 us
    pallas_call x1, Pallas kernels, finish(): pl.pallas_call(body, grid_spec=one_step(operands, 6, scratch, pltpu.HBM),...  4.39 us
    pallas_call x1, Pallas kernels, project(): pl.pallas_call(body, grid_spec=one_step(operands, 2), out_shape=[struct((...  3 us
  transfers between devices with their start and end apart: 28, of which 14 were waited for; matrix products, arithmetic and copies ran while one was open for 2% of the time, Pallas kernels for 6%

profile of v1, /device:TPU:0, one launch (start us, length us, event | category | flops | bytes accessed | tf_op | source)
XLA Modules:
  0.0 110.4 jit_solution(932751231007537118)
XLA Ops:
  1.5 3.1 %collective-permute-start = (bf16[128,256]{1,0:T(8,128)(2,1)S(1)}, bf16[128,256]{1,0:T(8,128)(2,1)S(1)}, u32[]{:S(2)}, u32[]{:S(2)}) collective-permute-start(bf16[128,256]{1,0:T(8,128)(2,1)S(1)} %dynamic-slice_select_fusion), channel_id=1, source_target_pairs={{0,8},{8,0},{16,24},{24,16},{1,9},{9,1},{17,25},{25,17},{2,10},{10... | collective-permute-start | bytes 196616 | tf_op jit(solution)/shard_map/ppermute | solution.py:22
  4.7 2.5 %collective-permute-start.2 = (bf16[128,256]{1,0:T(8,128)(2,1)S(1)}, bf16[128,256]{1,0:T(8,128)(2,1)S(1)}, u32[]{:S(2)}, u32[]{:S(2)}) collective-permute-start(bf16[128,256]{1,0:T(8,128)(2,1)S(1)} %dynamic-slice_select_fusion), channel_id=1, source_target_pairs={{0,24},{8,16},{16,8},{24,0},{1,25},{9,17},{17,9},{25,1},{2,26},{10... | collective-permute-start | bytes 196616 | tf_op jit(solution)/shard_map/ppermute | solution.py:22
  7.9 5.7 %collective-permute-done.1.refs_1_ = bf16[128,256]{1,0:T(8,128)(2,1)S(1)} collective-permute-done((bf16[128,256]{1,0:T(8,128)(2,1)S(1)}, bf16[128,256]{1,0:T(8,128)(2,1)S(1)}, u32[]{:S(2)}, u32[]{:S(2)}) %collective-permute-start.1) | collective-permute-done | bytes 65568 | tf_op jit(solution)/shard_map/ppermute | solution.py:22
  14.9 2.4 %collective-permute-start.5 = (bf16[384,256]{1,0:T(8,128)(2,1)}, bf16[384,256]{1,0:T(8,128)(2,1)}, u32[]{:S(2)}, u32[]{:S(2)}) collective-permute-start(bf16[384,256]{1,0:T(8,128)(2,1)} %constant_dynamic-update-slice_fusion), channel_id=1, source_target_pairs={{0,6},{2,4},{4,2},{6,0},{1,7},{3,5},{5,3},{7,1},{8,14},{10,12},{12... | collective-permute-start | bytes 589832 | tf_op jit(solution)/shard_map/ppermute | solution.py:22
  18.4 2.2 %copy-done.2 = bf16[1024,2048]{1,0:T(8,128)(2,1)S(1)} copy-done((bf16[1024,2048]{1,0:T(8,128)(2,1)S(1)}, bf16[1024,2048]{1,0:T(8,128)(2,1)}, u32[]{:S(2)}) %copy-start.2) | copy-done | bytes 4194328
  20.9 2.1 %copy-done = bf16[1024,2048]{1,0:T(8,128)(2,1)} copy-done((bf16[1024,2048]{1,0:T(8,128)(2,1)}, bf16[1024,2048]{1,0:T(8,128)(2,1)S(1)}, u32[]{:S(2)}) %copy-start) | copy-done | bytes 4194328
  23.9 3.2 %collective-permute-done.4.refs_4_ = bf16[384,256]{1,0:T(8,128)(2,1)} collective-permute-done((bf16[384,256]{1,0:T(8,128)(2,1)}, bf16[384,256]{1,0:T(8,128)(2,1)}, u32[]{:S(2)}, u32[]{:S(2)}) %collective-permute-start.4) | collective-permute-done | bytes 196640 | tf_op jit(solution)/shard_map/ppermute | solution.py:22
  27.2 2.2 %copy-done.1 = bf16[1024,2048]{1,0:T(8,128)(2,1)S(1)} copy-done((bf16[1024,2048]{1,0:T(8,128)(2,1)S(1)}, bf16[1024,2048]{1,0:T(8,128)(2,1)}, u32[]{:S(2)}) %copy-start.1) | copy-done | bytes 4194328
  31.2 3.0 %project.1 = (bf16[1024,256]{1,0:T(8,128)(2,1)S(1)}, bf16[2048,256]{1,0:T(8,128)(2,1)S(1)}) custom-call(s32[3]{0:T(128)S(1)} %pad_add_fusion.place_ref, bf16[1024,2048]{1,0:T(8,128)(2,1)S(1)} %copy-done.1, bf16[512,256]{1,0:T(8,128)(2,1)S(1)} %copy-done.11, bf16[512,256]{1,0:T(8,128)(2,1)S(1)} %copy-done.12, ...), custom_call_target="tpu_custom_call" | custom-call | tf_op jit(solution)/shard_map/project/pallas_call | solution.py:96
  34.5 2.1 %collective-permute-start.21 = (bf16[512,512]{1,0:T(8,128)(2,1)S(1)}, bf16[512,512]{1,0:T(8,128)(2,1)S(1)}, u32[]{:S(2)}, u32[]{:S(2)}) collective-permute-start(bf16[512,512]{1,0:T(8,128)(2,1)S(1)} %pad_maximum_fusion), channel_id=1, source_target_pairs={{0,8},{8,0},{16,24},{24,16},{1,9},{9,1},{17,25},{25,17},{2,10},{10... | collective-permute-start | bytes 1572872 | tf_op jit(solution)/shard_map/ppermute | solution.py:22
  36.6 1.4 %token_sums.1 = (f32[256,256]{1,0:T(8,128)S(1)}, bf16[256,256]{1,0:T(8,128)(2,1)S(1)}, bf16[256,256]{1,0:T(8,128)(2,1)S(1)}, bf16[256,256]{1,0:T(8,128)(2,1)S(1)}) custom-call(s32[3]{0:T(128)S(1)} %pad_add_fusion.place_ref, bf16[1024,256]{1,0:T(8,128)(2,1)S(1)} %get-tuple-element.41.own_ref, bf16[1024,256]{1,0:T(8,128)(2,1)S(1)} %collective-permute-done.6.other_ref, ...), custom_call_target="tpu_custom_call" | custom-call | tf_op jit(solution)/shard_map/token_sums/pallas_call | solution.py:124
  38.0 1.5 %collective-permute-start.7 = (bf16[256,256]{1,0:T(8,128)(2,1)S(1)}, bf16[256,256]{1,0:T(8,128)(2,1)S(1)}, u32[]{:S(2)}, u32[]{:S(2)}) collective-permute-start(bf16[256,256]{1,0:T(8,128)(2,1)S(1)} %get-tuple-element.43), channel_id=1, source_target_pairs={{0,2},{2,0},{4,6},{6,4},{1,3},{3,1},{5,7},{7,5},{8,10},{10,8},{12,... | collective-permute-start | bytes 393224 | tf_op jit(solution)/shard_map/ppermute | solution.py:22
  41.6 2.2 %collective-permute-done.7.refs_1_ = bf16[256,256]{1,0:T(8,128)(2,1)S(1)} collective-permute-done((bf16[256,256]{1,0:T(8,128)(2,1)S(1)}, bf16[256,256]{1,0:T(8,128)(2,1)S(1)}, u32[]{:S(2)}, u32[]{:S(2)}) %collective-permute-start.7) | collective-permute-done | bytes 131104 | tf_op jit(solution)/shard_map/ppermute | solution.py:22
  43.7 3.7 %collective-permute-done.8.refs_2_ = bf16[256,256]{1,0:T(8,128)(2,1)S(1)} collective-permute-done((bf16[256,256]{1,0:T(8,128)(2,1)S(1)}, bf16[256,256]{1,0:T(8,128)(2,1)S(1)}, u32[]{:S(2)}, u32[]{:S(2)}) %collective-permute-start.8) | collective-permute-done | bytes 131104 | tf_op jit(solution)/shard_map/ppermute | solution.py:22
  48.1 2.4 %collective-permute-start.12 = (bf16[64,256]{1,0:T(8,128)(2,1)S(1)}, bf16[64,256]{1,0:T(8,128)(2,1)S(1)}, u32[]{:S(2)}, u32[]{:S(2)}) collective-permute-start(bf16[64,256]{1,0:T(8,128)(2,1)S(1)} %get-tuple-element.49), channel_id=1, source_target_pairs={{0,24},{8,16},{16,8},{24,0},{1,25},{9,17},{17,9},{25,1},{2,26},{10... | collective-permute-start | bytes 98312 | tf_op jit(solution)/shard_map/ppermute | solution.py:22
  50.4 9.7 %collective-permute-done.22.refs_1_ = bf16[512,512]{1,0:T(8,128)(2,1)S(1)} collective-permute-done((bf16[512,512]{1,0:T(8,128)(2,1)S(1)}, bf16[512,512]{1,0:T(8,128)(2,1)S(1)}, u32[]{:S(2)}, u32[]{:S(2)}) %collective-permute-start.22) | collective-permute-done | bytes 524320 | tf_op jit(solution)/shard_map/ppermute | solution.py:22
  60.8 2.8 %collective-permute-start.11 = (bf16[64,256]{1,0:T(8,128)(2,1)S(1)}, bf16[64,256]{1,0:T(8,128)(2,1)S(1)}, u32[]{:S(2)}, u32[]{:S(2)}) collective-permute-start(bf16[64,256]{1,0:T(8,128)(2,1)S(1)} %get-tuple-element.48), channel_id=1, source_target_pairs={{0,16},{8,24},{16,0},{24,8},{1,17},{9,25},{17,1},{25,9},{2,18},{10... | collective-permute-start | bytes 98312 | tf_op jit(solution)/shard_map/ppermute | solution.py:22
  63.8 1.6 %collective-permute-start.24 = (bf16[512,512]{1,0:T(8,128)(2,1)S(1)}, bf16[512,512]{1,0:T(8,128)(2,1)S(1)}, u32[]{:S(2)}, u32[]{:S(2)}) collective-permute-start(bf16[512,512]{1,0:T(8,128)(2,1)S(1)} %pad_maximum_fusion.1), channel_id=1, source_target_pairs={{0,2},{2,0},{4,6},{6,4},{1,3},{3,1},{5,7},{7,5},{8,10},{10,8},{12,... | collective-permute-start | bytes 1572872 | tf_op jit(solution)/shard_map/ppermute | solution.py:22
  66.8 1.5 %collective-permute-start.13 = (bf16[64,256]{1,0:T(8,128)(2,1)S(1)}, bf16[64,256]{1,0:T(8,128)(2,1)S(1)}, u32[]{:S(2)}, u32[]{:S(2)}) collective-permute-start(bf16[64,256]{1,0:T(8,128)(2,1)S(1)} %get-tuple-element.50), channel_id=1, source_target_pairs={{0,8},{8,0},{16,24},{24,16},{1,9},{9,1},{17,25},{25,17},{2,10},{10... | collective-permute-start | bytes 98312 | tf_op jit(solution)/shard_map/ppermute | solution.py:22
  68.9 2.2 %collective-permute-done.13 = bf16[64,256]{1,0:T(8,128)(2,1)S(1)} collective-permute-done((bf16[64,256]{1,0:T(8,128)(2,1)S(1)}, bf16[64,256]{1,0:T(8,128)(2,1)S(1)}, u32[]{:S(2)}, u32[]{:S(2)}) %collective-permute-start.13) | collective-permute-done | bytes 32800 | tf_op jit(solution)/shard_map/ppermute | solution.py:22
  71.2 2.3 %collective-permute-start.14 = (bf16[64,256]{1,0:T(8,128)(2,1)S(1)}, bf16[64,256]{1,0:T(8,128)(2,1)S(1)}, u32[]{:S(2)}, u32[]{:S(2)}) collective-permute-start(bf16[64,256]{1,0:T(8,128)(2,1)S(1)} %get-tuple-element.50), channel_id=1, source_target_pairs={{0,16},{8,24},{16,0},{24,8},{1,17},{9,25},{17,1},{25,9},{2,18},{10... | collective-permute-start | bytes 98312 | tf_op jit(solution)/shard_map/ppermute | solution.py:22
  73.5 6.1 %collective-permute-done.14 = bf16[64,256]{1,0:T(8,128)(2,1)S(1)} collective-permute-done((bf16[64,256]{1,0:T(8,128)(2,1)S(1)}, bf16[64,256]{1,0:T(8,128)(2,1)S(1)}, u32[]{:S(2)}, u32[]{:S(2)}) %collective-permute-start.14) | collective-permute-done | bytes 32800 | tf_op jit(solution)/shard_map/ppermute | solution.py:22
  79.6 2.0 %collective-permute-start.15 = (bf16[64,256]{1,0:T(8,128)(2,1)S(1)}, bf16[64,256]{1,0:T(8,128)(2,1)S(1)}, u32[]{:S(2)}, u32[]{:S(2)}) collective-permute-start(bf16[64,256]{1,0:T(8,128)(2,1)S(1)} %get-tuple-element.50), channel_id=1, source_target_pairs={{0,24},{8,16},{16,8},{24,0},{1,25},{9,17},{17,9},{25,1},{2,26},{10... | collective-permute-start | bytes 98312 | tf_op jit(solution)/shard_map/ppermute | solution.py:22
  81.6 3.7 %collective-permute-done.15 = bf16[64,256]{1,0:T(8,128)(2,1)S(1)} collective-permute-done((bf16[64,256]{1,0:T(8,128)(2,1)S(1)}, bf16[64,256]{1,0:T(8,128)(2,1)S(1)}, u32[]{:S(2)}, u32[]{:S(2)}) %collective-permute-start.15) | collective-permute-done | bytes 32800 | tf_op jit(solution)/shard_map/ppermute | solution.py:22
  85.3 1.7 %collective-permute-start.18 = (bf16[320,256]{1,0:T(8,128)(2,1)S(1)}, bf16[320,256]{1,0:T(8,128)(2,1)S(1)}, u32[]{:S(2)}, u32[]{:S(2)}) collective-permute-start(bf16[320,256]{1,0:T(8,128)(2,1)S(1)} %constant_dynamic-update-slice_fusion.3.refs_0_), channel_id=1, source_target_pairs={{0,6},{2,4},{4,2},{6,0},{1,7},{3,5},{5,3},{7,1},{8,14},{10,12},{12... | collective-permute-start | bytes 491528 | tf_op jit(solution)/shard_map/ppermute | solution.py:22
  88.3 3.4 %collective-permute-done.18.refs_3_ = bf16[320,256]{1,0:T(8,128)(2,1)S(1)} collective-permute-done((bf16[320,256]{1,0:T(8,128)(2,1)S(1)}, bf16[320,256]{1,0:T(8,128)(2,1)S(1)}, u32[]{:S(2)}, u32[]{:S(2)}) %collective-permute-start.18) | collective-permute-done | bytes 163872 | tf_op jit(solution)/shard_map/ppermute | solution.py:22
  91.7 2.0 %collective-permute-start.27 = (bf16[256,512]{1,0:T(8,128)(2,1)S(1)}, bf16[256,512]{1,0:T(8,128)(2,1)S(1)}, u32[]{:S(2)}, u32[]{:S(2)}) collective-permute-start(bf16[256,512]{1,0:T(8,128)(2,1)S(1)} %get-tuple-element.72), channel_id=1, source_target_pairs={{0,4},{2,6},{4,0},{6,2},{1,5},{3,7},{5,1},{7,3},{8,12},{10,14},{12... | collective-permute-start | bytes 786440 | tf_op jit(solution)/shard_map/ppermute | solution.py:22
  93.7 1.5 %collective-permute-done.17.refs_2_ = bf16[320,256]{1,0:T(8,128)(2,1)S(1)} collective-permute-done((bf16[320,256]{1,0:T(8,128)(2,1)S(1)}, bf16[320,256]{1,0:T(8,128)(2,1)S(1)}, u32[]{:S(2)}, u32[]{:S(2)}) %collective-permute-start.17) | collective-permute-done | bytes 163872 | tf_op jit(solution)/shard_map/ppermute | solution.py:22
  95.2 1.5 %collective-permute-start.25 = (bf16[256,512]{1,0:T(8,128)(2,1)S(1)}, bf16[256,512]{1,0:T(8,128)(2,1)S(1)}, u32[]{:S(2)}, u32[]{:S(2)}) collective-permute-start(bf16[256,512]{1,0:T(8,128)(2,1)S(1)} %get-tuple-element.73), channel_id=1, source_target_pairs={{0,2},{2,0},{4,6},{6,4},{1,3},{3,1},{5,7},{7,5},{8,10},{10,8},{12,... | collective-permute-start | bytes 786440 | tf_op jit(solution)/shard_map/ppermute | solution.py:22
  98.5 4.8 %collective-permute-done.16.refs_1_ = bf16[320,256]{1,0:T(8,128)(2,1)S(1)} collective-permute-done((bf16[320,256]{1,0:T(8,128)(2,1)S(1)}, bf16[320,256]{1,0:T(8,128)(2,1)S(1)}, u32[]{:S(2)}, u32[]{:S(2)}) %collective-permute-start.16) | collective-permute-done | bytes 163872 | tf_op jit(solution)/shard_map/ppermute | solution.py:22
  104.6 1.4 %moments.1 = (f32[64,512]{1,0:T(8,128)}, f32[64,512]{1,0:T(8,128)}, f32[64,512]{1,0:T(8,128)}, f32[64,512]{1,0:T(8,128)}) custom-call(s32[3]{0:T(128)S(1)} %pad_add_fusion.place_ref, bf16[320,256]{1,0:T(8,128)(2,1)S(1)} %constant_dynamic-update-slice_fusion.3.refs_0_, bf16[320,256]{1,0:T(8,128)(2,1)S(1)} %collective-permute-done.16.refs_1_, ...), custom_call_target="tpu_custom_call" | custom-call | tf_op jit(solution)/shard_map/moments/pallas_call | solution.py:216
  106.1 4.4 %finish.1 = (f32[512,512]{1,0:T(8,128)}, f32[512,512]{1,0:T(8,128)}, f32[512,512]{1,0:T(8,128)}, f32[512,512]{1,0:T(8,128)}, bf16[2048,512]{1,0:T(8,128)(2,1)}, /*index=5*/bf16[2048,512]{1,0:T(8,128)(2,1)}) custom-call(s32[3]{0:T(128)S(1)} %pad_add_fusion.place_ref, f32[16,128]{1,0:T(8,128)S(1)} %get-tuple-element.54.so_ref, ...), custom_call_target="tpu_custom_call" | custom-call | tf_op jit(solution)/shard_map/finish/pallas_call | solution.py:352
  (80 shorter events, 17.4 us)
Async XLA Ops:
  1.5 5.7 %collective-permute-start = (bf16[128,256]{1,0:T(8,128)(2,1)S(1)}, bf16[128,256]{1,0:T(8,128)(2,1)S(1)}, u32[]{:S(2)}, u32[]{:S(2)}) collective-permute-start(bf16[128,256]{1,0:T(8,128)(2,1)S(1)} %dynamic-slice_select_fusion), channel_id=1, source_target_pairs={{0,8},{8,0},{16,24},{24,16},{1,9},{9,1},{17,25},{25,17},{2,10},{10... | collective-permute-start | bytes 196616 | tf_op jit(solution)/shard_map/ppermute | solution.py:22
  4.7 9.6 %collective-permute-start.2 = (bf16[128,256]{1,0:T(8,128)(2,1)S(1)}, bf16[128,256]{1,0:T(8,128)(2,1)S(1)}, u32[]{:S(2)}, u32[]{:S(2)}) collective-permute-start(bf16[128,256]{1,0:T(8,128)(2,1)S(1)} %dynamic-slice_select_fusion), channel_id=1, source_target_pairs={{0,24},{8,16},{16,8},{24,0},{1,25},{9,17},{17,9},{25,1},{2,26},{10... | collective-permute-start | bytes 196616 | tf_op jit(solution)/shard_map/ppermute | solution.py:22
  7.1 6.4 %collective-permute-start.1 = (bf16[128,256]{1,0:T(8,128)(2,1)S(1)}, bf16[128,256]{1,0:T(8,128)(2,1)S(1)}, u32[]{:S(2)}, u32[]{:S(2)}) collective-permute-start(bf16[128,256]{1,0:T(8,128)(2,1)S(1)} %dynamic-slice_select_fusion), channel_id=1, source_target_pairs={{0,16},{8,24},{16,0},{24,8},{1,17},{9,25},{17,1},{25,9},{2,18},{10... | collective-permute-start | bytes 196616 | tf_op jit(solution)/shard_map/ppermute | solution.py:22
  14.9 9.0 %collective-permute-start.5 = (bf16[384,256]{1,0:T(8,128)(2,1)}, bf16[384,256]{1,0:T(8,128)(2,1)}, u32[]{:S(2)}, u32[]{:S(2)}) collective-permute-start(bf16[384,256]{1,0:T(8,128)(2,1)} %constant_dynamic-update-slice_fusion), channel_id=1, source_target_pairs={{0,6},{2,4},{4,2},{6,0},{1,7},{3,5},{5,3},{7,1},{8,14},{10,12},{12... | collective-permute-start | bytes 589832 | tf_op jit(solution)/shard_map/ppermute | solution.py:22
  17.3 9.8 %collective-permute-start.4 = (bf16[384,256]{1,0:T(8,128)(2,1)}, bf16[384,256]{1,0:T(8,128)(2,1)}, u32[]{:S(2)}, u32[]{:S(2)}) collective-permute-start(bf16[384,256]{1,0:T(8,128)(2,1)} %constant_dynamic-update-slice_fusion), channel_id=1, source_target_pairs={{0,4},{2,6},{4,0},{6,2},{1,5},{3,7},{5,1},{7,3},{8,12},{10,14},{12... | collective-permute-start | bytes 589832 | tf_op jit(solution)/shard_map/ppermute | solution.py:22
  17.8 9.3 %collective-permute-start.3 = (bf16[384,256]{1,0:T(8,128)(2,1)}, bf16[384,256]{1,0:T(8,128)(2,1)}, u32[]{:S(2)}, u32[]{:S(2)}) collective-permute-start(bf16[384,256]{1,0:T(8,128)(2,1)} %constant_dynamic-update-slice_fusion), channel_id=1, source_target_pairs={{0,2},{2,0},{4,6},{6,4},{1,3},{3,1},{5,7},{7,5},{8,10},{10,8},{12,... | collective-permute-start | bytes 589832 | tf_op jit(solution)/shard_map/ppermute | solution.py:22
  34.2 2.4 %collective-permute-start.6 = (bf16[1024,256]{1,0:T(8,128)(2,1)S(1)}, bf16[1024,256]{1,0:T(8,128)(2,1)S(1)}, u32[]{:S(2)}, u32[]{:S(2)}) collective-permute-start(bf16[1024,256]{1,0:T(8,128)(2,1)S(1)} %get-tuple-element.41.own_ref), channel_id=1, source_target_pairs={{0,1},{1,0},{2,3},{3,2},{4,5},{5,4},{6,7},{7,6},{8,9},{9,8},{10,11... | collective-permute-start | bytes 1572872 | tf_op jit(solution)/shard_map/ppermute | solution.py:22
  34.4 31.8 %copy-start.7 = (f32[64,512]{1,0:T(8,128)S(1)}, f32[64,512]{1,0:T(8,128)}, u32[]{:S(2)}) copy-start(f32[64,512]{1,0:T(8,128)} %refs_4_.3) | copy-start | bytes 393220
  34.4 31.8 %copy-start.8 = (f32[64,512]{1,0:T(8,128)S(1)}, f32[64,512]{1,0:T(8,128)}, u32[]{:S(2)}) copy-start(f32[64,512]{1,0:T(8,128)} %refs_5_.3) | copy-start | bytes 393220
  34.4 31.8 %copy-start.9 = (f32[64,512]{1,0:T(8,128)S(1)}, f32[64,512]{1,0:T(8,128)}, u32[]{:S(2)}) copy-start(f32[64,512]{1,0:T(8,128)} %refs_6_.3) | copy-start | bytes 393220
  34.4 31.8 %copy-start.10 = (f32[64,512]{1,0:T(8,128)S(1)}, f32[64,512]{1,0:T(8,128)}, u32[]{:S(2)}) copy-start(f32[64,512]{1,0:T(8,128)} %refs_7_.3) | copy-start | bytes 393220
  34.4 25.7 %collective-permute-start.22 = (bf16[512,512]{1,0:T(8,128)(2,1)S(1)}, bf16[512,512]{1,0:T(8,128)(2,1)S(1)}, u32[]{:S(2)}, u32[]{:S(2)}) collective-permute-start(bf16[512,512]{1,0:T(8,128)(2,1)S(1)} %pad_maximum_fusion), channel_id=1, source_target_pairs={{0,16},{8,24},{16,0},{24,8},{1,17},{9,25},{17,1},{25,9},{2,18},{10... | collective-permute-start | bytes 1572872 | tf_op jit(solution)/shard_map/ppermute | solution.py:22
  34.5 26.3 %collective-permute-start.21 = (bf16[512,512]{1,0:T(8,128)(2,1)S(1)}, bf16[512,512]{1,0:T(8,128)(2,1)S(1)}, u32[]{:S(2)}, u32[]{:S(2)}) collective-permute-start(bf16[512,512]{1,0:T(8,128)(2,1)S(1)} %pad_maximum_fusion), channel_id=1, source_target_pairs={{0,8},{8,0},{16,24},{24,16},{1,9},{9,1},{17,25},{25,17},{2,10},{10... | collective-permute-start | bytes 1572872 | tf_op jit(solution)/shard_map/ppermute | solution.py:22
  38.0 5.7 %collective-permute-start.7 = (bf16[256,256]{1,0:T(8,128)(2,1)S(1)}, bf16[256,256]{1,0:T(8,128)(2,1)S(1)}, u32[]{:S(2)}, u32[]{:S(2)}) collective-permute-start(bf16[256,256]{1,0:T(8,128)(2,1)S(1)} %get-tuple-element.43), channel_id=1, source_target_pairs={{0,2},{2,0},{4,6},{6,4},{1,3},{3,1},{5,7},{7,5},{8,10},{10,8},{12,... | collective-permute-start | bytes 393224 | tf_op jit(solution)/shard_map/ppermute | solution.py:22
  39.5 7.9 %collective-permute-start.8 = (bf16[256,256]{1,0:T(8,128)(2,1)S(1)}, bf16[256,256]{1,0:T(8,128)(2,1)S(1)}, u32[]{:S(2)}, u32[]{:S(2)}) collective-permute-start(bf16[256,256]{1,0:T(8,128)(2,1)S(1)} %get-tuple-element.44), channel_id=1, source_target_pairs={{0,4},{2,6},{4,0},{6,2},{1,5},{3,7},{5,1},{7,3},{8,12},{10,14},{12... | collective-permute-start | bytes 393224 | tf_op jit(solution)/shard_map/ppermute | solution.py:22
  40.3 7.1 %collective-permute-start.9 = (bf16[256,256]{1,0:T(8,128)(2,1)S(1)}, bf16[256,256]{1,0:T(8,128)(2,1)S(1)}, u32[]{:S(2)}, u32[]{:S(2)}) collective-permute-start(bf16[256,256]{1,0:T(8,128)(2,1)S(1)} %get-tuple-element.45), channel_id=1, source_target_pairs={{0,6},{2,4},{4,2},{6,0},{1,7},{3,5},{5,3},{7,1},{8,14},{10,12},{12... | collective-permute-start | bytes 393224 | tf_op jit(solution)/shard_map/ppermute | solution.py:22
  43.7 52.9 %collective-permute-start.19 = (bf16[2048,256]{1,0:T(8,128)(2,1)S(1)}, bf16[2048,256]{1,0:T(8,128)(2,1)S(1)}, u32[]{:S(2)}, u32[]{:S(2)}) collective-permute-start(bf16[2048,256]{1,0:T(8,128)(2,1)S(1)} %get-tuple-element.53.own_ref.uo_ref), channel_id=1, source_target_pairs={{0,1},{1,0},{2,3},{3,2},{4,5},{5,4},{6,7},{7,6},{8,9},{9,8},{10,11... | collective-permute-start | bytes 3145736 | tf_op jit(solution)/shard_map/ppermute | solution.py:22
  48.1 18.1 %collective-permute-start.12 = (bf16[64,256]{1,0:T(8,128)(2,1)S(1)}, bf16[64,256]{1,0:T(8,128)(2,1)S(1)}, u32[]{:S(2)}, u32[]{:S(2)}) collective-permute-start(bf16[64,256]{1,0:T(8,128)(2,1)S(1)} %get-tuple-element.49), channel_id=1, source_target_pairs={{0,24},{8,16},{16,8},{24,0},{1,25},{9,17},{17,9},{25,1},{2,26},{10... | collective-permute-start | bytes 98312 | tf_op jit(solution)/shard_map/ppermute | solution.py:22
  60.8 4.6 %collective-permute-start.10 = (bf16[64,256]{1,0:T(8,128)(2,1)S(1)}, bf16[64,256]{1,0:T(8,128)(2,1)S(1)}, u32[]{:S(2)}, u32[]{:S(2)}) collective-permute-start(bf16[64,256]{1,0:T(8,128)(2,1)S(1)} %get-tuple-element.47), channel_id=1, source_target_pairs={{0,8},{8,0},{16,24},{24,16},{1,9},{9,1},{17,25},{25,17},{2,10},{10... | collective-permute-start | bytes 98312 | tf_op jit(solution)/shard_map/ppermute | solution.py:22
  60.8 5.4 %collective-permute-start.11 = (bf16[64,256]{1,0:T(8,128)(2,1)S(1)}, bf16[64,256]{1,0:T(8,128)(2,1)S(1)}, u32[]{:S(2)}, u32[]{:S(2)}) collective-permute-start(bf16[64,256]{1,0:T(8,128)(2,1)S(1)} %get-tuple-element.48), channel_id=1, source_target_pairs={{0,16},{8,24},{16,0},{24,8},{1,17},{9,25},{17,1},{25,9},{2,18},{10... | collective-permute-start | bytes 98312 | tf_op jit(solution)/shard_map/ppermute | solution.py:22
  63.8 42.2 %collective-permute-start.24 = (bf16[512,512]{1,0:T(8,128)(2,1)S(1)}, bf16[512,512]{1,0:T(8,128)(2,1)S(1)}, u32[]{:S(2)}, u32[]{:S(2)}) collective-permute-start(bf16[512,512]{1,0:T(8,128)(2,1)S(1)} %pad_maximum_fusion.1), channel_id=1, source_target_pairs={{0,2},{2,0},{4,6},{6,4},{1,3},{3,1},{5,7},{7,5},{8,10},{10,8},{12,... | collective-permute-start | bytes 1572872 | tf_op jit(solution)/shard_map/ppermute | solution.py:22
  65.4 40.6 %collective-permute-start.26 = (bf16[512,512]{1,0:T(8,128)(2,1)S(1)}, bf16[512,512]{1,0:T(8,128)(2,1)S(1)}, u32[]{:S(2)}, u32[]{:S(2)}) collective-permute-start(bf16[512,512]{1,0:T(8,128)(2,1)S(1)} %pad_maximum_fusion.2), channel_id=1, source_target_pairs={{0,4},{2,6},{4,0},{6,2},{1,5},{3,7},{5,1},{7,3},{8,12},{10,14},{12... | collective-permute-start | bytes 1572872 | tf_op jit(solution)/shard_map/ppermute | solution.py:22
  66.8 4.3 %collective-permute-start.13 = (bf16[64,256]{1,0:T(8,128)(2,1)S(1)}, bf16[64,256]{1,0:T(8,128)(2,1)S(1)}, u32[]{:S(2)}, u32[]{:S(2)}) collective-permute-start(bf16[64,256]{1,0:T(8,128)(2,1)S(1)} %get-tuple-element.50), channel_id=1, source_target_pairs={{0,8},{8,0},{16,24},{24,16},{1,9},{9,1},{17,25},{25,17},{2,10},{10... | collective-permute-start | bytes 98312 | tf_op jit(solution)/shard_map/ppermute | solution.py:22
  68.4 18.6 %collective-permute-start.23 = (bf16[512,512]{1,0:T(8,128)(2,1)S(1)}, bf16[512,512]{1,0:T(8,128)(2,1)S(1)}, u32[]{:S(2)}, u32[]{:S(2)}) collective-permute-start(bf16[512,512]{1,0:T(8,128)(2,1)S(1)} %collective-permute-done.22.refs_1_), channel_id=1, source_target_pairs={{0,8},{8,0},{16,24},{24,16},{1,9},{9,1},{17,25},{25,17},{2,10},{10... | collective-permute-start | bytes 1572872 | tf_op jit(solution)/shard_map/ppermute | solution.py:22
  71.2 8.4 %collective-permute-start.14 = (bf16[64,256]{1,0:T(8,128)(2,1)S(1)}, bf16[64,256]{1,0:T(8,128)(2,1)S(1)}, u32[]{:S(2)}, u32[]{:S(2)}) collective-permute-start(bf16[64,256]{1,0:T(8,128)(2,1)S(1)} %get-tuple-element.50), channel_id=1, source_target_pairs={{0,16},{8,24},{16,0},{24,8},{1,17},{9,25},{17,1},{25,9},{2,18},{10... | collective-permute-start | bytes 98312 | tf_op jit(solution)/shard_map/ppermute | solution.py:22
  79.6 5.7 %collective-permute-start.15 = (bf16[64,256]{1,0:T(8,128)(2,1)S(1)}, bf16[64,256]{1,0:T(8,128)(2,1)S(1)}, u32[]{:S(2)}, u32[]{:S(2)}) collective-permute-start(bf16[64,256]{1,0:T(8,128)(2,1)S(1)} %get-tuple-element.50), channel_id=1, source_target_pairs={{0,24},{8,16},{16,8},{24,0},{1,25},{9,17},{17,9},{25,1},{2,26},{10... | collective-permute-start | bytes 98312 | tf_op jit(solution)/shard_map/ppermute | solution.py:22
  85.3 6.4 %collective-permute-start.18 = (bf16[320,256]{1,0:T(8,128)(2,1)S(1)}, bf16[320,256]{1,0:T(8,128)(2,1)S(1)}, u32[]{:S(2)}, u32[]{:S(2)}) collective-permute-start(bf16[320,256]{1,0:T(8,128)(2,1)S(1)} %constant_dynamic-update-slice_fusion.3.refs_0_), channel_id=1, source_target_pairs={{0,6},{2,4},{4,2},{6,0},{1,7},{3,5},{5,3},{7,1},{8,14},{10,12},{12... | collective-permute-start | bytes 491528 | tf_op jit(solution)/shard_map/ppermute | solution.py:22
  87.0 8.2 %collective-permute-start.17 = (bf16[320,256]{1,0:T(8,128)(2,1)S(1)}, bf16[320,256]{1,0:T(8,128)(2,1)S(1)}, u32[]{:S(2)}, u32[]{:S(2)}) collective-permute-start(bf16[320,256]{1,0:T(8,128)(2,1)S(1)} %constant_dynamic-update-slice_fusion.3.refs_0_), channel_id=1, source_target_pairs={{0,4},{2,6},{4,0},{6,2},{1,5},{3,7},{5,1},{7,3},{8,12},{10,14},{12... | collective-permute-start | bytes 491528 | tf_op jit(solution)/shard_map/ppermute | solution.py:22
  91.7 14.3 %collective-permute-start.27 = (bf16[256,512]{1,0:T(8,128)(2,1)S(1)}, bf16[256,512]{1,0:T(8,128)(2,1)S(1)}, u32[]{:S(2)}, u32[]{:S(2)}) collective-permute-start(bf16[256,512]{1,0:T(8,128)(2,1)S(1)} %get-tuple-element.72), channel_id=1, source_target_pairs={{0,4},{2,6},{4,0},{6,2},{1,5},{3,7},{5,1},{7,3},{8,12},{10,14},{12... | collective-permute-start | bytes 786440 | tf_op jit(solution)/shard_map/ppermute | solution.py:22
  95.2 10.8 %collective-permute-start.25 = (bf16[256,512]{1,0:T(8,128)(2,1)S(1)}, bf16[256,512]{1,0:T(8,128)(2,1)S(1)}, u32[]{:S(2)}, u32[]{:S(2)}) collective-permute-start(bf16[256,512]{1,0:T(8,128)(2,1)S(1)} %get-tuple-element.73), channel_id=1, source_target_pairs={{0,2},{2,0},{4,6},{6,4},{1,3},{3,1},{5,7},{7,5},{8,10},{10,8},{12,... | collective-permute-start | bytes 786440 | tf_op jit(solution)/shard_map/ppermute | solution.py:22
  96.7 6.7 %collective-permute-start.16 = (bf16[320,256]{1,0:T(8,128)(2,1)S(1)}, bf16[320,256]{1,0:T(8,128)(2,1)S(1)}, u32[]{:S(2)}, u32[]{:S(2)}) collective-permute-start(bf16[320,256]{1,0:T(8,128)(2,1)S(1)} %constant_dynamic-update-slice_fusion.3.refs_0_), channel_id=1, source_target_pairs={{0,2},{2,0},{4,6},{6,4},{1,3},{3,1},{5,7},{7,5},{8,10},{10,8},{12,... | collective-permute-start | bytes 491528 | tf_op jit(solution)/shard_map/ppermute | solution.py:22
  104.6 1.5 %collective-permute-start.20 = (f32[16,128]{1,0:T(8,128)S(1)}, f32[16,128]{1,0:T(8,128)S(1)}, u32[]{:S(2)}, u32[]{:S(2)}) collective-permute-start(f32[16,128]{1,0:T(8,128)S(1)} %get-tuple-element.54.so_ref), channel_id=1, source_target_pairs={{0,1},{1,0},{2,3},{3,2},{4,5},{5,4},{6,7},{7,6},{8,9},{9,8},{10,11... | collective-permute-start | bytes 24584 | tf_op jit(solution)/shard_map/ppermute | solution.py:22
  (11 other events, 64.4 us)

commit v2 on v1

v2 whole, which is shorter than its diff:
```python
import functools

import jax
import jax.numpy as jnp
from jax import lax
from jax.experimental import pallas as pl
from jax.experimental.pallas import tpu as pltpu
from jax.sharding import PartitionSpec as P


F32 = jnp.float32
BF16 = jnp.bfloat16
DIRECT = 4
CONTRACT_ROWS = (((0,), (0,)), ((), ()))


def dot(left, right):
    return jnp.dot(left, right, preferred_element_type=F32)


def swap(values, axis, size, step):
    return lax.ppermute(values, axis, [(i, i ^ step) for i in range(size)])


def from_others(values, axis, size):
    if size <= DIRECT:
        return [swap(values, axis, size, k) for k in range(1, size)]
    whole = lax.all_gather(values, axis)
    order = lax.axis_index(axis) ^ jnp.arange(1, size)
    return [jnp.take(whole, order, axis=0).reshape((-1, *values.shape[1:]))]


def one_step(operands, n_outs, scratch=(), out_space=pltpu.VMEM):
    return pltpu.PrefetchScalarGridSpec(
        num_scalar_prefetch=1,
        grid=(),
        in_specs=[pl.BlockSpec(memory_space=pltpu.VMEM)] * len(operands),
        out_specs=[pl.BlockSpec(memory_space=out_space)] * n_outs,
        scratch_shapes=scratch,
    )


def grant(mib):
    return pltpu.CompilerParams(vmem_limit_bytes=mib << 20)


def struct(shape, kind):
    return jax.ShapeDtypeStruct(shape, kind)


def walk(refs, rows):
    k = 0
    for ref in refs:
        for offset in range(0, ref.shape[0], rows):
            k += 1
            yield k, ref, offset


def stage(values):
    def body(in_ref, out_ref, sem):
        copy = pltpu.make_async_copy(in_ref, out_ref, sem)
        copy.start()
        copy.wait()

    return pl.pallas_call(
        body,
        in_specs=[pl.BlockSpec(memory_space=pltpu.HBM)],
        out_specs=pl.BlockSpec(memory_space=pltpu.VMEM),
        out_shape=struct(values.shape, values.dtype),
        scratch_shapes=[pltpu.SemaphoreType.DMA],
        compiler_params=grant(10),
        name="stage",
    )(values)


def held_rows(place, masters, rep_size):
    rows, width = masters[0].shape
    half = rows // 2

    def body(place_ref, in_ref, gate_ref, out_ref):
        is_in = place_ref[2] == 0
        for side, which in enumerate(half_of(place_ref[1], rep_size)):
            at = pl.ds(pl.multiple_of(which * half, half), half)
            wanted = jnp.where(is_in if side == 0 else jnp.logical_not(is_in), in_ref[at, :], gate_ref[at, :])
            out_ref[side * half : (side + 1) * half, :] = wanted.astype(BF16)

    return pl.pallas_call(
        body,
        grid_spec=one_step(masters, 1),
        out_shape=[struct((rows, width), BF16)],
        compiler_params=grant(6),
        name="held_rows",
    )(place, *masters)[0]


def project(place, x, in_factor, gate_factor, direct, relayed, rep_size):
    tokens, model = x.shape
    rows, rank = in_factor.shape
    part = rows // rep_size
    n_direct = len(direct)

    def body(place_ref, x_ref, in_ref, gate_ref, *refs):
        pieces, (y_ref, whole_ref) = refs[:-2], refs[-2:]
        fs, rep = place_ref[0], place_ref[1]
        own = jnp.where(place_ref[2] == 0, in_ref[...], gate_ref[...])
        whole_ref[pl.ds(pl.multiple_of(fs * rows, rows), rows), :] = own
        groups = [(0, pieces[:n_direct])]
        groups += [(j + 1, [piece]) for j, piece in enumerate(pieces[n_direct:])]
        for j, group in groups:
            for k, ref, offset in walk(group, part):
                start = pl.multiple_of((fs ^ k) * rows + (rep ^ j) * part, part)
                whole_ref[pl.ds(start, part), :] = ref[offset : offset + part, :]
        y_ref[...] = dot(x_ref[...], whole_ref[...]).astype(BF16)

    operands = (x, in_factor, gate_factor, *direct, *relayed)
    return pl.pallas_call(
        body,
        grid_spec=one_step(operands, 2),
        out_shape=[struct((tokens, rank), BF16), struct((model, rank), BF16)],
        compiler_params=grant(12),
        name="project",
    )(place, *operands)


def token_sums(place, y, cotangents, rep_size):
    rank = y.shape[1]
    width = cotangents[0].shape[1]
    per = rep_size // 2
    columns = width // per

    def body(place_ref, y_ref, ci, cg, other_ci, other_cg, *refs):
        outs, scratch = refs[:-1], refs[-1]
        core = place_ref[2]
        halves = [jnp.where(core == 0, a[...], b[...]) for a, b in ((ci, cg), (other_ci, other_cg))]
        sums = lax.dot_general(
            y_ref[...], jnp.concatenate(halves, axis=1), CONTRACT_ROWS, preferred_element_type=F32
        )
        for n, half in enumerate((core, 1 - core)):
            for q in range(per):
                at = (n * per + q) * columns
                scratch[half * per + q] = sums[:, at : at + columns]
        for j, out in enumerate(outs):
            out[...] = scratch[place_ref[1] ^ j].astype(out.dtype)

    outs = [struct((rank, columns), BF16 if j else F32) for j in range(rep_size)]
    operands = (y, *cotangents)
    return pl.pallas_call(
        body,
        grid_spec=one_step(operands, len(outs), [pltpu.VMEM((rep_size, rank, columns), F32)]),
        out_shape=outs,
        compiler_params=grant(10),
        name="token_sums",
    )(place, *operands)


def add_up(place, parts, fs_size):
    rank, columns = parts[0].shape
    rows = rank // fs_size
    split = fs_size <= DIRECT

    def body(place_ref, *refs):
        sums, outs, scratch = refs[: len(parts)], refs[len(parts) : -1], refs[-1]
        total = tree([ref[...].astype(F32) for ref in sums])
        if not split:
            outs[0][...] = total.astype(BF16)
            return
        for k in range(fs_size):
            scratch[k] = total[k * rows : (k + 1) * rows, :]
        for k, out in enumerate(outs):
            out[...] = scratch[place_ref[0] ^ k].astype(out.dtype)

    outs = [struct((rank, columns), BF16)]
    if split:
        outs = [struct((rows, columns), BF16 if k else F32) for k in range(fs_size)]
    return pl.pallas_call(
        body,
        grid_spec=one_step(parts, len(outs), [pltpu.VMEM((fs_size, rows, columns), F32)]),
        out_shape=outs,
        compiler_params=grant(4),
        name="add_up",
    )(place, *parts)


def tree(values):
    while len(values) > 1:
        values = [sum(values[i : i + 2][1:], values[i]) for i in range(0, len(values), 2)]
    return values[0]


def advance(first, second, low):
    return 0.8 * first + 0.2 * low, 0.95 * second + 0.05 * low * low


def norm_block(place, parts, local, remote):
    rows, columns = parts[0].shape
    width = local[0].shape[1]
    count = len(parts)

    def body(place_ref, *refs):
        sums, states, (low_ref, normed_ref) = refs[:count], refs[count:-2], refs[-2:]
        low = tree([ref[...].astype(F32) for ref in sums]).astype(BF16)
        low_ref[...] = low
        start = place_ref[1] * columns
        core = place_ref[2]
        here = (start >= width) == (core == 1)
        at = pl.ds(pl.multiple_of(lax.rem(start, width), columns), columns)
        old = []
        for n in (0, 1):
            mine, remote = (jnp.where(core == 0, states[m + n][:, at], states[m + n + 2][:, at]) for m in (0, 4))
            old.append(jnp.where(here, mine, remote))
        first, second = advance(*old, low.astype(F32))
        normed_ref[...] = (first / jnp.sqrt(second)).astype(BF16)

    operands = (*parts, *local, *remote)
    block = struct((rows, columns), BF16)
    return pl.pallas_call(
        body,
        grid_spec=one_step(operands, 2),
        out_shape=[block, block],
        compiler_params=grant(3),
        name="norm_block",
    )(place, *operands)


def flat_rows(values):
    count, rows, width = values.shape
    if rows % 16:
        return values.astype(F32).reshape(count * rows, width).astype(BF16)
    return values.reshape(count * rows, width)


def gram(u):
    model, rank = u.shape

    def body(u_ref, out_ref):
        whole = u_ref[...]
        products = lax.dot_general(whole, whole, CONTRACT_ROWS, preferred_element_type=F32)
        upper = products.astype(BF16)
        out_ref[0] = upper
        out_ref[1] = (products - upper.astype(F32)).astype(BF16)

    return pl.pallas_call(
        body,
        out_shape=struct((2, rank, rank), BF16),
        compiler_params=grant(8),
        cost_estimate=pl.CostEstimate(flops=2 * model * rank * rank, bytes_accessed=0, transcendentals=0),
        name="gram",
    )(u)


def squares(place, blocks, products, fs_size, width):
    total, columns = blocks[0].shape
    rows = total // (fs_size + 1)
    tail = 16

    def body(place_ref, *refs):
        pieces, (gram_ref, keep_ref, give_ref, scratch, low_scratch) = refs[:-5], refs[-5:]
        fs, rep, core = place_ref[0], place_ref[1], place_ref[2]
        for j, ref in enumerate(pieces):
            start = (rep ^ j) * columns
            half = start // width
            at = pl.ds(pl.multiple_of(lax.rem(start, width), columns), columns)
            for k in range(fs_size):
                scratch[half, fs ^ k, :, at] = ref[k * rows : (k + 1) * rows, :]
            low_scratch[half, :, at] = ref[-rows:, :]
        square = 0.0
        for half in (0, 1):
            part = flat_rows(scratch[half])
            image = dot(gram_ref[0], part) + dot(gram_ref[1], part)
            square = square + jnp.sum(part.astype(F32) * image)
        for out, half in ((keep_ref, core), (give_ref, 1 - core)):
            out[: fs_size * rows, :] = flat_rows(scratch[half])
            out[fs_size * rows : total, :] = low_scratch[half]
            rest = jnp.full((tail, 128), square, F32)
            for n in range(3):
                piece = rest.astype(BF16)
                out[total:, n * 128 : (n + 1) * 128] = piece
                rest = rest - piece.astype(F32)

    operands = (*blocks, products)
    out = struct((total + tail, width), BF16)
    return pl.pallas_call(
        body,
        grid_spec=one_step(
            operands,
            2,
            [pltpu.VMEM((2, fs_size, rows, width), BF16), pltpu.VMEM((2, rows, width), BF16)],
        ),
        out_shape=[out, out],
        compiler_params=grant(6),
        name="squares",
    )(place, *operands)


def locate(arrays, first, rows):
    return [(first + n, offset) for n, array in enumerate(arrays) for offset in range(0, array.shape[0], rows)]


class Side:
    def __init__(self, number, place_ref, normed_ref, factor_ref, master_refs, state_refs, old_refs, places, rep_size, entries):
        self.rows, self.width = master_refs[0].shape
        self.rank = factor_ref.shape[1]
        self.moment_rows = state_refs[0].shape[0]
        self.half = self.rows // 2
        self.fs = place_ref[0]
        self.held = half_of(place_ref[1], rep_size)[number]
        self.is_in = place_ref[2] == number
        self.normed_ref, self.factor_ref, self.master_refs, self.state_refs = normed_ref, factor_ref, master_refs, state_refs
        self.old_refs, self.places = old_refs, places
        last = self.rank + self.moment_rows
        square = sum(normed_ref[last : last + 1, n * 128 : n * 128 + 1].astype(F32) for n in (2, 1, 0))
        self.scale = lax.rsqrt(square / entries + 0.1)

    def start(self, k):
        return (self.fs ^ k) * self.rows

    def product(self, start, size):
        rows = self.factor_ref[pl.ds(pl.multiple_of(start, size), size), :]
        return dot(rows, self.normed_ref[: self.rank, :])

    def own_rows(self, update_ref, master_ref, copy_ref):
        update = self.product(self.start(0), self.rows) * self.scale
        old = jnp.where(self.is_in, self.master_refs[0][...], self.master_refs[1][...])
        step = 0.05 * update
        update_ref[...] = update
        master_ref[...] = old - step
        copy_ref[...] = (old.astype(BF16).astype(F32) - step).astype(BF16)

    def other_rows(self, k, copy_ref):
        half = self.half
        for other in (0, 1):
            which = 1 - self.held if other else self.held
            number, offset = self.places[k - 1][other]
            step = (0.05 * self.scale) * self.product(self.start(k) + which * half, half)
            old = self.old_refs[number][offset : offset + half, :].astype(F32)
            copy_ref[pl.ds(pl.multiple_of(which * half, half), half), :] = (old - step).astype(BF16)

    def moments(self, first_ref, second_ref):
        low = self.normed_ref[self.rank : self.rank + self.moment_rows, :].astype(F32)
        fi, si, fg, sg = self.state_refs
        old = [jnp.where(self.is_in, a[...], b[...]) for a, b in ((fi, fg), (si, sg))]
        first_ref[...], second_ref[...] = advance(*old, low)


def prepare(place, normed, factor, masters, state, olds, places, ready, rep_size, entries):
    rows, width = masters[0].shape
    moment_rows = state[0].shape[0]

    def body(place_ref, n_ref, u_ref, im_ref, gm_ref, fi, si, fg, sg, *refs):
        old_refs, (mine, small, spread) = refs[: len(olds)], refs[len(olds) :]
        side = Side(0, place_ref, n_ref, u_ref, (im_ref, gm_ref), (fi, si, fg, sg), old_refs, places, rep_size, entries)
        side.own_rows(mine.at[1], mine.at[0], spread.at[0])
        side.moments(small.at[0], small.at[1])
        for k in range(1, ready + 1):
            side.other_rows(k, spread.at[k])

    operands = (normed, factor, *masters, *state, *olds)
    return pl.pallas_call(
        body,
        grid_spec=one_step(operands, 3),
        out_shape=[
            struct((2, rows, width), F32),
            struct((2, moment_rows, width), F32),
            struct((ready + 1, rows, width), BF16),
        ],
        compiler_params=grant(10),
        name="prepare",
    )(place, *operands)


def finish(place, normed, factors, masters, state, olds, places, prepared, ready, rep_size, entries):
    rows, width = masters[0].shape
    model = factors[0].shape[0]
    moment_rows = state[0].shape[0]
    fs_size = model // rows
    counts = [len(arrays) for arrays in olds]

    def body(place_ref, no_ref, nt_ref, uo_ref, ut_ref, im_ref, gm_ref, fi, si, fg, sg, *refs):
        old_refs, refs = (refs[: counts[0]], refs[counts[0] : sum(counts)]), refs[sum(counts) :]
        (own_mine, own_small, own_spread), outs, (spread, mine, small, sems) = refs[:3], refs[3:13], refs[13:]
        sides = [
            Side(n, place_ref, *pair, (im_ref, gm_ref), (fi, si, fg, sg), old_refs[n], places[n], rep_size, entries)
            for n, pair in enumerate(((no_ref, uo_ref), (nt_ref, ut_ref)))
        ]
        sent = []

        def send(side, source, number, k=None):
            targets = [outs[number], outs[number + 1]]
            if k is not None:
                block = pl.ds(pl.multiple_of(side.start(k), rows), rows)
                targets = [target.at[block, :] for target in targets]
            sem = sems.at[len(sent)]
            for wanted, target in zip((side.is_in, jnp.logical_not(side.is_in)), targets):

                @pl.when(wanted)
                def _(target=target):
                    pltpu.make_async_copy(source, target, sem).start()

            sent.append(pltpu.make_async_copy(source, targets[0], sem))

        own, other = sides
        for n in (0, 1):
            send(own, own_mine.at[n], 2 * n)
        for k in range(ready + 1):
            send(own, own_spread.at[k], 8, k)
        for n in (0, 1):
            send(own, own_small.at[n], 4 + 2 * n)
        other.own_rows(mine.at[1], mine.at[0], spread.at[0])
        for n in (0, 1):
            send(other, mine.at[n], 2 * n)
        send(other, spread.at[0], 8, 0)
        other.moments(small.at[0], small.at[1])
        for n in (0, 1):
            send(other, small.at[n], 4 + 2 * n)
        for k in range(1, fs_size):
            other.other_rows(k, spread.at[k])
            send(other, spread.at[k], 8, k)
        for k in range(ready + 1, fs_size):
            own.other_rows(k, spread.at[fs_size + k - ready - 1])
            send(own, spread.at[fs_size + k - ready - 1], 8, k)
        for copy in sent:
            copy.wait()

    operands = (*normed, *factors, *masters, *state, *olds[0], *olds[1], *prepared)
    moment, owned, big = struct((moment_rows, width), F32), struct((rows, width), F32), struct((model, width), BF16)
    scratch = [
        pltpu.VMEM((2 * fs_size - ready - 1, rows, width), BF16),
        pltpu.VMEM((2, rows, width), F32),
        pltpu.VMEM((2, moment_rows, width), F32),
        pltpu.SemaphoreType.DMA((2 * (4 + fs_size),)),
    ]
    return pl.pallas_call(
        body,
        grid_spec=one_step(operands, 10, scratch, pltpu.HBM),
        out_shape=[owned] * 4 + [moment] * 4 + [big] * 2,
        compiler_params=grant(20),
        name="finish",
    )(place, *operands)


def half_of(rep, rep_size):
    return rep & 1, (rep >> ((rep_size // 2).bit_length() - 1)) & 1


def layer(
    sizes,
    saved_input,
    cot_input,
    cot_gate,
    in_master,
    gate_master,
    in_factor,
    gate_factor,
    in_first,
    in_second,
    gate_first,
    gate_second,
):
    fs_size, rep_size, tp_size = sizes
    rows, width = in_master.shape
    part = rows // rep_size
    fs, rep, tp = (lax.axis_index(name) for name in ("fs", "rep", "tp"))
    place = jnp.stack([fs, rep, tp]).astype(jnp.int32)

    half = rows // 2

    def cut(values, index, size):
        return lax.dynamic_slice_in_dim(values, index * size, size, 0)

    def after(values, *others):
        return lax.optimization_barrier((values, *others))[0]

    def own(of_in, of_gate):
        return jnp.where(tp == 0, of_in, of_gate)

    direct = from_others(own(cut(in_factor, rep, part), cut(gate_factor, rep, part)), "fs", fs_size)
    state = (in_first, in_second, gate_first, gate_second)
    cotangents = [cot_input, cot_gate]
    cotangents += [swap(after(values, *direct), "tp", tp_size, 1) for values in cotangents]
    x = stage(saved_input)
    relayed = from_others(jnp.concatenate(direct, axis=0), "rep", rep_size)

    old = held_rows(place, (in_master, gate_master), rep_size)
    if fs_size == 4:
        near = swap(old, "fs", fs_size, 1)
        far = swap(after(old, *direct), "fs", fs_size, 2)
        halves = [near, far]
    else:
        halves = from_others(old, "fs", fs_size)

    def rest_of(values, cue):
        ready = after(values, cue).reshape(-1, 2, half, width)
        return [
            swap(ready[:, side].reshape(-1, width), "rep", rep_size, step)
            for side, step in ((0, 1), (1, rep_size // 2))
        ]

    y, u_own = project(place, x, in_factor, gate_factor, direct, relayed, rep_size)
    sums = token_sums(place, y, cotangents, rep_size)
    parts = [sums[0]] + [swap(sums[j], "rep", rep_size, j) for j in range(1, rep_size)]
    u_other = swap(after(u_own, sums[-1]), "tp", tp_size, 1)
    remote_state = [swap(after(values, sums[-1]), "tp", tp_size, 1) for values in state]
    products = gram(after(u_own, sums[-1]))
    rest = rest_of(halves[0], sums[-1])
    sums = add_up(place, parts, fs_size)
    if fs_size <= DIRECT:
        parts = [sums[0]] + [swap(sums[k], "fs", fs_size, k) for k in range(1, fs_size)]
    else:
        parts = [lax.psum_scatter(sums[0], "fs", scatter_dimension=0, tiled=True)]
    low, normed = norm_block(place, parts, state, remote_state)
    column = jnp.concatenate([normed, *from_others(normed, "fs", fs_size), low], axis=0)
    if fs_size == 4:
        rest += rest_of(far, sums[-1])
        last = [swap(after(far, sums[-1])[:half], "fs", fs_size, 1)]
        last.append(swap(after(far, normed)[half:], "fs", fs_size, 1))
        last_rest = [swap(after(last[0], column), "rep", rep_size, 1)]
        last_rest.append(swap(after(last[1], column), "rep", rep_size, rep_size // 2))
    blocks = [column] + from_others(column, "rep", rep_size)
    kept, given = squares(place, blocks, products, fs_size, width)
    got = swap(given, "tp", tp_size, 1)

    entries = float(rows * fs_size * width * tp_size)
    masters = (in_master, gate_master)
    if fs_size == 4:
        ready = 2
        olds = [[near, far, rest[side], rest[2 + side], last[side], last_rest[side]] for side in (0, 1)]
        places = [[[(0, side * half), (2, 0)], [(1, side * half), (3, 0)], [(4, 0), (5, 0)]] for side in (0, 1)]
    else:
        ready = 0
        olds = [[*halves, *rest[side::2]] for side in (0, 1)]
        found = [(locate(halves, 0, half)[side::2], locate(rest[side::2], len(halves), half)) for side in (0, 1)]
        places = [list(zip(*pair)) for pair in found]
    early = olds[0][: 2 * ready]
    prepared = prepare(place, kept, u_own, masters, state, early, places[0], ready, rep_size, entries)
    outs = finish(
        place, (kept, got), (u_own, u_other), masters, state, olds, places, prepared, ready, rep_size, entries
    )
    order = (0, 1, 2, 3, 4, 6, 5, 7, 8, 9)
    return tuple(outs[n] for n in order)


def solution(mesh):
    sizes = tuple(mesh.shape[name] for name in ("fs", "rep", "tp"))
    owned, moment = P("fs", "tp"), P("fs", "tp")
    return jax.shard_map(
        functools.partial(layer, sizes),
        mesh=mesh,
        in_specs=(
            P(("fs", "rep"), None),
            P(("fs", "rep"), "tp"),
            P(("fs", "rep"), "tp"),
            owned,
            owned,
            P("fs", None),
            P("fs", None),
            moment,
            moment,
            moment,
            moment,
        ),
        out_specs=(owned,) * 4 + (moment,) * 4 + (P(None, "tp"),) * 2,
        check_vma=False,
    )
```

time: 111 us -> 99.1 us (0.89)
  waiting for transfers between devices: 47.8 us -> 34.9 us
  starting transfers between devices: 36 us -> 44.2 us
  local copies, waits for them, and re-layouts: 10.5 us -> 4.84 us
  Pallas kernels: 14.2 us -> 12.9 us
    ppermute x28 -> x36, waiting for transfers between devices: 47.8 us -> 34.9 us  [swap(): return lax.ppermute(values, axis, [(i, i ^ step) for i in range(size)])]
    ppermute x28 -> x36, starting transfers between devices: 36 us -> 44.2 us  [swap(): return lax.ppermute(values, axis, [(i, i ^ step) for i in range(size)])]
    unnamed x36 -> x32, local copies, waits for them, and re-layouts: 9.63 us -> 4.72 us
    pallas_call x1, Pallas kernels: 3 us -> 1.86 us  [project(): pl.pallas_call(body, grid_spec=one_step(operands, 2), out_shape=[struct((...]
    pallas_call x4 -> x5, Pallas kernels: 8.3 us -> 8.11 us  [the longest x1 4.44 us: finish(): pl.pallas_call(body, grid_spec=one_step(operands, 10, scratch, pltpu.HBM)...]
  transfers between devices with their start and end apart: 28 -> 36, of which waited for: 14 -> 19; matrix products, arithmetic and copies ran while one was open for 2% -> 0% of each run, Pallas kernels for 6% -> 9%
where the time goes in v2:
time: 99.1 us; the launch traced here: 98.8 us
  starting transfers between devices  44.2 us (45%)
  waiting for transfers between devices  34.9 us (35%)
  Pallas kernels  12.9 us (13%)
  local copies, waits for them, and re-layouts  4.84 us (5%)
    ppermute x36, starting transfers between devices, swap(): return lax.ppermute(values, axis, [(i, i ^ step) for i in range(size)])  44.2 us
    ppermute x36, waiting for transfers between devices, swap(): return lax.ppermute(values, axis, [(i, i ^ step) for i in range(size)])  34.9 us
    unnamed x32, local copies, waits for them, and re-layouts  4.72 us
    pallas_call x1, Pallas kernels, finish(): pl.pallas_call(body, grid_spec=one_step(operands, 10, scratch, pltpu.HBM)...  4.44 us
  transfers between devices with their start and end apart: 36, of which 19 were waited for; matrix products, arithmetic and copies ran while one was open for 0% of the time, Pallas kernels for 9%

profile of v2, /device:TPU:0, one launch (start us, length us, event | category | flops | bytes accessed | tf_op | source)
XLA Modules:
  0.0 98.8 jit_solution(8442077952315804661)
XLA Ops:
  1.5 5.1 %collective-permute-start.2 = (bf16[128,256]{1,0:T(8,128)(2,1)S(1)}, bf16[128,256]{1,0:T(8,128)(2,1)S(1)}, u32[]{:S(2)}, u32[]{:S(2)}) collective-permute-start(bf16[128,256]{1,0:T(8,128)(2,1)S(1)} %dynamic-slice_select_fusion), channel_id=1, source_target_pairs={{0,24},{8,16},{16,8},{24,0},{1,25},{9,17},{17,9},{25,1},{2,26},{10... | collective-permute-start | bytes 196616 | tf_op jit(solution)/shard_map/ppermute | solution.py:22
  7.3 1.8 %collective-permute-done.2.refs_2_ = bf16[128,256]{1,0:T(8,128)(2,1)S(1)} collective-permute-done((bf16[128,256]{1,0:T(8,128)(2,1)S(1)}, bf16[128,256]{1,0:T(8,128)(2,1)S(1)}, u32[]{:S(2)}, u32[]{:S(2)}) %collective-permute-start.2) | collective-permute-done | bytes 65568 | tf_op jit(solution)/shard_map/ppermute | solution.py:22
  9.2 3.1 %collective-permute-done.1.refs_1_ = bf16[128,256]{1,0:T(8,128)(2,1)S(1)} collective-permute-done((bf16[128,256]{1,0:T(8,128)(2,1)S(1)}, bf16[128,256]{1,0:T(8,128)(2,1)S(1)}, u32[]{:S(2)}, u32[]{:S(2)}) %collective-permute-start.1) | collective-permute-done | bytes 65568 | tf_op jit(solution)/shard_map/ppermute | solution.py:22
  12.8 2.5 %collective-permute-start.5 = (bf16[384,256]{1,0:T(8,128)(2,1)S(1)}, bf16[384,256]{1,0:T(8,128)(2,1)S(1)}, u32[]{:S(2)}, u32[]{:S(2)}) collective-permute-start(bf16[384,256]{1,0:T(8,128)(2,1)S(1)} %constant_dynamic-update-slice_fusion), channel_id=1, source_target_pairs={{0,6},{2,4},{4,2},{6,0},{1,7},{3,5},{5,3},{7,1},{8,14},{10,12},{12... | collective-permute-start | bytes 589832 | tf_op jit(solution)/shard_map/ppermute | solution.py:22
  20.7 1.7 %collective-permute-start.27 = (bf16[512,512]{1,0:T(8,128)(2,1)S(1)}, bf16[512,512]{1,0:T(8,128)(2,1)S(1)}, u32[]{:S(2)}, u32[]{:S(2)}) collective-permute-start(bf16[512,512]{1,0:T(8,128)(2,1)S(1)} %held_rows.1), channel_id=1, source_target_pairs={{0,16},{8,24},{16,0},{24,8},{1,17},{9,25},{17,1},{25,9},{2,18},{10... | collective-permute-start | bytes 1572872 | tf_op jit(solution)/shard_map/ppermute | solution.py:22
  22.4 2.4 %collective-permute-done.4.refs_4_ = bf16[384,256]{1,0:T(8,128)(2,1)S(1)} collective-permute-done((bf16[384,256]{1,0:T(8,128)(2,1)S(1)}, bf16[384,256]{1,0:T(8,128)(2,1)S(1)}, u32[]{:S(2)}, u32[]{:S(2)}) %collective-permute-start.4) | collective-permute-done | bytes 196640 | tf_op jit(solution)/shard_map/ppermute | solution.py:22
  24.8 1.5 %collective-permute-start.3 = (bf16[384,256]{1,0:T(8,128)(2,1)S(1)}, bf16[384,256]{1,0:T(8,128)(2,1)S(1)}, u32[]{:S(2)}, u32[]{:S(2)}) collective-permute-start(bf16[384,256]{1,0:T(8,128)(2,1)S(1)} %constant_dynamic-update-slice_fusion), channel_id=1, source_target_pairs={{0,2},{2,0},{4,6},{6,4},{1,3},{3,1},{5,7},{7,5},{8,10},{10,8},{12,... | collective-permute-start | bytes 589832 | tf_op jit(solution)/shard_map/ppermute | solution.py:22
  26.3 2.2 %copy-done.4 = bf16[1024,2048]{1,0:T(8,128)(2,1)S(1)} copy-done((bf16[1024,2048]{1,0:T(8,128)(2,1)S(1)}, bf16[1024,2048]{1,0:T(8,128)(2,1)}, u32[]{:S(2)}) %copy-start.4) | copy-done | bytes 4194328
  28.8 2.8 %collective-permute-done.3.refs_3_ = bf16[384,256]{1,0:T(8,128)(2,1)S(1)} collective-permute-done((bf16[384,256]{1,0:T(8,128)(2,1)S(1)}, bf16[384,256]{1,0:T(8,128)(2,1)S(1)}, u32[]{:S(2)}, u32[]{:S(2)}) %collective-permute-start.3) | collective-permute-done | bytes 196640 | tf_op jit(solution)/shard_map/ppermute | solution.py:22
  31.7 1.9 %project.1 = (bf16[1024,256]{1,0:T(8,128)(2,1)S(1)}, bf16[2048,256]{1,0:T(8,128)(2,1)S(1)}) custom-call(s32[3]{0:T(128)S(1)} %pad_add_fusion.place_ref, bf16[1024,2048]{1,0:T(8,128)(2,1)S(1)} %stage.1.x_ref, bf16[512,256]{1,0:T(8,128)(2,1)S(1)} %copy-done.11, bf16[512,256]{1,0:T(8,128)(2,1)S(1)} %copy-done.12, ...), custom_call_target="tpu_custom_call" | custom-call | tf_op jit(solution)/shard_map/project/pallas_call | solution.py:116
  33.6 1.3 %token_sums.1 = (f32[256,256]{1,0:T(8,128)S(1)}, bf16[256,256]{1,0:T(8,128)(2,1)S(1)}, bf16[256,256]{1,0:T(8,128)(2,1)S(1)}, bf16[256,256]{1,0:T(8,128)(2,1)S(1)}) custom-call(s32[3]{0:T(128)S(1)} %pad_add_fusion.place_ref, bf16[1024,256]{1,0:T(8,128)(2,1)S(1)} %get-tuple-element.50.y_ref, bf16[1024,512]{1,0:T(8,128)(2,1)S(1)} %copy-done.9, ...), custom_call_target="tpu_custom_call" | custom-call | tf_op jit(solution)/shard_map/token_sums/pallas_call | solution.py:147
  35.0 1.6 %collective-permute-start.8 = (bf16[256,256]{1,0:T(8,128)(2,1)S(1)}, bf16[256,256]{1,0:T(8,128)(2,1)S(1)}, u32[]{:S(2)}, u32[]{:S(2)}) collective-permute-start(bf16[256,256]{1,0:T(8,128)(2,1)S(1)} %get-tuple-element.54), channel_id=1, source_target_pairs={{0,2},{2,0},{4,6},{6,4},{1,3},{3,1},{5,7},{7,5},{8,10},{10,8},{12,... | collective-permute-start | bytes 393224 | tf_op jit(solution)/shard_map/ppermute | solution.py:22
  36.8 1.7 %collective-permute-start.10 = (bf16[256,256]{1,0:T(8,128)(2,1)S(1)}, bf16[256,256]{1,0:T(8,128)(2,1)S(1)}, u32[]{:S(2)}, u32[]{:S(2)}) collective-permute-start(bf16[256,256]{1,0:T(8,128)(2,1)S(1)} %get-tuple-element.56), channel_id=1, source_target_pairs={{0,6},{2,4},{4,2},{6,0},{1,7},{3,5},{5,3},{7,1},{8,14},{10,12},{12... | collective-permute-start | bytes 393224 | tf_op jit(solution)/shard_map/ppermute | solution.py:22
  38.5 4.0 %collective-permute-done.26.refs_0_.refs_6_ = bf16[512,512]{1,0:T(8,128)(2,1)S(1)} collective-permute-done((bf16[512,512]{1,0:T(8,128)(2,1)S(1)}, bf16[512,512]{1,0:T(8,128)(2,1)S(1)}, u32[]{:S(2)}, u32[]{:S(2)}) %collective-permute-start.26) | collective-permute-done | bytes 524320 | tf_op jit(solution)/shard_map/ppermute | solution.py:22
  46.0 3.2 %collective-permute-start.12 = (bf16[64,256]{1,0:T(8,128)(2,1)S(1)}, bf16[64,256]{1,0:T(8,128)(2,1)S(1)}, u32[]{:S(2)}, u32[]{:S(2)}) collective-permute-start(bf16[64,256]{1,0:T(8,128)(2,1)S(1)} %get-tuple-element.59), channel_id=1, source_target_pairs={{0,16},{8,24},{16,0},{24,8},{1,17},{9,25},{17,1},{25,9},{2,18},{10... | collective-permute-start | bytes 98312 | tf_op jit(solution)/shard_map/ppermute | solution.py:22
  51.0 4.2 %collective-permute-done.13.refs_3_ = bf16[64,256]{1,0:T(8,128)(2,1)S(1)} collective-permute-done((bf16[64,256]{1,0:T(8,128)(2,1)S(1)}, bf16[64,256]{1,0:T(8,128)(2,1)S(1)}, u32[]{:S(2)}, u32[]{:S(2)}) %collective-permute-start.13) | collective-permute-done | bytes 32800 | tf_op jit(solution)/shard_map/ppermute | solution.py:22
  57.0 3.3 %collective-permute-start.18 = (bf16[64,256]{1,0:T(8,128)(2,1)S(1)}, bf16[64,256]{1,0:T(8,128)(2,1)S(1)}, u32[]{:S(2)}, u32[]{:S(2)}) collective-permute-start(bf16[64,256]{1,0:T(8,128)(2,1)S(1)} %get-tuple-element.65), channel_id=1, source_target_pairs={{0,8},{8,0},{16,24},{24,16},{1,9},{9,1},{17,25},{25,17},{2,10},{10... | collective-permute-start | bytes 98312 | tf_op jit(solution)/shard_map/ppermute | solution.py:22
  60.3 2.0 %collective-permute-done.18 = bf16[64,256]{1,0:T(8,128)(2,1)S(1)} collective-permute-done((bf16[64,256]{1,0:T(8,128)(2,1)S(1)}, bf16[64,256]{1,0:T(8,128)(2,1)S(1)}, u32[]{:S(2)}, u32[]{:S(2)}) %collective-permute-start.18) | collective-permute-done | bytes 32800 | tf_op jit(solution)/shard_map/ppermute | solution.py:22
  62.4 2.5 %collective-permute-start.23 = (bf16[320,256]{1,0:T(8,128)(2,1)S(1)}, bf16[320,256]{1,0:T(8,128)(2,1)S(1)}, u32[]{:S(2)}, u32[]{:S(2)}) collective-permute-start(bf16[320,256]{1,0:T(8,128)(2,1)S(1)} %constant_dynamic-update-slice_fusion.3.refs_0_), channel_id=1, source_target_pairs={{0,6},{2,4},{4,2},{6,0},{1,7},{3,5},{5,3},{7,1},{8,14},{10,12},{12... | collective-permute-start | bytes 491528 | tf_op jit(solution)/shard_map/ppermute | solution.py:22
  65.0 1.9 %collective-permute-start.34 = (bf16[256,512]{1,0:T(8,128)(2,1)S(1)}, bf16[256,512]{1,0:T(8,128)(2,1)S(1)}, u32[]{:S(2)}, u32[]{:S(2)}) collective-permute-start(bf16[256,512]{1,0:T(8,128)(2,1)S(1)} %slice.23), channel_id=1, source_target_pairs={{0,8},{8,0},{16,24},{24,16},{1,9},{9,1},{17,25},{25,17},{2,10},{10... | collective-permute-start | bytes 786440 | tf_op jit(solution)/shard_map/ppermute | solution.py:22
  67.4 1.4 %collective-permute-done.23.refs_3_ = bf16[320,256]{1,0:T(8,128)(2,1)S(1)} collective-permute-done((bf16[320,256]{1,0:T(8,128)(2,1)S(1)}, bf16[320,256]{1,0:T(8,128)(2,1)S(1)}, u32[]{:S(2)}, u32[]{:S(2)}) %collective-permute-start.23) | collective-permute-done | bytes 163872 | tf_op jit(solution)/shard_map/ppermute | solution.py:22
  68.8 1.5 %collective-permute-start.21 = (bf16[320,256]{1,0:T(8,128)(2,1)S(1)}, bf16[320,256]{1,0:T(8,128)(2,1)S(1)}, u32[]{:S(2)}, u32[]{:S(2)}) collective-permute-start(bf16[320,256]{1,0:T(8,128)(2,1)S(1)} %constant_dynamic-update-slice_fusion.3.refs_0_), channel_id=1, source_target_pairs={{0,2},{2,0},{4,6},{6,4},{1,3},{3,1},{5,7},{7,5},{8,10},{10,8},{12,... | collective-permute-start | bytes 491528 | tf_op jit(solution)/shard_map/ppermute | solution.py:22
  70.3 1.9 %collective-permute-done.22.refs_2_ = bf16[320,256]{1,0:T(8,128)(2,1)S(1)} collective-permute-done((bf16[320,256]{1,0:T(8,128)(2,1)S(1)}, bf16[320,256]{1,0:T(8,128)(2,1)S(1)}, u32[]{:S(2)}, u32[]{:S(2)}) %collective-permute-start.22) | collective-permute-done | bytes 163872 | tf_op jit(solution)/shard_map/ppermute | solution.py:22
  72.7 2.1 %collective-permute-done.21.refs_1_ = bf16[320,256]{1,0:T(8,128)(2,1)S(1)} collective-permute-done((bf16[320,256]{1,0:T(8,128)(2,1)S(1)}, bf16[320,256]{1,0:T(8,128)(2,1)S(1)}, u32[]{:S(2)}, u32[]{:S(2)}) %collective-permute-start.21) | collective-permute-done | bytes 163872 | tf_op jit(solution)/shard_map/ppermute | solution.py:22
  77.3 1.2 %squares.1 = (bf16[336,512]{1,0:T(8,128)(2,1)S(1)}, bf16[336,512]{1,0:T(8,128)(2,1)S(1)}) custom-call(s32[3]{0:T(128)S(1)} %pad_add_fusion.place_ref, bf16[320,256]{1,0:T(8,128)(2,1)S(1)} %constant_dynamic-update-slice_fusion.3.refs_0_, bf16[320,256]{1,0:T(8,128)(2,1)S(1)} %collective-permute-done.21.refs_1_, ...), custom_call_target="tpu_custom_call" | custom-call | tf_op jit(solution)/shard_map/squares/pallas_call | solution.py:282
  78.7 3.2 %collective-permute-start.33 = (bf16[256,512]{1,0:T(8,128)(2,1)S(1)}, bf16[256,512]{1,0:T(8,128)(2,1)S(1)}, u32[]{:S(2)}, u32[]{:S(2)}) collective-permute-start(bf16[256,512]{1,0:T(8,128)(2,1)S(1)} %get-tuple-element.90), channel_id=1, source_target_pairs={{0,4},{2,6},{4,0},{6,2},{1,5},{3,7},{5,1},{7,3},{8,12},{10,14},{12... | collective-permute-start | bytes 786440 | tf_op jit(solution)/shard_map/ppermute | solution.py:22
  82.5 1.5 %collective-permute-start.31 = (bf16[256,512]{1,0:T(8,128)(2,1)S(1)}, bf16[256,512]{1,0:T(8,128)(2,1)S(1)}, u32[]{:S(2)}, u32[]{:S(2)}) collective-permute-start(bf16[256,512]{1,0:T(8,128)(2,1)S(1)} %collective-permute-done.30.refs_4_), channel_id=1, source_target_pairs={{0,2},{2,0},{4,6},{6,4},{1,3},{3,1},{5,7},{7,5},{8,10},{10,8},{12,... | collective-permute-start | bytes 786440 | tf_op jit(solution)/shard_map/ppermute | solution.py:22
  84.0 2.1 %collective-permute-done.29.refs_3_ = bf16[256,512]{1,0:T(8,128)(2,1)S(1)} collective-permute-done((bf16[256,512]{1,0:T(8,128)(2,1)S(1)}, bf16[256,512]{1,0:T(8,128)(2,1)S(1)}, u32[]{:S(2)}, u32[]{:S(2)}) %collective-permute-start.29) | collective-permute-done | bytes 262176 | tf_op jit(solution)/shard_map/ppermute | solution.py:22
  86.1 3.4 %collective-permute-start.35 = (bf16[256,512]{1,0:T(8,128)(2,1)S(1)}, bf16[256,512]{1,0:T(8,128)(2,1)S(1)}, u32[]{:S(2)}, u32[]{:S(2)}) collective-permute-start(bf16[256,512]{1,0:T(8,128)(2,1)S(1)} %collective-permute-done.34.refs_10_), channel_id=1, source_target_pairs={{0,4},{2,6},{4,0},{6,2},{1,5},{3,7},{5,1},{7,3},{8,12},{10,14},{12... | collective-permute-start | bytes 786440 | tf_op jit(solution)/shard_map/ppermute | solution.py:22
  89.5 1.3 %prepare.1 = (f32[2,512,512]{2,1,0:T(8,128)S(1)}, f32[2,64,512]{2,1,0:T(8,128)S(1)}, bf16[3,512,512]{2,1,0:T(8,128)(2,1)S(1)}) custom-call(s32[3]{0:T(128)S(1)} %pad_add_fusion.place_ref, bf16[336,512]{1,0:T(8,128)(2,1)S(1)} %get-tuple-element.69.n_ref.no_ref, bf16[2048,256]{1,0:T(8,128)(2,1)S(1)} %get-tuple-element.68.u_ref.uo_ref, ...), custom_call_target="tpu_custom_call" | custom-call | tf_op jit(solution)/shard_map/prepare/pallas_call | solution.py:358
  91.0 3.4 %collective-permute-done.35.refs_11_ = bf16[256,512]{1,0:T(8,128)(2,1)S(1)} collective-permute-done((bf16[256,512]{1,0:T(8,128)(2,1)S(1)}, bf16[256,512]{1,0:T(8,128)(2,1)S(1)}, u32[]{:S(2)}, u32[]{:S(2)}) %collective-permute-start.35) | collective-permute-done | bytes 262176 | tf_op jit(solution)/shard_map/ppermute | solution.py:22
  94.4 4.4 %finish.1 = (f32[512,512]{1,0:T(8,128)}, f32[512,512]{1,0:T(8,128)}, f32[512,512]{1,0:T(8,128)}, f32[512,512]{1,0:T(8,128)}, f32[64,512]{1,0:T(8,128)}, /*index=...) custom-call(s32[3]{0:T(128)S(1)} %pad_add_fusion.place_ref, ...), custom_call_target="tpu_custom_call" | custom-call | tf_op jit(solution)/shard_map/finish/pallas_call | solution.py:432
  (90 shorter events, 19.8 us)
Async XLA Ops:
  1.5 7.6 %collective-permute-start.2 = (bf16[128,256]{1,0:T(8,128)(2,1)S(1)}, bf16[128,256]{1,0:T(8,128)(2,1)S(1)}, u32[]{:S(2)}, u32[]{:S(2)}) collective-permute-start(bf16[128,256]{1,0:T(8,128)(2,1)S(1)} %dynamic-slice_select_fusion), channel_id=1, source_target_pairs={{0,24},{8,16},{16,8},{24,0},{1,25},{9,17},{17,9},{25,1},{2,26},{10... | collective-permute-start | bytes 196616 | tf_op jit(solution)/shard_map/ppermute | solution.py:22
  6.7 5.6 %collective-permute-start.1 = (bf16[128,256]{1,0:T(8,128)(2,1)S(1)}, bf16[128,256]{1,0:T(8,128)(2,1)S(1)}, u32[]{:S(2)}, u32[]{:S(2)}) collective-permute-start(bf16[128,256]{1,0:T(8,128)(2,1)S(1)} %dynamic-slice_select_fusion), channel_id=1, source_target_pairs={{0,16},{8,24},{16,0},{24,8},{1,17},{9,25},{17,1},{25,9},{2,18},{10... | collective-permute-start | bytes 196616 | tf_op jit(solution)/shard_map/ppermute | solution.py:22
  6.7 5.6 %collective-permute-start = (bf16[128,256]{1,0:T(8,128)(2,1)S(1)}, bf16[128,256]{1,0:T(8,128)(2,1)S(1)}, u32[]{:S(2)}, u32[]{:S(2)}) collective-permute-start(bf16[128,256]{1,0:T(8,128)(2,1)S(1)} %dynamic-slice_select_fusion), channel_id=1, source_target_pairs={{0,8},{8,0},{16,24},{24,16},{1,9},{9,1},{17,25},{25,17},{2,10},{10... | collective-permute-start | bytes 196616 | tf_op jit(solution)/shard_map/ppermute | solution.py:22
  12.3 21.2 %collective-permute-start.6 = (bf16[1024,512]{1,0:T(8,128)(2,1)}, bf16[1024,512]{1,0:T(8,128)(2,1)S(1)}, u32[]{:S(2)}, u32[]{:S(2)}) collective-permute-start(bf16[1024,512]{1,0:T(8,128)(2,1)} %ci.1), channel_id=1, source_target_pairs={{0,1},{1,0},{2,3},{3,2},{4,5},{5,4},{6,7},{7,6},{8,9},{9,8},{10,11... | collective-permute-start | bytes 3145736 | tf_op jit(solution)/shard_map/ppermute | solution.py:22
  12.3 21.2 %collective-permute-start.7 = (bf16[1024,512]{1,0:T(8,128)(2,1)}, bf16[1024,512]{1,0:T(8,128)(2,1)S(1)}, u32[]{:S(2)}, u32[]{:S(2)}) collective-permute-start(bf16[1024,512]{1,0:T(8,128)(2,1)} %cg.1), channel_id=1, source_target_pairs={{0,1},{1,0},{2,3},{3,2},{4,5},{5,4},{6,7},{7,6},{8,9},{9,8},{10,11... | collective-permute-start | bytes 3145736 | tf_op jit(solution)/shard_map/ppermute | solution.py:22
  12.8 7.9 %collective-permute-start.5 = (bf16[384,256]{1,0:T(8,128)(2,1)S(1)}, bf16[384,256]{1,0:T(8,128)(2,1)S(1)}, u32[]{:S(2)}, u32[]{:S(2)}) collective-permute-start(bf16[384,256]{1,0:T(8,128)(2,1)S(1)} %constant_dynamic-update-slice_fusion), channel_id=1, source_target_pairs={{0,6},{2,4},{4,2},{6,0},{1,7},{3,5},{5,3},{7,1},{8,14},{10,12},{12... | collective-permute-start | bytes 589832 | tf_op jit(solution)/shard_map/ppermute | solution.py:22
  15.3 9.5 %collective-permute-start.4 = (bf16[384,256]{1,0:T(8,128)(2,1)S(1)}, bf16[384,256]{1,0:T(8,128)(2,1)S(1)}, u32[]{:S(2)}, u32[]{:S(2)}) collective-permute-start(bf16[384,256]{1,0:T(8,128)(2,1)S(1)} %constant_dynamic-update-slice_fusion), channel_id=1, source_target_pairs={{0,4},{2,6},{4,0},{6,2},{1,5},{3,7},{5,1},{7,3},{8,12},{10,14},{12... | collective-permute-start | bytes 589832 | tf_op jit(solution)/shard_map/ppermute | solution.py:22
  19.0 23.5 %collective-permute-start.26 = (bf16[512,512]{1,0:T(8,128)(2,1)S(1)}, bf16[512,512]{1,0:T(8,128)(2,1)S(1)}, u32[]{:S(2)}, u32[]{:S(2)}) collective-permute-start(bf16[512,512]{1,0:T(8,128)(2,1)S(1)} %held_rows.1), channel_id=1, source_target_pairs={{0,8},{8,0},{16,24},{24,16},{1,9},{9,1},{17,25},{25,17},{2,10},{10... | collective-permute-start | bytes 1572872 | tf_op jit(solution)/shard_map/ppermute | solution.py:22
  20.7 25.1 %collective-permute-start.27 = (bf16[512,512]{1,0:T(8,128)(2,1)S(1)}, bf16[512,512]{1,0:T(8,128)(2,1)S(1)}, u32[]{:S(2)}, u32[]{:S(2)}) collective-permute-start(bf16[512,512]{1,0:T(8,128)(2,1)S(1)} %held_rows.1), channel_id=1, source_target_pairs={{0,16},{8,24},{16,0},{24,8},{1,17},{9,25},{17,1},{25,9},{2,18},{10... | collective-permute-start | bytes 1572872 | tf_op jit(solution)/shard_map/ppermute | solution.py:22
  24.8 6.8 %collective-permute-start.3 = (bf16[384,256]{1,0:T(8,128)(2,1)S(1)}, bf16[384,256]{1,0:T(8,128)(2,1)S(1)}, u32[]{:S(2)}, u32[]{:S(2)}) collective-permute-start(bf16[384,256]{1,0:T(8,128)(2,1)S(1)} %constant_dynamic-update-slice_fusion), channel_id=1, source_target_pairs={{0,2},{2,0},{4,6},{6,4},{1,3},{3,1},{5,7},{7,5},{8,10},{10,8},{12,... | collective-permute-start | bytes 589832 | tf_op jit(solution)/shard_map/ppermute | solution.py:22
  35.0 7.6 %collective-permute-start.8 = (bf16[256,256]{1,0:T(8,128)(2,1)S(1)}, bf16[256,256]{1,0:T(8,128)(2,1)S(1)}, u32[]{:S(2)}, u32[]{:S(2)}) collective-permute-start(bf16[256,256]{1,0:T(8,128)(2,1)S(1)} %get-tuple-element.54), channel_id=1, source_target_pairs={{0,2},{2,0},{4,6},{6,4},{1,3},{3,1},{5,7},{7,5},{8,10},{10,8},{12,... | collective-permute-start | bytes 393224 | tf_op jit(solution)/shard_map/ppermute | solution.py:22
  36.5 7.1 %collective-permute-start.9 = (bf16[256,256]{1,0:T(8,128)(2,1)S(1)}, bf16[256,256]{1,0:T(8,128)(2,1)S(1)}, u32[]{:S(2)}, u32[]{:S(2)}) collective-permute-start(bf16[256,256]{1,0:T(8,128)(2,1)S(1)} %get-tuple-element.55), channel_id=1, source_target_pairs={{0,4},{2,6},{4,0},{6,2},{1,5},{3,7},{5,1},{7,3},{8,12},{10,14},{12... | collective-permute-start | bytes 393224 | tf_op jit(solution)/shard_map/ppermute | solution.py:22
  36.8 6.8 %collective-permute-start.10 = (bf16[256,256]{1,0:T(8,128)(2,1)S(1)}, bf16[256,256]{1,0:T(8,128)(2,1)S(1)}, u32[]{:S(2)}, u32[]{:S(2)}) collective-permute-start(bf16[256,256]{1,0:T(8,128)(2,1)S(1)} %get-tuple-element.56), channel_id=1, source_target_pairs={{0,6},{2,4},{4,2},{6,0},{1,7},{3,5},{5,3},{7,1},{8,14},{10,12},{12... | collective-permute-start | bytes 393224 | tf_op jit(solution)/shard_map/ppermute | solution.py:22
  42.5 6.6 %collective-permute-start.15 = (f32[64,512]{1,0:T(8,128)S(1)}, f32[64,512]{1,0:T(8,128)S(1)}, u32[]{:S(2)}, u32[]{:S(2)}) collective-permute-start(f32[64,512]{1,0:T(8,128)S(1)} %copy-done.6), channel_id=1, source_target_pairs={{0,1},{1,0},{2,3},{3,2},{4,5},{5,4},{6,7},{7,6},{8,9},{9,8},{10,11... | collective-permute-start | bytes 393224 | tf_op jit(solution)/shard_map/ppermute | solution.py:22
  43.6 6.6 %collective-permute-start.16 = (f32[64,512]{1,0:T(8,128)S(1)}, f32[64,512]{1,0:T(8,128)S(1)}, u32[]{:S(2)}, u32[]{:S(2)}) collective-permute-start(f32[64,512]{1,0:T(8,128)S(1)} %copy-done.7), channel_id=1, source_target_pairs={{0,1},{1,0},{2,3},{3,2},{4,5},{5,4},{6,7},{7,6},{8,9},{9,8},{10,11... | collective-permute-start | bytes 393224 | tf_op jit(solution)/shard_map/ppermute | solution.py:22
  43.7 6.7 %collective-permute-start.17 = (f32[64,512]{1,0:T(8,128)S(1)}, f32[64,512]{1,0:T(8,128)S(1)}, u32[]{:S(2)}, u32[]{:S(2)}) collective-permute-start(f32[64,512]{1,0:T(8,128)S(1)} %copy-done.8), channel_id=1, source_target_pairs={{0,1},{1,0},{2,3},{3,2},{4,5},{5,4},{6,7},{7,6},{8,9},{9,8},{10,11... | collective-permute-start | bytes 393224 | tf_op jit(solution)/shard_map/ppermute | solution.py:22
  49.1 6.1 %collective-permute-start.13 = (bf16[64,256]{1,0:T(8,128)(2,1)S(1)}, bf16[64,256]{1,0:T(8,128)(2,1)S(1)}, u32[]{:S(2)}, u32[]{:S(2)}) collective-permute-start(bf16[64,256]{1,0:T(8,128)(2,1)S(1)} %get-tuple-element.60), channel_id=1, source_target_pairs={{0,24},{8,16},{16,8},{24,0},{1,25},{9,17},{17,9},{25,1},{2,26},{10... | collective-permute-start | bytes 98312 | tf_op jit(solution)/shard_map/ppermute | solution.py:22
  50.3 44.1 %collective-permute-start.25 = (bf16[2048,256]{1,0:T(8,128)(2,1)S(1)}, bf16[2048,256]{1,0:T(8,128)(2,1)S(1)}, u32[]{:S(2)}, u32[]{:S(2)}) collective-permute-start(bf16[2048,256]{1,0:T(8,128)(2,1)S(1)} %get-tuple-element.68.u_ref.uo_ref), channel_id=1, source_target_pairs={{0,1},{1,0},{2,3},{3,2},{4,5},{5,4},{6,7},{7,6},{8,9},{9,8},{10,11... | collective-permute-start | bytes 3145736 | tf_op jit(solution)/shard_map/ppermute | solution.py:22
  50.3 25.7 %collective-permute-start.30 = (bf16[256,512]{1,0:T(8,128)(2,1)S(1)}, bf16[256,512]{1,0:T(8,128)(2,1)S(1)}, u32[]{:S(2)}, u32[]{:S(2)}) collective-permute-start(bf16[256,512]{1,0:T(8,128)(2,1)S(1)} %slice.20), channel_id=1, source_target_pairs={{0,8},{8,0},{16,24},{24,16},{1,9},{9,1},{17,25},{25,17},{2,10},{10... | collective-permute-start | bytes 786440 | tf_op jit(solution)/shard_map/ppermute | solution.py:22
  55.8 6.6 %collective-permute-start.20 = (bf16[64,256]{1,0:T(8,128)(2,1)S(1)}, bf16[64,256]{1,0:T(8,128)(2,1)S(1)}, u32[]{:S(2)}, u32[]{:S(2)}) collective-permute-start(bf16[64,256]{1,0:T(8,128)(2,1)S(1)} %get-tuple-element.65), channel_id=1, source_target_pairs={{0,24},{8,16},{16,8},{24,0},{1,25},{9,17},{17,9},{25,1},{2,26},{10... | collective-permute-start | bytes 98312 | tf_op jit(solution)/shard_map/ppermute | solution.py:22
  57.0 5.4 %collective-permute-start.19 = (bf16[64,256]{1,0:T(8,128)(2,1)S(1)}, bf16[64,256]{1,0:T(8,128)(2,1)S(1)}, u32[]{:S(2)}, u32[]{:S(2)}) collective-permute-start(bf16[64,256]{1,0:T(8,128)(2,1)S(1)} %get-tuple-element.65), channel_id=1, source_target_pairs={{0,16},{8,24},{16,0},{24,8},{1,17},{9,25},{17,1},{25,9},{2,18},{10... | collective-permute-start | bytes 98312 | tf_op jit(solution)/shard_map/ppermute | solution.py:22
  62.4 6.4 %collective-permute-start.23 = (bf16[320,256]{1,0:T(8,128)(2,1)S(1)}, bf16[320,256]{1,0:T(8,128)(2,1)S(1)}, u32[]{:S(2)}, u32[]{:S(2)}) collective-permute-start(bf16[320,256]{1,0:T(8,128)(2,1)S(1)} %constant_dynamic-update-slice_fusion.3.refs_0_), channel_id=1, source_target_pairs={{0,6},{2,4},{4,2},{6,0},{1,7},{3,5},{5,3},{7,1},{8,14},{10,12},{12... | collective-permute-start | bytes 491528 | tf_op jit(solution)/shard_map/ppermute | solution.py:22
  65.0 13.6 %collective-permute-start.34 = (bf16[256,512]{1,0:T(8,128)(2,1)S(1)}, bf16[256,512]{1,0:T(8,128)(2,1)S(1)}, u32[]{:S(2)}, u32[]{:S(2)}) collective-permute-start(bf16[256,512]{1,0:T(8,128)(2,1)S(1)} %slice.23), channel_id=1, source_target_pairs={{0,8},{8,0},{16,24},{24,16},{1,9},{9,1},{17,25},{25,17},{2,10},{10... | collective-permute-start | bytes 786440 | tf_op jit(solution)/shard_map/ppermute | solution.py:22
  66.9 5.3 %collective-permute-start.22 = (bf16[320,256]{1,0:T(8,128)(2,1)S(1)}, bf16[320,256]{1,0:T(8,128)(2,1)S(1)}, u32[]{:S(2)}, u32[]{:S(2)}) collective-permute-start(bf16[320,256]{1,0:T(8,128)(2,1)S(1)} %constant_dynamic-update-slice_fusion.3.refs_0_), channel_id=1, source_target_pairs={{0,4},{2,6},{4,0},{6,2},{1,5},{3,7},{5,1},{7,3},{8,12},{10,14},{12... | collective-permute-start | bytes 491528 | tf_op jit(solution)/shard_map/ppermute | solution.py:22
  68.8 6.0 %collective-permute-start.21 = (bf16[320,256]{1,0:T(8,128)(2,1)S(1)}, bf16[320,256]{1,0:T(8,128)(2,1)S(1)}, u32[]{:S(2)}, u32[]{:S(2)}) collective-permute-start(bf16[320,256]{1,0:T(8,128)(2,1)S(1)} %constant_dynamic-update-slice_fusion.3.refs_0_), channel_id=1, source_target_pairs={{0,2},{2,0},{4,6},{6,4},{1,3},{3,1},{5,7},{7,5},{8,10},{10,8},{12,... | collective-permute-start | bytes 491528 | tf_op jit(solution)/shard_map/ppermute | solution.py:22
  72.2 6.5 %collective-permute-start.32 = (bf16[256,512]{1,0:T(8,128)(2,1)S(1)}, bf16[256,512]{1,0:T(8,128)(2,1)S(1)}, u32[]{:S(2)}, u32[]{:S(2)}) collective-permute-start(bf16[256,512]{1,0:T(8,128)(2,1)S(1)} %get-tuple-element.92), channel_id=1, source_target_pairs={{0,4},{2,6},{4,0},{6,2},{1,5},{3,7},{5,1},{7,3},{8,12},{10,14},{12... | collective-permute-start | bytes 786440 | tf_op jit(solution)/shard_map/ppermute | solution.py:22
  74.8 7.7 %collective-permute-start.28 = (bf16[256,512]{1,0:T(8,128)(2,1)S(1)}, bf16[256,512]{1,0:T(8,128)(2,1)S(1)}, u32[]{:S(2)}, u32[]{:S(2)}) collective-permute-start(bf16[256,512]{1,0:T(8,128)(2,1)S(1)} %get-tuple-element.93), channel_id=1, source_target_pairs={{0,2},{2,0},{4,6},{6,4},{1,3},{3,1},{5,7},{7,5},{8,10},{10,8},{12,... | collective-permute-start | bytes 786440 | tf_op jit(solution)/shard_map/ppermute | solution.py:22
  76.0 10.0 %collective-permute-start.29 = (bf16[256,512]{1,0:T(8,128)(2,1)S(1)}, bf16[256,512]{1,0:T(8,128)(2,1)S(1)}, u32[]{:S(2)}, u32[]{:S(2)}) collective-permute-start(bf16[256,512]{1,0:T(8,128)(2,1)S(1)} %get-tuple-element.91), channel_id=1, source_target_pairs={{0,2},{2,0},{4,6},{6,4},{1,3},{3,1},{5,7},{7,5},{8,10},{10,8},{12,... | collective-permute-start | bytes 786440 | tf_op jit(solution)/shard_map/ppermute | solution.py:22
  78.6 15.8 %collective-permute-start.24 = (bf16[336,512]{1,0:T(8,128)(2,1)S(1)}, bf16[336,512]{1,0:T(8,128)(2,1)S(1)}, u32[]{:S(2)}, u32[]{:S(2)}) collective-permute-start(bf16[336,512]{1,0:T(8,128)(2,1)S(1)} %get-tuple-element.70), channel_id=1, source_target_pairs={{0,1},{1,0},{2,3},{3,2},{4,5},{5,4},{6,7},{7,6},{8,9},{9,8},{10,11... | collective-permute-start | bytes 1032200 | tf_op jit(solution)/shard_map/ppermute | solution.py:22
  78.7 12.2 %collective-permute-start.33 = (bf16[256,512]{1,0:T(8,128)(2,1)S(1)}, bf16[256,512]{1,0:T(8,128)(2,1)S(1)}, u32[]{:S(2)}, u32[]{:S(2)}) collective-permute-start(bf16[256,512]{1,0:T(8,128)(2,1)S(1)} %get-tuple-element.90), channel_id=1, source_target_pairs={{0,4},{2,6},{4,0},{6,2},{1,5},{3,7},{5,1},{7,3},{8,12},{10,14},{12... | collective-permute-start | bytes 786440 | tf_op jit(solution)/shard_map/ppermute | solution.py:22
  82.5 8.4 %collective-permute-start.31 = (bf16[256,512]{1,0:T(8,128)(2,1)S(1)}, bf16[256,512]{1,0:T(8,128)(2,1)S(1)}, u32[]{:S(2)}, u32[]{:S(2)}) collective-permute-start(bf16[256,512]{1,0:T(8,128)(2,1)S(1)} %collective-permute-done.30.refs_4_), channel_id=1, source_target_pairs={{0,2},{2,0},{4,6},{6,4},{1,3},{3,1},{5,7},{7,5},{8,10},{10,8},{12,... | collective-permute-start | bytes 786440 | tf_op jit(solution)/shard_map/ppermute | solution.py:22
  86.1 8.3 %collective-permute-start.35 = (bf16[256,512]{1,0:T(8,128)(2,1)S(1)}, bf16[256,512]{1,0:T(8,128)(2,1)S(1)}, u32[]{:S(2)}, u32[]{:S(2)}) collective-permute-start(bf16[256,512]{1,0:T(8,128)(2,1)S(1)} %collective-permute-done.34.refs_10_), channel_id=1, source_target_pairs={{0,4},{2,6},{4,0},{6,2},{1,5},{3,7},{5,1},{7,3},{8,12},{10,14},{12... | collective-permute-start | bytes 786440 | tf_op jit(solution)/shard_map/ppermute | solution.py:22
  (17 other events, 146.1 us)

commit v3 on v2

--- a/solution.py
+++ b/solution.py
@@ -191,6 +191,10 @@
     return 0.8 * first + 0.2 * low, 0.95 * second + 0.05 * low * low
 
 
+def normalize(first, second):
+    return (first / jnp.sqrt(second)).astype(BF16)
+
+
 def norm_block(place, parts, local, remote):
     rows, columns = parts[0].shape
     width = local[0].shape[1]
@@ -209,7 +213,7 @@
             mine, remote = (jnp.where(core == 0, states[m + n][:, at], states[m + n + 2][:, at]) for m in (0, 4))
             old.append(jnp.where(here, mine, remote))
         first, second = advance(*old, low.astype(F32))
-        normed_ref[...] = (first / jnp.sqrt(second)).astype(BF16)
+        normed_ref[...] = normalize(first, second)
 
     operands = (*parts, *local, *remote)
     block = struct((rows, columns), BF16)
@@ -248,36 +252,42 @@
     )(u)
 
 
-def squares(place, blocks, products, fs_size, width):
-    total, columns = blocks[0].shape
-    rows = total // (fs_size + 1)
+def squares(place, blocks, products, local, remote, fs_size):
+    rank, columns = blocks[0].shape
+    rows, width = local[0].shape
+    total = rank + rows
     tail = 16
+    count = len(blocks)
 
     def body(place_ref, *refs):
-        pieces, (gram_ref, keep_ref, give_ref, scratch, low_scratch) = refs[:-5], refs[-5:]
+        pieces, states, (gram_ref, keep_ref, give_ref, scratch, low_scratch) = refs[:count], refs[count:-5], refs[-5:]
         fs, rep, core = place_ref[0], place_ref[1], place_ref[2]
         for j, ref in enumerate(pieces):
             start = (rep ^ j) * columns
             half = start // width
             at = pl.ds(pl.multiple_of(lax.rem(start, width), columns), columns)
-            for k in range(fs_size):
+            low_scratch[half, :, at] = ref[:rows, :]
+            for k in range(1, fs_size):
                 scratch[half, fs ^ k, :, at] = ref[k * rows : (k + 1) * rows, :]
-            low_scratch[half, :, at] = ref[-rows:, :]
+        for half, first in ((core, 0), (1 - core, 4)):
+            old = [jnp.where(core == 0, states[first + n][...], states[first + n + 2][...]) for n in (0, 1)]
+            new = advance(*old, low_scratch[half].astype(F32))
+            scratch[half, fs] = normalize(*new)
         square = 0.0
         for half in (0, 1):
             part = flat_rows(scratch[half])
             image = dot(gram_ref[0], part) + dot(gram_ref[1], part)
             square = square + jnp.sum(part.astype(F32) * image)
         for out, half in ((keep_ref, core), (give_ref, 1 - core)):
-            out[: fs_size * rows, :] = flat_rows(scratch[half])
-            out[fs_size * rows : total, :] = low_scratch[half]
+            out[:rank, :] = flat_rows(scratch[half])
+            out[rank:total, :] = low_scratch[half]
             rest = jnp.full((tail, 128), square, F32)
             for n in range(3):
                 piece = rest.astype(BF16)
                 out[total:, n * 128 : (n + 1) * 128] = piece
                 rest = rest - piece.astype(F32)
 
-    operands = (*blocks, products)
+    operands = (*blocks, *local, *remote, products)
     out = struct((total + tail, width), BF16)
     return pl.pallas_call(
         body,
@@ -508,7 +518,7 @@
     else:
         parts = [lax.psum_scatter(sums[0], "fs", scatter_dimension=0, tiled=True)]
     low, normed = norm_block(place, parts, state, remote_state)
-    column = jnp.concatenate([normed, *from_others(normed, "fs", fs_size), low], axis=0)
+    column = jnp.concatenate([low, *from_others(normed, "fs", fs_size)], axis=0)
     if fs_size == 4:
         rest += rest_of(far, sums[-1])
         last = [swap(after(far, sums[-1])[:half], "fs", fs_size, 1)]
@@ -516,7 +526,7 @@
         last_rest = [swap(after(last[0], column), "rep", rep_size, 1)]
         last_rest.append(swap(after(last[1], column), "rep", rep_size, rep_size // 2))
     blocks = [column] + from_others(column, "rep", rep_size)
-    kept, given = squares(place, blocks, products, fs_size, width)
+    kept, given = squares(place, blocks, products, state, remote_state, fs_size)
     got = swap(given, "tp", tp_size, 1)
 
     entries = float(rows * fs_size * width * tp_size)

time: 99.1 us -> 98.2 us (level)
  starting transfers between devices: 44.2 us -> 42.8 us
    ppermute x36, starting transfers between devices: 44.2 us -> 42.8 us  [swap(): return lax.ppermute(values, axis, [(i, i ^ step) for i in range(size)])]
    unnamed x32 -> x31, local copies, waits for them, and re-layouts: 4.72 us -> 4.71 us
where the time goes in v3:
time: 98.2 us; the launch traced here: 98 us
  starting transfers between devices  42.8 us (44%)
  waiting for transfers between devices  35.3 us (36%)
  Pallas kernels  13.1 us (13%)
  local copies, waits for them, and re-layouts  4.83 us (5%)
    ppermute x36, starting transfers between devices, swap(): return lax.ppermute(values, axis, [(i, i ^ step) for i in range(size)])  42.8 us
    ppermute x36, waiting for transfers between devices, swap(): return lax.ppermute(values, axis, [(i, i ^ step) for i in range(size)])  35.3 us
    unnamed x31, local copies, waits for them, and re-layouts  4.71 us
    pallas_call x1, Pallas kernels, finish(): pl.pallas_call(body, grid_spec=one_step(operands, 10, scratch, pltpu.HBM)...  4.43 us
  transfers between devices with their start and end apart: 36, of which 19 were waited for; matrix products, arithmetic and copies ran while one was open for 0% of the time, Pallas kernels for 9%

profile of v3, /device:TPU:0, one launch (start us, length us, event | category | flops | bytes accessed | tf_op | source)
XLA Modules:
  0.0 98.0 jit_solution(5313454583878972352)
XLA Ops:
  1.5 5.1 %collective-permute-start.2 = (bf16[128,256]{1,0:T(8,128)(2,1)S(1)}, bf16[128,256]{1,0:T(8,128)(2,1)S(1)}, u32[]{:S(2)}, u32[]{:S(2)}) collective-permute-start(bf16[128,256]{1,0:T(8,128)(2,1)S(1)} %dynamic-slice_select_fusion), channel_id=1, source_target_pairs={{0,24},{8,16},{16,8},{24,0},{1,25},{9,17},{17,9},{25,1},{2,26},{10... | collective-permute-start | bytes 196616 | tf_op jit(solution)/shard_map/ppermute | solution.py:22
  7.3 1.8 %collective-permute-done.2.refs_2_ = bf16[128,256]{1,0:T(8,128)(2,1)S(1)} collective-permute-done((bf16[128,256]{1,0:T(8,128)(2,1)S(1)}, bf16[128,256]{1,0:T(8,128)(2,1)S(1)}, u32[]{:S(2)}, u32[]{:S(2)}) %collective-permute-start.2) | collective-permute-done | bytes 65568 | tf_op jit(solution)/shard_map/ppermute | solution.py:22
  9.2 3.1 %collective-permute-done.1.refs_1_ = bf16[128,256]{1,0:T(8,128)(2,1)S(1)} collective-permute-done((bf16[128,256]{1,0:T(8,128)(2,1)S(1)}, bf16[128,256]{1,0:T(8,128)(2,1)S(1)}, u32[]{:S(2)}, u32[]{:S(2)}) %collective-permute-start.1) | collective-permute-done | bytes 65568 | tf_op jit(solution)/shard_map/ppermute | solution.py:22
  12.8 2.5 %collective-permute-start.5 = (bf16[384,256]{1,0:T(8,128)(2,1)S(1)}, bf16[384,256]{1,0:T(8,128)(2,1)S(1)}, u32[]{:S(2)}, u32[]{:S(2)}) collective-permute-start(bf16[384,256]{1,0:T(8,128)(2,1)S(1)} %constant_dynamic-update-slice_fusion), channel_id=1, source_target_pairs={{0,6},{2,4},{4,2},{6,0},{1,7},{3,5},{5,3},{7,1},{8,14},{10,12},{12... | collective-permute-start | bytes 589832 | tf_op jit(solution)/shard_map/ppermute | solution.py:22
  20.7 1.7 %collective-permute-start.27 = (bf16[512,512]{1,0:T(8,128)(2,1)S(1)}, bf16[512,512]{1,0:T(8,128)(2,1)S(1)}, u32[]{:S(2)}, u32[]{:S(2)}) collective-permute-start(bf16[512,512]{1,0:T(8,128)(2,1)S(1)} %held_rows.1), channel_id=1, source_target_pairs={{0,16},{8,24},{16,0},{24,8},{1,17},{9,25},{17,1},{25,9},{2,18},{10... | collective-permute-start | bytes 1572872 | tf_op jit(solution)/shard_map/ppermute | solution.py:22
  22.4 2.4 %collective-permute-done.4.refs_4_ = bf16[384,256]{1,0:T(8,128)(2,1)S(1)} collective-permute-done((bf16[384,256]{1,0:T(8,128)(2,1)S(1)}, bf16[384,256]{1,0:T(8,128)(2,1)S(1)}, u32[]{:S(2)}, u32[]{:S(2)}) %collective-permute-start.4) | collective-permute-done | bytes 196640 | tf_op jit(solution)/shard_map/ppermute | solution.py:22
  24.8 1.5 %collective-permute-start.3 = (bf16[384,256]{1,0:T(8,128)(2,1)S(1)}, bf16[384,256]{1,0:T(8,128)(2,1)S(1)}, u32[]{:S(2)}, u32[]{:S(2)}) collective-permute-start(bf16[384,256]{1,0:T(8,128)(2,1)S(1)} %constant_dynamic-update-slice_fusion), channel_id=1, source_target_pairs={{0,2},{2,0},{4,6},{6,4},{1,3},{3,1},{5,7},{7,5},{8,10},{10,8},{12,... | collective-permute-start | bytes 589832 | tf_op jit(solution)/shard_map/ppermute | solution.py:22
  26.3 2.2 %copy-done.4 = bf16[1024,2048]{1,0:T(8,128)(2,1)S(1)} copy-done((bf16[1024,2048]{1,0:T(8,128)(2,1)S(1)}, bf16[1024,2048]{1,0:T(8,128)(2,1)}, u32[]{:S(2)}) %copy-start.4) | copy-done | bytes 4194328
  28.8 2.8 %collective-permute-done.3.refs_3_ = bf16[384,256]{1,0:T(8,128)(2,1)S(1)} collective-permute-done((bf16[384,256]{1,0:T(8,128)(2,1)S(1)}, bf16[384,256]{1,0:T(8,128)(2,1)S(1)}, u32[]{:S(2)}, u32[]{:S(2)}) %collective-permute-start.3) | collective-permute-done | bytes 196640 | tf_op jit(solution)/shard_map/ppermute | solution.py:22
  31.7 1.9 %project.1 = (bf16[1024,256]{1,0:T(8,128)(2,1)S(1)}, bf16[2048,256]{1,0:T(8,128)(2,1)S(1)}) custom-call(s32[3]{0:T(128)S(1)} %pad_add_fusion.place_ref, bf16[1024,2048]{1,0:T(8,128)(2,1)S(1)} %stage.1.x_ref, bf16[512,256]{1,0:T(8,128)(2,1)S(1)} %copy-done.11, bf16[512,256]{1,0:T(8,128)(2,1)S(1)} %copy-done.12, ...), custom_call_target="tpu_custom_call" | custom-call | tf_op jit(solution)/shard_map/project/pallas_call | solution.py:116
  33.6 1.3 %token_sums.1 = (f32[256,256]{1,0:T(8,128)S(1)}, bf16[256,256]{1,0:T(8,128)(2,1)S(1)}, bf16[256,256]{1,0:T(8,128)(2,1)S(1)}, bf16[256,256]{1,0:T(8,128)(2,1)S(1)}) custom-call(s32[3]{0:T(128)S(1)} %pad_add_fusion.place_ref, bf16[1024,256]{1,0:T(8,128)(2,1)S(1)} %get-tuple-element.50.y_ref, bf16[1024,512]{1,0:T(8,128)(2,1)S(1)} %copy-done.9, ...), custom_call_target="tpu_custom_call" | custom-call | tf_op jit(solution)/shard_map/token_sums/pallas_call | solution.py:147
  35.0 1.6 %collective-permute-start.8 = (bf16[256,256]{1,0:T(8,128)(2,1)S(1)}, bf16[256,256]{1,0:T(8,128)(2,1)S(1)}, u32[]{:S(2)}, u32[]{:S(2)}) collective-permute-start(bf16[256,256]{1,0:T(8,128)(2,1)S(1)} %get-tuple-element.54), channel_id=1, source_target_pairs={{0,2},{2,0},{4,6},{6,4},{1,3},{3,1},{5,7},{7,5},{8,10},{10,8},{12,... | collective-permute-start | bytes 393224 | tf_op jit(solution)/shard_map/ppermute | solution.py:22
  36.8 1.7 %collective-permute-start.10 = (bf16[256,256]{1,0:T(8,128)(2,1)S(1)}, bf16[256,256]{1,0:T(8,128)(2,1)S(1)}, u32[]{:S(2)}, u32[]{:S(2)}) collective-permute-start(bf16[256,256]{1,0:T(8,128)(2,1)S(1)} %get-tuple-element.56), channel_id=1, source_target_pairs={{0,6},{2,4},{4,2},{6,0},{1,7},{3,5},{5,3},{7,1},{8,14},{10,12},{12... | collective-permute-start | bytes 393224 | tf_op jit(solution)/shard_map/ppermute | solution.py:22
  38.5 4.0 %collective-permute-done.26.refs_0_.refs_6_ = bf16[512,512]{1,0:T(8,128)(2,1)S(1)} collective-permute-done((bf16[512,512]{1,0:T(8,128)(2,1)S(1)}, bf16[512,512]{1,0:T(8,128)(2,1)S(1)}, u32[]{:S(2)}, u32[]{:S(2)}) %collective-permute-start.26) | collective-permute-done | bytes 524320 | tf_op jit(solution)/shard_map/ppermute | solution.py:22
  46.0 3.2 %collective-permute-start.12 = (bf16[64,256]{1,0:T(8,128)(2,1)S(1)}, bf16[64,256]{1,0:T(8,128)(2,1)S(1)}, u32[]{:S(2)}, u32[]{:S(2)}) collective-permute-start(bf16[64,256]{1,0:T(8,128)(2,1)S(1)} %get-tuple-element.59), channel_id=1, source_target_pairs={{0,16},{8,24},{16,0},{24,8},{1,17},{9,25},{17,1},{25,9},{2,18},{10... | collective-permute-start | bytes 98312 | tf_op jit(solution)/shard_map/ppermute | solution.py:22
  51.0 4.2 %collective-permute-done.13.refs_3_ = bf16[64,256]{1,0:T(8,128)(2,1)S(1)} collective-permute-done((bf16[64,256]{1,0:T(8,128)(2,1)S(1)}, bf16[64,256]{1,0:T(8,128)(2,1)S(1)}, u32[]{:S(2)}, u32[]{:S(2)}) %collective-permute-start.13) | collective-permute-done | bytes 32800 | tf_op jit(solution)/shard_map/ppermute | solution.py:22
  57.0 3.3 %collective-permute-start.18 = (bf16[64,256]{1,0:T(8,128)(2,1)S(1)}, bf16[64,256]{1,0:T(8,128)(2,1)S(1)}, u32[]{:S(2)}, u32[]{:S(2)}) collective-permute-start(bf16[64,256]{1,0:T(8,128)(2,1)S(1)} %get-tuple-element.66), channel_id=1, source_target_pairs={{0,8},{8,0},{16,24},{24,16},{1,9},{9,1},{17,25},{25,17},{2,10},{10... | collective-permute-start | bytes 98312 | tf_op jit(solution)/shard_map/ppermute | solution.py:22
  60.3 2.0 %collective-permute-done.18 = bf16[64,256]{1,0:T(8,128)(2,1)S(1)} collective-permute-done((bf16[64,256]{1,0:T(8,128)(2,1)S(1)}, bf16[64,256]{1,0:T(8,128)(2,1)S(1)}, u32[]{:S(2)}, u32[]{:S(2)}) %collective-permute-start.18) | collective-permute-done | bytes 32800 | tf_op jit(solution)/shard_map/ppermute | solution.py:22
  62.4 2.5 %collective-permute-start.23 = (bf16[256,256]{1,0:T(8,128)(2,1)S(1)}, bf16[256,256]{1,0:T(8,128)(2,1)S(1)}, u32[]{:S(2)}, u32[]{:S(2)}) collective-permute-start(bf16[256,256]{1,0:T(8,128)(2,1)S(1)} %constant_dynamic-update-slice_fusion.3.refs_0_), channel_id=1, source_target_pairs={{0,6},{2,4},{4,2},{6,0},{1,7},{3,5},{5,3},{7,1},{8,14},{10,12},{12... | collective-permute-start | bytes 393224 | tf_op jit(solution)/shard_map/ppermute | solution.py:22
  65.0 1.9 %collective-permute-start.34 = (bf16[256,512]{1,0:T(8,128)(2,1)S(1)}, bf16[256,512]{1,0:T(8,128)(2,1)S(1)}, u32[]{:S(2)}, u32[]{:S(2)}) collective-permute-start(bf16[256,512]{1,0:T(8,128)(2,1)S(1)} %slice.23), channel_id=1, source_target_pairs={{0,8},{8,0},{16,24},{24,16},{1,9},{9,1},{17,25},{25,17},{2,10},{10... | collective-permute-start | bytes 786440 | tf_op jit(solution)/shard_map/ppermute | solution.py:22
  68.4 1.4 %collective-permute-start.21 = (bf16[256,256]{1,0:T(8,128)(2,1)S(1)}, bf16[256,256]{1,0:T(8,128)(2,1)S(1)}, u32[]{:S(2)}, u32[]{:S(2)}) collective-permute-start(bf16[256,256]{1,0:T(8,128)(2,1)S(1)} %constant_dynamic-update-slice_fusion.3.refs_0_), channel_id=1, source_target_pairs={{0,2},{2,0},{4,6},{6,4},{1,3},{3,1},{5,7},{7,5},{8,10},{10,8},{12,... | collective-permute-start | bytes 393224 | tf_op jit(solution)/shard_map/ppermute | solution.py:22
  69.9 2.1 %collective-permute-done.22.refs_2_ = bf16[256,256]{1,0:T(8,128)(2,1)S(1)} collective-permute-done((bf16[256,256]{1,0:T(8,128)(2,1)S(1)}, bf16[256,256]{1,0:T(8,128)(2,1)S(1)}, u32[]{:S(2)}, u32[]{:S(2)}) %collective-permute-start.22) | collective-permute-done | bytes 131104 | tf_op jit(solution)/shard_map/ppermute | solution.py:22
  72.7 1.6 %collective-permute-done.21.refs_1_ = bf16[256,256]{1,0:T(8,128)(2,1)S(1)} collective-permute-done((bf16[256,256]{1,0:T(8,128)(2,1)S(1)}, bf16[256,256]{1,0:T(8,128)(2,1)S(1)}, u32[]{:S(2)}, u32[]{:S(2)}) %collective-permute-start.21) | collective-permute-done | bytes 131104 | tf_op jit(solution)/shard_map/ppermute | solution.py:22
  74.3 1.3 %collective-permute-start.28 = (bf16[256,512]{1,0:T(8,128)(2,1)S(1)}, bf16[256,512]{1,0:T(8,128)(2,1)S(1)}, u32[]{:S(2)}, u32[]{:S(2)}) collective-permute-start(bf16[256,512]{1,0:T(8,128)(2,1)S(1)} %get-tuple-element.93), channel_id=1, source_target_pairs={{0,2},{2,0},{4,6},{6,4},{1,3},{3,1},{5,7},{7,5},{8,10},{10,8},{12,... | collective-permute-start | bytes 786440 | tf_op jit(solution)/shard_map/ppermute | solution.py:22
  76.8 1.5 %squares.1 = (bf16[336,512]{1,0:T(8,128)(2,1)S(1)}, bf16[336,512]{1,0:T(8,128)(2,1)S(1)}) custom-call(s32[3]{0:T(128)S(1)} %pad_add_fusion.place_ref, bf16[256,256]{1,0:T(8,128)(2,1)S(1)} %constant_dynamic-update-slice_fusion.3.refs_0_, bf16[256,256]{1,0:T(8,128)(2,1)S(1)} %collective-permute-done.21.refs_1_, ...), custom_call_target="tpu_custom_call" | custom-call | tf_op jit(solution)/shard_map/squares/pallas_call | solution.py:292
  78.4 2.6 %collective-permute-start.33 = (bf16[256,512]{1,0:T(8,128)(2,1)S(1)}, bf16[256,512]{1,0:T(8,128)(2,1)S(1)}, u32[]{:S(2)}, u32[]{:S(2)}) collective-permute-start(bf16[256,512]{1,0:T(8,128)(2,1)S(1)} %get-tuple-element.90), channel_id=1, source_target_pairs={{0,4},{2,6},{4,0},{6,2},{1,5},{3,7},{5,1},{7,3},{8,12},{10,14},{12... | collective-permute-start | bytes 786440 | tf_op jit(solution)/shard_map/ppermute | solution.py:22
  81.8 1.4 %collective-permute-start.31 = (bf16[256,512]{1,0:T(8,128)(2,1)S(1)}, bf16[256,512]{1,0:T(8,128)(2,1)S(1)}, u32[]{:S(2)}, u32[]{:S(2)}) collective-permute-start(bf16[256,512]{1,0:T(8,128)(2,1)S(1)} %collective-permute-done.30.refs_4_), channel_id=1, source_target_pairs={{0,2},{2,0},{4,6},{6,4},{1,3},{3,1},{5,7},{7,5},{8,10},{10,8},{12,... | collective-permute-start | bytes 786440 | tf_op jit(solution)/shard_map/ppermute | solution.py:22
  83.2 2.3 %collective-permute-done.29.refs_3_ = bf16[256,512]{1,0:T(8,128)(2,1)S(1)} collective-permute-done((bf16[256,512]{1,0:T(8,128)(2,1)S(1)}, bf16[256,512]{1,0:T(8,128)(2,1)S(1)}, u32[]{:S(2)}, u32[]{:S(2)}) %collective-permute-start.29) | collective-permute-done | bytes 262176 | tf_op jit(solution)/shard_map/ppermute | solution.py:22
  85.5 2.5 %collective-permute-start.35 = (bf16[256,512]{1,0:T(8,128)(2,1)S(1)}, bf16[256,512]{1,0:T(8,128)(2,1)S(1)}, u32[]{:S(2)}, u32[]{:S(2)}) collective-permute-start(bf16[256,512]{1,0:T(8,128)(2,1)S(1)} %collective-permute-done.34.refs_10_), channel_id=1, source_target_pairs={{0,4},{2,6},{4,0},{6,2},{1,5},{3,7},{5,1},{7,3},{8,12},{10,14},{12... | collective-permute-start | bytes 786440 | tf_op jit(solution)/shard_map/ppermute | solution.py:22
  88.1 1.3 %prepare.1 = (f32[2,512,512]{2,1,0:T(8,128)S(1)}, f32[2,64,512]{2,1,0:T(8,128)S(1)}, bf16[3,512,512]{2,1,0:T(8,128)(2,1)S(1)}) custom-call(s32[3]{0:T(128)S(1)} %pad_add_fusion.place_ref, bf16[336,512]{1,0:T(8,128)(2,1)S(1)} %get-tuple-element.69.n_ref.no_ref, bf16[2048,256]{1,0:T(8,128)(2,1)S(1)} %get-tuple-element.68.u_ref.uo_ref, ...), custom_call_target="tpu_custom_call" | custom-call | tf_op jit(solution)/shard_map/prepare/pallas_call | solution.py:368
  90.3 3.3 %collective-permute-done.35.refs_11_ = bf16[256,512]{1,0:T(8,128)(2,1)S(1)} collective-permute-done((bf16[256,512]{1,0:T(8,128)(2,1)S(1)}, bf16[256,512]{1,0:T(8,128)(2,1)S(1)}, u32[]{:S(2)}, u32[]{:S(2)}) %collective-permute-start.35) | collective-permute-done | bytes 262176 | tf_op jit(solution)/shard_map/ppermute | solution.py:22
  93.5 4.4 %finish.1 = (f32[512,512]{1,0:T(8,128)}, f32[512,512]{1,0:T(8,128)}, f32[512,512]{1,0:T(8,128)}, f32[512,512]{1,0:T(8,128)}, f32[64,512]{1,0:T(8,128)}, /*index=...) custom-call(s32[3]{0:T(128)S(1)} %pad_add_fusion.place_ref, ...), custom_call_target="tpu_custom_call" | custom-call | tf_op jit(solution)/shard_map/finish/pallas_call | solution.py:442
  (89 shorter events, 20.7 us)
Async XLA Ops:
  1.5 7.6 %collective-permute-start.2 = (bf16[128,256]{1,0:T(8,128)(2,1)S(1)}, bf16[128,256]{1,0:T(8,128)(2,1)S(1)}, u32[]{:S(2)}, u32[]{:S(2)}) collective-permute-start(bf16[128,256]{1,0:T(8,128)(2,1)S(1)} %dynamic-slice_select_fusion), channel_id=1, source_target_pairs={{0,24},{8,16},{16,8},{24,0},{1,25},{9,17},{17,9},{25,1},{2,26},{10... | collective-permute-start | bytes 196616 | tf_op jit(solution)/shard_map/ppermute | solution.py:22
  6.7 5.6 %collective-permute-start.1 = (bf16[128,256]{1,0:T(8,128)(2,1)S(1)}, bf16[128,256]{1,0:T(8,128)(2,1)S(1)}, u32[]{:S(2)}, u32[]{:S(2)}) collective-permute-start(bf16[128,256]{1,0:T(8,128)(2,1)S(1)} %dynamic-slice_select_fusion), channel_id=1, source_target_pairs={{0,16},{8,24},{16,0},{24,8},{1,17},{9,25},{17,1},{25,9},{2,18},{10... | collective-permute-start | bytes 196616 | tf_op jit(solution)/shard_map/ppermute | solution.py:22
  6.7 5.6 %collective-permute-start = (bf16[128,256]{1,0:T(8,128)(2,1)S(1)}, bf16[128,256]{1,0:T(8,128)(2,1)S(1)}, u32[]{:S(2)}, u32[]{:S(2)}) collective-permute-start(bf16[128,256]{1,0:T(8,128)(2,1)S(1)} %dynamic-slice_select_fusion), channel_id=1, source_target_pairs={{0,8},{8,0},{16,24},{24,16},{1,9},{9,1},{17,25},{25,17},{2,10},{10... | collective-permute-start | bytes 196616 | tf_op jit(solution)/shard_map/ppermute | solution.py:22
  12.3 21.2 %collective-permute-start.6 = (bf16[1024,512]{1,0:T(8,128)(2,1)}, bf16[1024,512]{1,0:T(8,128)(2,1)S(1)}, u32[]{:S(2)}, u32[]{:S(2)}) collective-permute-start(bf16[1024,512]{1,0:T(8,128)(2,1)} %ci.1), channel_id=1, source_target_pairs={{0,1},{1,0},{2,3},{3,2},{4,5},{5,4},{6,7},{7,6},{8,9},{9,8},{10,11... | collective-permute-start | bytes 3145736 | tf_op jit(solution)/shard_map/ppermute | solution.py:22
  12.3 21.2 %collective-permute-start.7 = (bf16[1024,512]{1,0:T(8,128)(2,1)}, bf16[1024,512]{1,0:T(8,128)(2,1)S(1)}, u32[]{:S(2)}, u32[]{:S(2)}) collective-permute-start(bf16[1024,512]{1,0:T(8,128)(2,1)} %cg.1), channel_id=1, source_target_pairs={{0,1},{1,0},{2,3},{3,2},{4,5},{5,4},{6,7},{7,6},{8,9},{9,8},{10,11... | collective-permute-start | bytes 3145736 | tf_op jit(solution)/shard_map/ppermute | solution.py:22
  12.8 7.9 %collective-permute-start.5 = (bf16[384,256]{1,0:T(8,128)(2,1)S(1)}, bf16[384,256]{1,0:T(8,128)(2,1)S(1)}, u32[]{:S(2)}, u32[]{:S(2)}) collective-permute-start(bf16[384,256]{1,0:T(8,128)(2,1)S(1)} %constant_dynamic-update-slice_fusion), channel_id=1, source_target_pairs={{0,6},{2,4},{4,2},{6,0},{1,7},{3,5},{5,3},{7,1},{8,14},{10,12},{12... | collective-permute-start | bytes 589832 | tf_op jit(solution)/shard_map/ppermute | solution.py:22
  15.3 9.5 %collective-permute-start.4 = (bf16[384,256]{1,0:T(8,128)(2,1)S(1)}, bf16[384,256]{1,0:T(8,128)(2,1)S(1)}, u32[]{:S(2)}, u32[]{:S(2)}) collective-permute-start(bf16[384,256]{1,0:T(8,128)(2,1)S(1)} %constant_dynamic-update-slice_fusion), channel_id=1, source_target_pairs={{0,4},{2,6},{4,0},{6,2},{1,5},{3,7},{5,1},{7,3},{8,12},{10,14},{12... | collective-permute-start | bytes 589832 | tf_op jit(solution)/shard_map/ppermute | solution.py:22
  19.0 23.5 %collective-permute-start.26 = (bf16[512,512]{1,0:T(8,128)(2,1)S(1)}, bf16[512,512]{1,0:T(8,128)(2,1)S(1)}, u32[]{:S(2)}, u32[]{:S(2)}) collective-permute-start(bf16[512,512]{1,0:T(8,128)(2,1)S(1)} %held_rows.1), channel_id=1, source_target_pairs={{0,8},{8,0},{16,24},{24,16},{1,9},{9,1},{17,25},{25,17},{2,10},{10... | collective-permute-start | bytes 1572872 | tf_op jit(solution)/shard_map/ppermute | solution.py:22
  20.7 25.1 %collective-permute-start.27 = (bf16[512,512]{1,0:T(8,128)(2,1)S(1)}, bf16[512,512]{1,0:T(8,128)(2,1)S(1)}, u32[]{:S(2)}, u32[]{:S(2)}) collective-permute-start(bf16[512,512]{1,0:T(8,128)(2,1)S(1)} %held_rows.1), channel_id=1, source_target_pairs={{0,16},{8,24},{16,0},{24,8},{1,17},{9,25},{17,1},{25,9},{2,18},{10... | collective-permute-start | bytes 1572872 | tf_op jit(solution)/shard_map/ppermute | solution.py:22
  24.8 6.8 %collective-permute-start.3 = (bf16[384,256]{1,0:T(8,128)(2,1)S(1)}, bf16[384,256]{1,0:T(8,128)(2,1)S(1)}, u32[]{:S(2)}, u32[]{:S(2)}) collective-permute-start(bf16[384,256]{1,0:T(8,128)(2,1)S(1)} %constant_dynamic-update-slice_fusion), channel_id=1, source_target_pairs={{0,2},{2,0},{4,6},{6,4},{1,3},{3,1},{5,7},{7,5},{8,10},{10,8},{12,... | collective-permute-start | bytes 589832 | tf_op jit(solution)/shard_map/ppermute | solution.py:22
  35.0 7.6 %collective-permute-start.8 = (bf16[256,256]{1,0:T(8,128)(2,1)S(1)}, bf16[256,256]{1,0:T(8,128)(2,1)S(1)}, u32[]{:S(2)}, u32[]{:S(2)}) collective-permute-start(bf16[256,256]{1,0:T(8,128)(2,1)S(1)} %get-tuple-element.54), channel_id=1, source_target_pairs={{0,2},{2,0},{4,6},{6,4},{1,3},{3,1},{5,7},{7,5},{8,10},{10,8},{12,... | collective-permute-start | bytes 393224 | tf_op jit(solution)/shard_map/ppermute | solution.py:22
  36.5 7.1 %collective-permute-start.9 = (bf16[256,256]{1,0:T(8,128)(2,1)S(1)}, bf16[256,256]{1,0:T(8,128)(2,1)S(1)}, u32[]{:S(2)}, u32[]{:S(2)}) collective-permute-start(bf16[256,256]{1,0:T(8,128)(2,1)S(1)} %get-tuple-element.55), channel_id=1, source_target_pairs={{0,4},{2,6},{4,0},{6,2},{1,5},{3,7},{5,1},{7,3},{8,12},{10,14},{12... | collective-permute-start | bytes 393224 | tf_op jit(solution)/shard_map/ppermute | solution.py:22
  36.8 6.8 %collective-permute-start.10 = (bf16[256,256]{1,0:T(8,128)(2,1)S(1)}, bf16[256,256]{1,0:T(8,128)(2,1)S(1)}, u32[]{:S(2)}, u32[]{:S(2)}) collective-permute-start(bf16[256,256]{1,0:T(8,128)(2,1)S(1)} %get-tuple-element.56), channel_id=1, source_target_pairs={{0,6},{2,4},{4,2},{6,0},{1,7},{3,5},{5,3},{7,1},{8,14},{10,12},{12... | collective-permute-start | bytes 393224 | tf_op jit(solution)/shard_map/ppermute | solution.py:22
  42.5 6.6 %collective-permute-start.15 = (f32[64,512]{1,0:T(8,128)S(1)}, f32[64,512]{1,0:T(8,128)S(1)}, u32[]{:S(2)}, u32[]{:S(2)}) collective-permute-start(f32[64,512]{1,0:T(8,128)S(1)} %copy-done.6), channel_id=1, source_target_pairs={{0,1},{1,0},{2,3},{3,2},{4,5},{5,4},{6,7},{7,6},{8,9},{9,8},{10,11... | collective-permute-start | bytes 393224 | tf_op jit(solution)/shard_map/ppermute | solution.py:22
  43.6 6.6 %collective-permute-start.16 = (f32[64,512]{1,0:T(8,128)S(1)}, f32[64,512]{1,0:T(8,128)S(1)}, u32[]{:S(2)}, u32[]{:S(2)}) collective-permute-start(f32[64,512]{1,0:T(8,128)S(1)} %copy-done.7), channel_id=1, source_target_pairs={{0,1},{1,0},{2,3},{3,2},{4,5},{5,4},{6,7},{7,6},{8,9},{9,8},{10,11... | collective-permute-start | bytes 393224 | tf_op jit(solution)/shard_map/ppermute | solution.py:22
  43.7 6.7 %collective-permute-start.17 = (f32[64,512]{1,0:T(8,128)S(1)}, f32[64,512]{1,0:T(8,128)S(1)}, u32[]{:S(2)}, u32[]{:S(2)}) collective-permute-start(f32[64,512]{1,0:T(8,128)S(1)} %copy-done.8), channel_id=1, source_target_pairs={{0,1},{1,0},{2,3},{3,2},{4,5},{5,4},{6,7},{7,6},{8,9},{9,8},{10,11... | collective-permute-start | bytes 393224 | tf_op jit(solution)/shard_map/ppermute | solution.py:22
  49.1 6.1 %collective-permute-start.13 = (bf16[64,256]{1,0:T(8,128)(2,1)S(1)}, bf16[64,256]{1,0:T(8,128)(2,1)S(1)}, u32[]{:S(2)}, u32[]{:S(2)}) collective-permute-start(bf16[64,256]{1,0:T(8,128)(2,1)S(1)} %get-tuple-element.60), channel_id=1, source_target_pairs={{0,24},{8,16},{16,8},{24,0},{1,25},{9,17},{17,9},{25,1},{2,26},{10... | collective-permute-start | bytes 98312 | tf_op jit(solution)/shard_map/ppermute | solution.py:22
  50.3 43.3 %collective-permute-start.25 = (bf16[2048,256]{1,0:T(8,128)(2,1)S(1)}, bf16[2048,256]{1,0:T(8,128)(2,1)S(1)}, u32[]{:S(2)}, u32[]{:S(2)}) collective-permute-start(bf16[2048,256]{1,0:T(8,128)(2,1)S(1)} %get-tuple-element.68.u_ref.uo_ref), channel_id=1, source_target_pairs={{0,1},{1,0},{2,3},{3,2},{4,5},{5,4},{6,7},{7,6},{8,9},{9,8},{10,11... | collective-permute-start | bytes 3145736 | tf_op jit(solution)/shard_map/ppermute | solution.py:22
  50.3 25.2 %collective-permute-start.30 = (bf16[256,512]{1,0:T(8,128)(2,1)S(1)}, bf16[256,512]{1,0:T(8,128)(2,1)S(1)}, u32[]{:S(2)}, u32[]{:S(2)}) collective-permute-start(bf16[256,512]{1,0:T(8,128)(2,1)S(1)} %slice.20), channel_id=1, source_target_pairs={{0,8},{8,0},{16,24},{24,16},{1,9},{9,1},{17,25},{25,17},{2,10},{10... | collective-permute-start | bytes 786440 | tf_op jit(solution)/shard_map/ppermute | solution.py:22
  55.8 6.6 %collective-permute-start.20 = (bf16[64,256]{1,0:T(8,128)(2,1)S(1)}, bf16[64,256]{1,0:T(8,128)(2,1)S(1)}, u32[]{:S(2)}, u32[]{:S(2)}) collective-permute-start(bf16[64,256]{1,0:T(8,128)(2,1)S(1)} %get-tuple-element.66), channel_id=1, source_target_pairs={{0,24},{8,16},{16,8},{24,0},{1,25},{9,17},{17,9},{25,1},{2,26},{10... | collective-permute-start | bytes 98312 | tf_op jit(solution)/shard_map/ppermute | solution.py:22
  57.0 5.4 %collective-permute-start.19 = (bf16[64,256]{1,0:T(8,128)(2,1)S(1)}, bf16[64,256]{1,0:T(8,128)(2,1)S(1)}, u32[]{:S(2)}, u32[]{:S(2)}) collective-permute-start(bf16[64,256]{1,0:T(8,128)(2,1)S(1)} %get-tuple-element.66), channel_id=1, source_target_pairs={{0,16},{8,24},{16,0},{24,8},{1,17},{9,25},{17,1},{25,9},{2,18},{10... | collective-permute-start | bytes 98312 | tf_op jit(solution)/shard_map/ppermute | solution.py:22
  57.0 5.3 %collective-permute-start.18 = (bf16[64,256]{1,0:T(8,128)(2,1)S(1)}, bf16[64,256]{1,0:T(8,128)(2,1)S(1)}, u32[]{:S(2)}, u32[]{:S(2)}) collective-permute-start(bf16[64,256]{1,0:T(8,128)(2,1)S(1)} %get-tuple-element.66), channel_id=1, source_target_pairs={{0,8},{8,0},{16,24},{24,16},{1,9},{9,1},{17,25},{25,17},{2,10},{10... | collective-permute-start | bytes 98312 | tf_op jit(solution)/shard_map/ppermute | solution.py:22
  62.4 6.0 %collective-permute-start.23 = (bf16[256,256]{1,0:T(8,128)(2,1)S(1)}, bf16[256,256]{1,0:T(8,128)(2,1)S(1)}, u32[]{:S(2)}, u32[]{:S(2)}) collective-permute-start(bf16[256,256]{1,0:T(8,128)(2,1)S(1)} %constant_dynamic-update-slice_fusion.3.refs_0_), channel_id=1, source_target_pairs={{0,6},{2,4},{4,2},{6,0},{1,7},{3,5},{5,3},{7,1},{8,14},{10,12},{12... | collective-permute-start | bytes 393224 | tf_op jit(solution)/shard_map/ppermute | solution.py:22
  65.0 13.4 %collective-permute-start.34 = (bf16[256,512]{1,0:T(8,128)(2,1)S(1)}, bf16[256,512]{1,0:T(8,128)(2,1)S(1)}, u32[]{:S(2)}, u32[]{:S(2)}) collective-permute-start(bf16[256,512]{1,0:T(8,128)(2,1)S(1)} %slice.23), channel_id=1, source_target_pairs={{0,8},{8,0},{16,24},{24,16},{1,9},{9,1},{17,25},{25,17},{2,10},{10... | collective-permute-start | bytes 786440 | tf_op jit(solution)/shard_map/ppermute | solution.py:22
  68.4 5.9 %collective-permute-start.21 = (bf16[256,256]{1,0:T(8,128)(2,1)S(1)}, bf16[256,256]{1,0:T(8,128)(2,1)S(1)}, u32[]{:S(2)}, u32[]{:S(2)}) collective-permute-start(bf16[256,256]{1,0:T(8,128)(2,1)S(1)} %constant_dynamic-update-slice_fusion.3.refs_0_), channel_id=1, source_target_pairs={{0,2},{2,0},{4,6},{6,4},{1,3},{3,1},{5,7},{7,5},{8,10},{10,8},{12,... | collective-permute-start | bytes 393224 | tf_op jit(solution)/shard_map/ppermute | solution.py:22
  72.0 6.5 %collective-permute-start.32 = (bf16[256,512]{1,0:T(8,128)(2,1)S(1)}, bf16[256,512]{1,0:T(8,128)(2,1)S(1)}, u32[]{:S(2)}, u32[]{:S(2)}) collective-permute-start(bf16[256,512]{1,0:T(8,128)(2,1)S(1)} %get-tuple-element.92), channel_id=1, source_target_pairs={{0,4},{2,6},{4,0},{6,2},{1,5},{3,7},{5,1},{7,3},{8,12},{10,14},{12... | collective-permute-start | bytes 786440 | tf_op jit(solution)/shard_map/ppermute | solution.py:22
  74.3 7.5 %collective-permute-start.28 = (bf16[256,512]{1,0:T(8,128)(2,1)S(1)}, bf16[256,512]{1,0:T(8,128)(2,1)S(1)}, u32[]{:S(2)}, u32[]{:S(2)}) collective-permute-start(bf16[256,512]{1,0:T(8,128)(2,1)S(1)} %get-tuple-element.93), channel_id=1, source_target_pairs={{0,2},{2,0},{4,6},{6,4},{1,3},{3,1},{5,7},{7,5},{8,10},{10,8},{12,... | collective-permute-start | bytes 786440 | tf_op jit(solution)/shard_map/ppermute | solution.py:22
  75.6 9.9 %collective-permute-start.29 = (bf16[256,512]{1,0:T(8,128)(2,1)S(1)}, bf16[256,512]{1,0:T(8,128)(2,1)S(1)}, u32[]{:S(2)}, u32[]{:S(2)}) collective-permute-start(bf16[256,512]{1,0:T(8,128)(2,1)S(1)} %get-tuple-element.91), channel_id=1, source_target_pairs={{0,2},{2,0},{4,6},{6,4},{1,3},{3,1},{5,7},{7,5},{8,10},{10,8},{12,... | collective-permute-start | bytes 786440 | tf_op jit(solution)/shard_map/ppermute | solution.py:22
  78.4 11.9 %collective-permute-start.24 = (bf16[336,512]{1,0:T(8,128)(2,1)S(1)}, bf16[336,512]{1,0:T(8,128)(2,1)S(1)}, u32[]{:S(2)}, u32[]{:S(2)}) collective-permute-start(bf16[336,512]{1,0:T(8,128)(2,1)S(1)} %get-tuple-element.70), channel_id=1, source_target_pairs={{0,1},{1,0},{2,3},{3,2},{4,5},{5,4},{6,7},{7,6},{8,9},{9,8},{10,11... | collective-permute-start | bytes 1032200 | tf_op jit(solution)/shard_map/ppermute | solution.py:22
  78.4 10.9 %collective-permute-start.33 = (bf16[256,512]{1,0:T(8,128)(2,1)S(1)}, bf16[256,512]{1,0:T(8,128)(2,1)S(1)}, u32[]{:S(2)}, u32[]{:S(2)}) collective-permute-start(bf16[256,512]{1,0:T(8,128)(2,1)S(1)} %get-tuple-element.90), channel_id=1, source_target_pairs={{0,4},{2,6},{4,0},{6,2},{1,5},{3,7},{5,1},{7,3},{8,12},{10,14},{12... | collective-permute-start | bytes 786440 | tf_op jit(solution)/shard_map/ppermute | solution.py:22
  81.8 8.4 %collective-permute-start.31 = (bf16[256,512]{1,0:T(8,128)(2,1)S(1)}, bf16[256,512]{1,0:T(8,128)(2,1)S(1)}, u32[]{:S(2)}, u32[]{:S(2)}) collective-permute-start(bf16[256,512]{1,0:T(8,128)(2,1)S(1)} %collective-permute-done.30.refs_4_), channel_id=1, source_target_pairs={{0,2},{2,0},{4,6},{6,4},{1,3},{3,1},{5,7},{7,5},{8,10},{10,8},{12,... | collective-permute-start | bytes 786440 | tf_op jit(solution)/shard_map/ppermute | solution.py:22
  85.5 8.0 %collective-permute-start.35 = (bf16[256,512]{1,0:T(8,128)(2,1)S(1)}, bf16[256,512]{1,0:T(8,128)(2,1)S(1)}, u32[]{:S(2)}, u32[]{:S(2)}) collective-permute-start(bf16[256,512]{1,0:T(8,128)(2,1)S(1)} %collective-permute-done.34.refs_10_), channel_id=1, source_target_pairs={{0,4},{2,6},{4,0},{6,2},{1,5},{3,7},{5,1},{7,3},{8,12},{10,14},{12... | collective-permute-start | bytes 786440 | tf_op jit(solution)/shard_map/ppermute | solution.py:22
  (17 other events, 133.3 us)

commit v4 on v3

--- a/solution.py
+++ b/solution.py
@@ -22,9 +22,16 @@
     return lax.ppermute(values, axis, [(i, i ^ step) for i in range(size)])
 
 
+def to_others(blocks, axis, size):
+    arrived = []
+    for k in range(1, size):
+        arrived.append(swap(blocks[k], axis, size, k))
+    return arrived
+
+
 def from_others(values, axis, size):
     if size <= DIRECT:
-        return [swap(values, axis, size, k) for k in range(1, size)]
+        return to_others([values] * size, axis, size)
     whole = lax.all_gather(values, axis)
     order = lax.axis_index(axis) ^ jnp.arange(1, size)
     return [jnp.take(whole, order, axis=0).reshape((-1, *values.shape[1:]))]
@@ -192,7 +199,7 @@
 
 
 def normalize(first, second):
-    return (first / jnp.sqrt(second)).astype(BF16)
+    return (first * lax.rsqrt(second)).astype(BF16)
 
 
 def norm_block(place, parts, local, remote):
@@ -319,7 +326,7 @@
         self.old_refs, self.places = old_refs, places
         last = self.rank + self.moment_rows
         square = sum(normed_ref[last : last + 1, n * 128 : n * 128 + 1].astype(F32) for n in (2, 1, 0))
-        self.scale = lax.rsqrt(square / entries + 0.1)
+        self.scale = lax.rsqrt(jnp.maximum(square, 0.0) / entries + 0.1)
 
     def start(self, k):
         return (self.fs ^ k) * self.rows
@@ -394,40 +401,40 @@
         ]
         sent = []
 
-        def send(side, source, number, k=None):
-            targets = [outs[number], outs[number + 1]]
-            if k is not None:
-                block = pl.ds(pl.multiple_of(side.start(k), rows), rows)
-                targets = [target.at[block, :] for target in targets]
-            sem = sems.at[len(sent)]
-            for wanted, target in zip((side.is_in, jnp.logical_not(side.is_in)), targets):
-
-                @pl.when(wanted)
-                def _(target=target):
-                    pltpu.make_async_copy(source, target, sem).start()
-
-            sent.append(pltpu.make_async_copy(source, targets[0], sem))
+        def send(side, *jobs):
+            for chosen in (0, 1):
+                copies = []
+                for n, (source, number, k) in enumerate(jobs):
+                    target = outs[number + chosen]
+                    if k is not None:
+                        target = target.at[pl.ds(pl.multiple_of(side.start(k), rows), rows), :]
+                    copies.append(pltpu.make_async_copy(source, target, sems.at[len(sent) + n]))
+
+                @pl.when(side.is_in == (chosen == 0))
+                def _(copies=copies):
+                    for n, copy in enumerate(copies):
+                        copy.start(priority=(len(sent) + n) % 2)
+
+            sent.extend(copies)
 
         own, other = sides
-        for n in (0, 1):
-            send(own, own_mine.at[n], 2 * n)
-        for k in range(ready + 1):
-            send(own, own_spread.at[k], 8, k)
-        for n in (0, 1):
-            send(own, own_small.at[n], 4 + 2 * n)
+        send(
+            own,
+            *((own_mine.at[n], 2 * n, None) for n in (0, 1)),
+            *((own_spread.at[k], 8, k) for k in range(ready + 1)),
+            *((own_small.at[n], 4 + 2 * n, None) for n in (0, 1)),
+        )
         other.own_rows(mine.at[1], mine.at[0], spread.at[0])
-        for n in (0, 1):
-            send(other, mine.at[n], 2 * n)
-        send(other, spread.at[0], 8, 0)
-        other.moments(small.at[0], small.at[1])
-        for n in (0, 1):
-            send(other, small.at[n], 4 + 2 * n)
+        send(other, (mine.at[0], 0, None), (mine.at[1], 2, None), (spread.at[0], 8, 0))
         for k in range(1, fs_size):
             other.other_rows(k, spread.at[k])
-            send(other, spread.at[k], 8, k)
+            send(other, (spread.at[k], 8, k))
         for k in range(ready + 1, fs_size):
-            own.other_rows(k, spread.at[fs_size + k - ready - 1])
-            send(own, spread.at[fs_size + k - ready - 1], 8, k)
+            at = fs_size + k - ready - 1
+            own.other_rows(k, spread.at[at])
+            send(own, (spread.at[at], 8, k))
+        other.moments(small.at[0], small.at[1])
+        send(other, *((small.at[n], 4 + 2 * n, None) for n in (0, 1)))
         for copy in sent:
             copy.wait()
 
@@ -507,14 +514,14 @@
 
     y, u_own = project(place, x, in_factor, gate_factor, direct, relayed, rep_size)
     sums = token_sums(place, y, cotangents, rep_size)
-    parts = [sums[0]] + [swap(sums[j], "rep", rep_size, j) for j in range(1, rep_size)]
+    parts = [sums[0]] + to_others(sums, "rep", rep_size)
     u_other = swap(after(u_own, sums[-1]), "tp", tp_size, 1)
     remote_state = [swap(after(values, sums[-1]), "tp", tp_size, 1) for values in state]
     products = gram(after(u_own, sums[-1]))
     rest = rest_of(halves[0], sums[-1])
     sums = add_up(place, parts, fs_size)
     if fs_size <= DIRECT:
-        parts = [sums[0]] + [swap(sums[k], "fs", fs_size, k) for k in range(1, fs_size)]
+        parts = [sums[0]] + to_others(sums, "fs", fs_size)
     else:
         parts = [lax.psum_scatter(sums[0], "fs", scatter_dimension=0, tiled=True)]
     low, normed = norm_block(place, parts, state, remote_state)

time: 98.2 us -> 98.1 us (level)
  no operation moved by 1% of the time
where the time goes in v4:
time: 98.1 us; the launch traced here: 97.9 us
  starting transfers between devices  42.8 us (44%)
  waiting for transfers between devices  35.3 us (36%)
  Pallas kernels  13 us (13%)
  local copies, waits for them, and re-layouts  4.83 us (5%)
    ppermute x36, starting transfers between devices, swap(): return lax.ppermute(values, axis, [(i, i ^ step) for i in range(size)])  42.8 us
    ppermute x36, waiting for transfers between devices, swap(): return lax.ppermute(values, axis, [(i, i ^ step) for i in range(size)])  35.3 us
    unnamed x31, local copies, waits for them, and re-layouts  4.71 us
    pallas_call x1, Pallas kernels, finish(): pl.pallas_call(body, grid_spec=one_step(operands, 10, scratch, pltpu.HBM)...  4.42 us
  transfers between devices with their start and end apart: 36, of which 19 were waited for; matrix products, arithmetic and copies ran while one was open for 0% of the time, Pallas kernels for 9%

profile of v4, /device:TPU:0, one launch (start us, length us, event | category | flops | bytes accessed | tf_op | source)
XLA Modules:
  0.0 97.9 jit_solution(1687557311618403431)
XLA Ops:
  1.5 5.1 %collective-permute-start.2 = (bf16[128,256]{1,0:T(8,128)(2,1)S(1)}, bf16[128,256]{1,0:T(8,128)(2,1)S(1)}, u32[]{:S(2)}, u32[]{:S(2)}) collective-permute-start(bf16[128,256]{1,0:T(8,128)(2,1)S(1)} %dynamic-slice_select_fusion), channel_id=1, source_target_pairs={{0,24},{8,16},{16,8},{24,0},{1,25},{9,17},{17,9},{25,1},{2,26},{10... | collective-permute-start | bytes 196616 | tf_op jit(solution)/shard_map/ppermute | solution.py:22
  7.3 1.8 %collective-permute-done.2.refs_2_ = bf16[128,256]{1,0:T(8,128)(2,1)S(1)} collective-permute-done((bf16[128,256]{1,0:T(8,128)(2,1)S(1)}, bf16[128,256]{1,0:T(8,128)(2,1)S(1)}, u32[]{:S(2)}, u32[]{:S(2)}) %collective-permute-start.2) | collective-permute-done | bytes 65568 | tf_op jit(solution)/shard_map/ppermute | solution.py:22
  9.2 3.1 %collective-permute-done.1.refs_1_ = bf16[128,256]{1,0:T(8,128)(2,1)S(1)} collective-permute-done((bf16[128,256]{1,0:T(8,128)(2,1)S(1)}, bf16[128,256]{1,0:T(8,128)(2,1)S(1)}, u32[]{:S(2)}, u32[]{:S(2)}) %collective-permute-start.1) | collective-permute-done | bytes 65568 | tf_op jit(solution)/shard_map/ppermute | solution.py:22
  12.8 2.5 %collective-permute-start.5 = (bf16[384,256]{1,0:T(8,128)(2,1)S(1)}, bf16[384,256]{1,0:T(8,128)(2,1)S(1)}, u32[]{:S(2)}, u32[]{:S(2)}) collective-permute-start(bf16[384,256]{1,0:T(8,128)(2,1)S(1)} %constant_dynamic-update-slice_fusion), channel_id=1, source_target_pairs={{0,6},{2,4},{4,2},{6,0},{1,7},{3,5},{5,3},{7,1},{8,14},{10,12},{12... | collective-permute-start | bytes 589832 | tf_op jit(solution)/shard_map/ppermute | solution.py:22
  20.7 1.7 %collective-permute-start.27 = (bf16[512,512]{1,0:T(8,128)(2,1)S(1)}, bf16[512,512]{1,0:T(8,128)(2,1)S(1)}, u32[]{:S(2)}, u32[]{:S(2)}) collective-permute-start(bf16[512,512]{1,0:T(8,128)(2,1)S(1)} %held_rows.1), channel_id=1, source_target_pairs={{0,16},{8,24},{16,0},{24,8},{1,17},{9,25},{17,1},{25,9},{2,18},{10... | collective-permute-start | bytes 1572872 | tf_op jit(solution)/shard_map/ppermute | solution.py:22
  22.4 2.4 %collective-permute-done.4.refs_4_ = bf16[384,256]{1,0:T(8,128)(2,1)S(1)} collective-permute-done((bf16[384,256]{1,0:T(8,128)(2,1)S(1)}, bf16[384,256]{1,0:T(8,128)(2,1)S(1)}, u32[]{:S(2)}, u32[]{:S(2)}) %collective-permute-start.4) | collective-permute-done | bytes 196640 | tf_op jit(solution)/shard_map/ppermute | solution.py:22
  24.8 1.5 %collective-permute-start.3 = (bf16[384,256]{1,0:T(8,128)(2,1)S(1)}, bf16[384,256]{1,0:T(8,128)(2,1)S(1)}, u32[]{:S(2)}, u32[]{:S(2)}) collective-permute-start(bf16[384,256]{1,0:T(8,128)(2,1)S(1)} %constant_dynamic-update-slice_fusion), channel_id=1, source_target_pairs={{0,2},{2,0},{4,6},{6,4},{1,3},{3,1},{5,7},{7,5},{8,10},{10,8},{12,... | collective-permute-start | bytes 589832 | tf_op jit(solution)/shard_map/ppermute | solution.py:22
  26.3 2.2 %copy-done.4 = bf16[1024,2048]{1,0:T(8,128)(2,1)S(1)} copy-done((bf16[1024,2048]{1,0:T(8,128)(2,1)S(1)}, bf16[1024,2048]{1,0:T(8,128)(2,1)}, u32[]{:S(2)}) %copy-start.4) | copy-done | bytes 4194328
  28.8 2.8 %collective-permute-done.3.refs_3_ = bf16[384,256]{1,0:T(8,128)(2,1)S(1)} collective-permute-done((bf16[384,256]{1,0:T(8,128)(2,1)S(1)}, bf16[384,256]{1,0:T(8,128)(2,1)S(1)}, u32[]{:S(2)}, u32[]{:S(2)}) %collective-permute-start.3) | collective-permute-done | bytes 196640 | tf_op jit(solution)/shard_map/ppermute | solution.py:22
  31.7 1.9 %project.1 = (bf16[1024,256]{1,0:T(8,128)(2,1)S(1)}, bf16[2048,256]{1,0:T(8,128)(2,1)S(1)}) custom-call(s32[3]{0:T(128)S(1)} %pad_add_fusion.place_ref, bf16[1024,2048]{1,0:T(8,128)(2,1)S(1)} %stage.1.x_ref, bf16[512,256]{1,0:T(8,128)(2,1)S(1)} %copy-done.11, bf16[512,256]{1,0:T(8,128)(2,1)S(1)} %copy-done.12, ...), custom_call_target="tpu_custom_call" | custom-call | tf_op jit(solution)/shard_map/project/pallas_call | solution.py:123
  33.6 1.3 %token_sums.1 = (f32[256,256]{1,0:T(8,128)S(1)}, bf16[256,256]{1,0:T(8,128)(2,1)S(1)}, bf16[256,256]{1,0:T(8,128)(2,1)S(1)}, bf16[256,256]{1,0:T(8,128)(2,1)S(1)}) custom-call(s32[3]{0:T(128)S(1)} %pad_add_fusion.place_ref, bf16[1024,256]{1,0:T(8,128)(2,1)S(1)} %get-tuple-element.50.y_ref, bf16[1024,512]{1,0:T(8,128)(2,1)S(1)} %copy-done.9, ...), custom_call_target="tpu_custom_call" | custom-call | tf_op jit(solution)/shard_map/token_sums/pallas_call | solution.py:154
  35.0 1.6 %collective-permute-start.8 = (bf16[256,256]{1,0:T(8,128)(2,1)S(1)}, bf16[256,256]{1,0:T(8,128)(2,1)S(1)}, u32[]{:S(2)}, u32[]{:S(2)}) collective-permute-start(bf16[256,256]{1,0:T(8,128)(2,1)S(1)} %get-tuple-element.54), channel_id=1, source_target_pairs={{0,2},{2,0},{4,6},{6,4},{1,3},{3,1},{5,7},{7,5},{8,10},{10,8},{12,... | collective-permute-start | bytes 393224 | tf_op jit(solution)/shard_map/ppermute | solution.py:22
  36.8 1.7 %collective-permute-start.10 = (bf16[256,256]{1,0:T(8,128)(2,1)S(1)}, bf16[256,256]{1,0:T(8,128)(2,1)S(1)}, u32[]{:S(2)}, u32[]{:S(2)}) collective-permute-start(bf16[256,256]{1,0:T(8,128)(2,1)S(1)} %get-tuple-element.56), channel_id=1, source_target_pairs={{0,6},{2,4},{4,2},{6,0},{1,7},{3,5},{5,3},{7,1},{8,14},{10,12},{12... | collective-permute-start | bytes 393224 | tf_op jit(solution)/shard_map/ppermute | solution.py:22
  38.5 4.0 %collective-permute-done.26.refs_0_.refs_6_ = bf16[512,512]{1,0:T(8,128)(2,1)S(1)} collective-permute-done((bf16[512,512]{1,0:T(8,128)(2,1)S(1)}, bf16[512,512]{1,0:T(8,128)(2,1)S(1)}, u32[]{:S(2)}, u32[]{:S(2)}) %collective-permute-start.26) | collective-permute-done | bytes 524320 | tf_op jit(solution)/shard_map/ppermute | solution.py:22
  46.0 3.2 %collective-permute-start.12 = (bf16[64,256]{1,0:T(8,128)(2,1)S(1)}, bf16[64,256]{1,0:T(8,128)(2,1)S(1)}, u32[]{:S(2)}, u32[]{:S(2)}) collective-permute-start(bf16[64,256]{1,0:T(8,128)(2,1)S(1)} %get-tuple-element.59), channel_id=1, source_target_pairs={{0,16},{8,24},{16,0},{24,8},{1,17},{9,25},{17,1},{25,9},{2,18},{10... | collective-permute-start | bytes 98312 | tf_op jit(solution)/shard_map/ppermute | solution.py:22
  51.0 4.2 %collective-permute-done.13.refs_3_ = bf16[64,256]{1,0:T(8,128)(2,1)S(1)} collective-permute-done((bf16[64,256]{1,0:T(8,128)(2,1)S(1)}, bf16[64,256]{1,0:T(8,128)(2,1)S(1)}, u32[]{:S(2)}, u32[]{:S(2)}) %collective-permute-start.13) | collective-permute-done | bytes 32800 | tf_op jit(solution)/shard_map/ppermute | solution.py:22
  57.0 3.3 %collective-permute-start.18 = (bf16[64,256]{1,0:T(8,128)(2,1)S(1)}, bf16[64,256]{1,0:T(8,128)(2,1)S(1)}, u32[]{:S(2)}, u32[]{:S(2)}) collective-permute-start(bf16[64,256]{1,0:T(8,128)(2,1)S(1)} %get-tuple-element.66), channel_id=1, source_target_pairs={{0,8},{8,0},{16,24},{24,16},{1,9},{9,1},{17,25},{25,17},{2,10},{10... | collective-permute-start | bytes 98312 | tf_op jit(solution)/shard_map/ppermute | solution.py:22
  60.2 2.0 %collective-permute-done.18 = bf16[64,256]{1,0:T(8,128)(2,1)S(1)} collective-permute-done((bf16[64,256]{1,0:T(8,128)(2,1)S(1)}, bf16[64,256]{1,0:T(8,128)(2,1)S(1)}, u32[]{:S(2)}, u32[]{:S(2)}) %collective-permute-start.18) | collective-permute-done | bytes 32800 | tf_op jit(solution)/shard_map/ppermute | solution.py:22
  62.4 2.5 %collective-permute-start.23 = (bf16[256,256]{1,0:T(8,128)(2,1)S(1)}, bf16[256,256]{1,0:T(8,128)(2,1)S(1)}, u32[]{:S(2)}, u32[]{:S(2)}) collective-permute-start(bf16[256,256]{1,0:T(8,128)(2,1)S(1)} %constant_dynamic-update-slice_fusion.3.refs_0_), channel_id=1, source_target_pairs={{0,6},{2,4},{4,2},{6,0},{1,7},{3,5},{5,3},{7,1},{8,14},{10,12},{12... | collective-permute-start | bytes 393224 | tf_op jit(solution)/shard_map/ppermute | solution.py:22
  65.0 1.9 %collective-permute-start.34 = (bf16[256,512]{1,0:T(8,128)(2,1)S(1)}, bf16[256,512]{1,0:T(8,128)(2,1)S(1)}, u32[]{:S(2)}, u32[]{:S(2)}) collective-permute-start(bf16[256,512]{1,0:T(8,128)(2,1)S(1)} %slice.23), channel_id=1, source_target_pairs={{0,8},{8,0},{16,24},{24,16},{1,9},{9,1},{17,25},{25,17},{2,10},{10... | collective-permute-start | bytes 786440 | tf_op jit(solution)/shard_map/ppermute | solution.py:22
  68.4 1.4 %collective-permute-start.21 = (bf16[256,256]{1,0:T(8,128)(2,1)S(1)}, bf16[256,256]{1,0:T(8,128)(2,1)S(1)}, u32[]{:S(2)}, u32[]{:S(2)}) collective-permute-start(bf16[256,256]{1,0:T(8,128)(2,1)S(1)} %constant_dynamic-update-slice_fusion.3.refs_0_), channel_id=1, source_target_pairs={{0,2},{2,0},{4,6},{6,4},{1,3},{3,1},{5,7},{7,5},{8,10},{10,8},{12,... | collective-permute-start | bytes 393224 | tf_op jit(solution)/shard_map/ppermute | solution.py:22
  69.8 2.1 %collective-permute-done.22.refs_2_ = bf16[256,256]{1,0:T(8,128)(2,1)S(1)} collective-permute-done((bf16[256,256]{1,0:T(8,128)(2,1)S(1)}, bf16[256,256]{1,0:T(8,128)(2,1)S(1)}, u32[]{:S(2)}, u32[]{:S(2)}) %collective-permute-start.22) | collective-permute-done | bytes 131104 | tf_op jit(solution)/shard_map/ppermute | solution.py:22
  72.7 1.6 %collective-permute-done.21.refs_1_ = bf16[256,256]{1,0:T(8,128)(2,1)S(1)} collective-permute-done((bf16[256,256]{1,0:T(8,128)(2,1)S(1)}, bf16[256,256]{1,0:T(8,128)(2,1)S(1)}, u32[]{:S(2)}, u32[]{:S(2)}) %collective-permute-start.21) | collective-permute-done | bytes 131104 | tf_op jit(solution)/shard_map/ppermute | solution.py:22
  74.3 1.3 %collective-permute-start.28 = (bf16[256,512]{1,0:T(8,128)(2,1)S(1)}, bf16[256,512]{1,0:T(8,128)(2,1)S(1)}, u32[]{:S(2)}, u32[]{:S(2)}) collective-permute-start(bf16[256,512]{1,0:T(8,128)(2,1)S(1)} %get-tuple-element.93), channel_id=1, source_target_pairs={{0,2},{2,0},{4,6},{6,4},{1,3},{3,1},{5,7},{7,5},{8,10},{10,8},{12,... | collective-permute-start | bytes 786440 | tf_op jit(solution)/shard_map/ppermute | solution.py:22
  76.8 1.5 %squares.1 = (bf16[336,512]{1,0:T(8,128)(2,1)S(1)}, bf16[336,512]{1,0:T(8,128)(2,1)S(1)}) custom-call(s32[3]{0:T(128)S(1)} %pad_add_fusion.place_ref, bf16[256,256]{1,0:T(8,128)(2,1)S(1)} %constant_dynamic-update-slice_fusion.3.refs_0_, bf16[256,256]{1,0:T(8,128)(2,1)S(1)} %collective-permute-done.21.refs_1_, ...), custom_call_target="tpu_custom_call" | custom-call | tf_op jit(solution)/shard_map/squares/pallas_call | solution.py:299
  78.4 2.6 %collective-permute-start.33 = (bf16[256,512]{1,0:T(8,128)(2,1)S(1)}, bf16[256,512]{1,0:T(8,128)(2,1)S(1)}, u32[]{:S(2)}, u32[]{:S(2)}) collective-permute-start(bf16[256,512]{1,0:T(8,128)(2,1)S(1)} %get-tuple-element.90), channel_id=1, source_target_pairs={{0,4},{2,6},{4,0},{6,2},{1,5},{3,7},{5,1},{7,3},{8,12},{10,14},{12... | collective-permute-start | bytes 786440 | tf_op jit(solution)/shard_map/ppermute | solution.py:22
  81.8 1.4 %collective-permute-start.31 = (bf16[256,512]{1,0:T(8,128)(2,1)S(1)}, bf16[256,512]{1,0:T(8,128)(2,1)S(1)}, u32[]{:S(2)}, u32[]{:S(2)}) collective-permute-start(bf16[256,512]{1,0:T(8,128)(2,1)S(1)} %collective-permute-done.30.refs_4_), channel_id=1, source_target_pairs={{0,2},{2,0},{4,6},{6,4},{1,3},{3,1},{5,7},{7,5},{8,10},{10,8},{12,... | collective-permute-start | bytes 786440 | tf_op jit(solution)/shard_map/ppermute | solution.py:22
  83.2 2.4 %collective-permute-done.29.refs_3_ = bf16[256,512]{1,0:T(8,128)(2,1)S(1)} collective-permute-done((bf16[256,512]{1,0:T(8,128)(2,1)S(1)}, bf16[256,512]{1,0:T(8,128)(2,1)S(1)}, u32[]{:S(2)}, u32[]{:S(2)}) %collective-permute-start.29) | collective-permute-done | bytes 262176 | tf_op jit(solution)/shard_map/ppermute | solution.py:22
  85.6 2.6 %collective-permute-start.35 = (bf16[256,512]{1,0:T(8,128)(2,1)S(1)}, bf16[256,512]{1,0:T(8,128)(2,1)S(1)}, u32[]{:S(2)}, u32[]{:S(2)}) collective-permute-start(bf16[256,512]{1,0:T(8,128)(2,1)S(1)} %collective-permute-done.34.refs_10_), channel_id=1, source_target_pairs={{0,4},{2,6},{4,0},{6,2},{1,5},{3,7},{5,1},{7,3},{8,12},{10,14},{12... | collective-permute-start | bytes 786440 | tf_op jit(solution)/shard_map/ppermute | solution.py:22
  88.1 1.3 %prepare.1 = (f32[2,512,512]{2,1,0:T(8,128)S(1)}, f32[2,64,512]{2,1,0:T(8,128)S(1)}, bf16[3,512,512]{2,1,0:T(8,128)(2,1)S(1)}) custom-call(s32[3]{0:T(128)S(1)} %pad_add_fusion.place_ref, bf16[336,512]{1,0:T(8,128)(2,1)S(1)} %get-tuple-element.69.n_ref.no_ref, bf16[2048,256]{1,0:T(8,128)(2,1)S(1)} %get-tuple-element.68.u_ref.uo_ref, ...), custom_call_target="tpu_custom_call" | custom-call | tf_op jit(solution)/shard_map/prepare/pallas_call | solution.py:375
  90.2 3.2 %collective-permute-done.35.refs_11_ = bf16[256,512]{1,0:T(8,128)(2,1)S(1)} collective-permute-done((bf16[256,512]{1,0:T(8,128)(2,1)S(1)}, bf16[256,512]{1,0:T(8,128)(2,1)S(1)}, u32[]{:S(2)}, u32[]{:S(2)}) %collective-permute-start.35) | collective-permute-done | bytes 262176 | tf_op jit(solution)/shard_map/ppermute | solution.py:22
  93.5 4.4 %finish.1 = (f32[512,512]{1,0:T(8,128)}, f32[512,512]{1,0:T(8,128)}, f32[512,512]{1,0:T(8,128)}, f32[512,512]{1,0:T(8,128)}, f32[64,512]{1,0:T(8,128)}, /*index=...) custom-call(s32[3]{0:T(128)S(1)} %pad_add_fusion.place_ref, ...), custom_call_target="tpu_custom_call" | custom-call | tf_op jit(solution)/shard_map/finish/pallas_call | solution.py:449
  (89 shorter events, 20.6 us)
Async XLA Ops:
  1.5 7.6 %collective-permute-start.2 = (bf16[128,256]{1,0:T(8,128)(2,1)S(1)}, bf16[128,256]{1,0:T(8,128)(2,1)S(1)}, u32[]{:S(2)}, u32[]{:S(2)}) collective-permute-start(bf16[128,256]{1,0:T(8,128)(2,1)S(1)} %dynamic-slice_select_fusion), channel_id=1, source_target_pairs={{0,24},{8,16},{16,8},{24,0},{1,25},{9,17},{17,9},{25,1},{2,26},{10... | collective-permute-start | bytes 196616 | tf_op jit(solution)/shard_map/ppermute | solution.py:22
  6.7 5.6 %collective-permute-start.1 = (bf16[128,256]{1,0:T(8,128)(2,1)S(1)}, bf16[128,256]{1,0:T(8,128)(2,1)S(1)}, u32[]{:S(2)}, u32[]{:S(2)}) collective-permute-start(bf16[128,256]{1,0:T(8,128)(2,1)S(1)} %dynamic-slice_select_fusion), channel_id=1, source_target_pairs={{0,16},{8,24},{16,0},{24,8},{1,17},{9,25},{17,1},{25,9},{2,18},{10... | collective-permute-start | bytes 196616 | tf_op jit(solution)/shard_map/ppermute | solution.py:22
  6.7 5.6 %collective-permute-start = (bf16[128,256]{1,0:T(8,128)(2,1)S(1)}, bf16[128,256]{1,0:T(8,128)(2,1)S(1)}, u32[]{:S(2)}, u32[]{:S(2)}) collective-permute-start(bf16[128,256]{1,0:T(8,128)(2,1)S(1)} %dynamic-slice_select_fusion), channel_id=1, source_target_pairs={{0,8},{8,0},{16,24},{24,16},{1,9},{9,1},{17,25},{25,17},{2,10},{10... | collective-permute-start | bytes 196616 | tf_op jit(solution)/shard_map/ppermute | solution.py:22
  12.3 21.2 %collective-permute-start.6 = (bf16[1024,512]{1,0:T(8,128)(2,1)}, bf16[1024,512]{1,0:T(8,128)(2,1)S(1)}, u32[]{:S(2)}, u32[]{:S(2)}) collective-permute-start(bf16[1024,512]{1,0:T(8,128)(2,1)} %ci.1), channel_id=1, source_target_pairs={{0,1},{1,0},{2,3},{3,2},{4,5},{5,4},{6,7},{7,6},{8,9},{9,8},{10,11... | collective-permute-start | bytes 3145736 | tf_op jit(solution)/shard_map/ppermute | solution.py:22
  12.3 21.2 %collective-permute-start.7 = (bf16[1024,512]{1,0:T(8,128)(2,1)}, bf16[1024,512]{1,0:T(8,128)(2,1)S(1)}, u32[]{:S(2)}, u32[]{:S(2)}) collective-permute-start(bf16[1024,512]{1,0:T(8,128)(2,1)} %cg.1), channel_id=1, source_target_pairs={{0,1},{1,0},{2,3},{3,2},{4,5},{5,4},{6,7},{7,6},{8,9},{9,8},{10,11... | collective-permute-start | bytes 3145736 | tf_op jit(solution)/shard_map/ppermute | solution.py:22
  12.8 7.9 %collective-permute-start.5 = (bf16[384,256]{1,0:T(8,128)(2,1)S(1)}, bf16[384,256]{1,0:T(8,128)(2,1)S(1)}, u32[]{:S(2)}, u32[]{:S(2)}) collective-permute-start(bf16[384,256]{1,0:T(8,128)(2,1)S(1)} %constant_dynamic-update-slice_fusion), channel_id=1, source_target_pairs={{0,6},{2,4},{4,2},{6,0},{1,7},{3,5},{5,3},{7,1},{8,14},{10,12},{12... | collective-permute-start | bytes 589832 | tf_op jit(solution)/shard_map/ppermute | solution.py:22
  15.3 9.5 %collective-permute-start.4 = (bf16[384,256]{1,0:T(8,128)(2,1)S(1)}, bf16[384,256]{1,0:T(8,128)(2,1)S(1)}, u32[]{:S(2)}, u32[]{:S(2)}) collective-permute-start(bf16[384,256]{1,0:T(8,128)(2,1)S(1)} %constant_dynamic-update-slice_fusion), channel_id=1, source_target_pairs={{0,4},{2,6},{4,0},{6,2},{1,5},{3,7},{5,1},{7,3},{8,12},{10,14},{12... | collective-permute-start | bytes 589832 | tf_op jit(solution)/shard_map/ppermute | solution.py:22
  19.0 23.5 %collective-permute-start.26 = (bf16[512,512]{1,0:T(8,128)(2,1)S(1)}, bf16[512,512]{1,0:T(8,128)(2,1)S(1)}, u32[]{:S(2)}, u32[]{:S(2)}) collective-permute-start(bf16[512,512]{1,0:T(8,128)(2,1)S(1)} %held_rows.1), channel_id=1, source_target_pairs={{0,8},{8,0},{16,24},{24,16},{1,9},{9,1},{17,25},{25,17},{2,10},{10... | collective-permute-start | bytes 1572872 | tf_op jit(solution)/shard_map/ppermute | solution.py:22
  20.7 25.1 %collective-permute-start.27 = (bf16[512,512]{1,0:T(8,128)(2,1)S(1)}, bf16[512,512]{1,0:T(8,128)(2,1)S(1)}, u32[]{:S(2)}, u32[]{:S(2)}) collective-permute-start(bf16[512,512]{1,0:T(8,128)(2,1)S(1)} %held_rows.1), channel_id=1, source_target_pairs={{0,16},{8,24},{16,0},{24,8},{1,17},{9,25},{17,1},{25,9},{2,18},{10... | collective-permute-start | bytes 1572872 | tf_op jit(solution)/shard_map/ppermute | solution.py:22
  24.8 6.8 %collective-permute-start.3 = (bf16[384,256]{1,0:T(8,128)(2,1)S(1)}, bf16[384,256]{1,0:T(8,128)(2,1)S(1)}, u32[]{:S(2)}, u32[]{:S(2)}) collective-permute-start(bf16[384,256]{1,0:T(8,128)(2,1)S(1)} %constant_dynamic-update-slice_fusion), channel_id=1, source_target_pairs={{0,2},{2,0},{4,6},{6,4},{1,3},{3,1},{5,7},{7,5},{8,10},{10,8},{12,... | collective-permute-start | bytes 589832 | tf_op jit(solution)/shard_map/ppermute | solution.py:22
  35.0 7.6 %collective-permute-start.8 = (bf16[256,256]{1,0:T(8,128)(2,1)S(1)}, bf16[256,256]{1,0:T(8,128)(2,1)S(1)}, u32[]{:S(2)}, u32[]{:S(2)}) collective-permute-start(bf16[256,256]{1,0:T(8,128)(2,1)S(1)} %get-tuple-element.54), channel_id=1, source_target_pairs={{0,2},{2,0},{4,6},{6,4},{1,3},{3,1},{5,7},{7,5},{8,10},{10,8},{12,... | collective-permute-start | bytes 393224 | tf_op jit(solution)/shard_map/ppermute | solution.py:22
  36.5 7.1 %collective-permute-start.9 = (bf16[256,256]{1,0:T(8,128)(2,1)S(1)}, bf16[256,256]{1,0:T(8,128)(2,1)S(1)}, u32[]{:S(2)}, u32[]{:S(2)}) collective-permute-start(bf16[256,256]{1,0:T(8,128)(2,1)S(1)} %get-tuple-element.55), channel_id=1, source_target_pairs={{0,4},{2,6},{4,0},{6,2},{1,5},{3,7},{5,1},{7,3},{8,12},{10,14},{12... | collective-permute-start | bytes 393224 | tf_op jit(solution)/shard_map/ppermute | solution.py:22
  36.8 6.8 %collective-permute-start.10 = (bf16[256,256]{1,0:T(8,128)(2,1)S(1)}, bf16[256,256]{1,0:T(8,128)(2,1)S(1)}, u32[]{:S(2)}, u32[]{:S(2)}) collective-permute-start(bf16[256,256]{1,0:T(8,128)(2,1)S(1)} %get-tuple-element.56), channel_id=1, source_target_pairs={{0,6},{2,4},{4,2},{6,0},{1,7},{3,5},{5,3},{7,1},{8,14},{10,12},{12... | collective-permute-start | bytes 393224 | tf_op jit(solution)/shard_map/ppermute | solution.py:22
  42.5 6.6 %collective-permute-start.15 = (f32[64,512]{1,0:T(8,128)S(1)}, f32[64,512]{1,0:T(8,128)S(1)}, u32[]{:S(2)}, u32[]{:S(2)}) collective-permute-start(f32[64,512]{1,0:T(8,128)S(1)} %copy-done.6), channel_id=1, source_target_pairs={{0,1},{1,0},{2,3},{3,2},{4,5},{5,4},{6,7},{7,6},{8,9},{9,8},{10,11... | collective-permute-start | bytes 393224 | tf_op jit(solution)/shard_map/ppermute | solution.py:22
  43.6 6.6 %collective-permute-start.16 = (f32[64,512]{1,0:T(8,128)S(1)}, f32[64,512]{1,0:T(8,128)S(1)}, u32[]{:S(2)}, u32[]{:S(2)}) collective-permute-start(f32[64,512]{1,0:T(8,128)S(1)} %copy-done.7), channel_id=1, source_target_pairs={{0,1},{1,0},{2,3},{3,2},{4,5},{5,4},{6,7},{7,6},{8,9},{9,8},{10,11... | collective-permute-start | bytes 393224 | tf_op jit(solution)/shard_map/ppermute | solution.py:22
  43.7 6.7 %collective-permute-start.17 = (f32[64,512]{1,0:T(8,128)S(1)}, f32[64,512]{1,0:T(8,128)S(1)}, u32[]{:S(2)}, u32[]{:S(2)}) collective-permute-start(f32[64,512]{1,0:T(8,128)S(1)} %copy-done.8), channel_id=1, source_target_pairs={{0,1},{1,0},{2,3},{3,2},{4,5},{5,4},{6,7},{7,6},{8,9},{9,8},{10,11... | collective-permute-start | bytes 393224 | tf_op jit(solution)/shard_map/ppermute | solution.py:22
  49.1 6.1 %collective-permute-start.13 = (bf16[64,256]{1,0:T(8,128)(2,1)S(1)}, bf16[64,256]{1,0:T(8,128)(2,1)S(1)}, u32[]{:S(2)}, u32[]{:S(2)}) collective-permute-start(bf16[64,256]{1,0:T(8,128)(2,1)S(1)} %get-tuple-element.60), channel_id=1, source_target_pairs={{0,24},{8,16},{16,8},{24,0},{1,25},{9,17},{17,9},{25,1},{2,26},{10... | collective-permute-start | bytes 98312 | tf_op jit(solution)/shard_map/ppermute | solution.py:22
  50.3 43.2 %collective-permute-start.25 = (bf16[2048,256]{1,0:T(8,128)(2,1)S(1)}, bf16[2048,256]{1,0:T(8,128)(2,1)S(1)}, u32[]{:S(2)}, u32[]{:S(2)}) collective-permute-start(bf16[2048,256]{1,0:T(8,128)(2,1)S(1)} %get-tuple-element.68.u_ref.uo_ref), channel_id=1, source_target_pairs={{0,1},{1,0},{2,3},{3,2},{4,5},{5,4},{6,7},{7,6},{8,9},{9,8},{10,11... | collective-permute-start | bytes 3145736 | tf_op jit(solution)/shard_map/ppermute | solution.py:22
  50.3 25.2 %collective-permute-start.30 = (bf16[256,512]{1,0:T(8,128)(2,1)S(1)}, bf16[256,512]{1,0:T(8,128)(2,1)S(1)}, u32[]{:S(2)}, u32[]{:S(2)}) collective-permute-start(bf16[256,512]{1,0:T(8,128)(2,1)S(1)} %slice.20), channel_id=1, source_target_pairs={{0,8},{8,0},{16,24},{24,16},{1,9},{9,1},{17,25},{25,17},{2,10},{10... | collective-permute-start | bytes 786440 | tf_op jit(solution)/shard_map/ppermute | solution.py:22
  55.8 6.6 %collective-permute-start.20 = (bf16[64,256]{1,0:T(8,128)(2,1)S(1)}, bf16[64,256]{1,0:T(8,128)(2,1)S(1)}, u32[]{:S(2)}, u32[]{:S(2)}) collective-permute-start(bf16[64,256]{1,0:T(8,128)(2,1)S(1)} %get-tuple-element.66), channel_id=1, source_target_pairs={{0,24},{8,16},{16,8},{24,0},{1,25},{9,17},{17,9},{25,1},{2,26},{10... | collective-permute-start | bytes 98312 | tf_op jit(solution)/shard_map/ppermute | solution.py:22
  57.0 5.4 %collective-permute-start.19 = (bf16[64,256]{1,0:T(8,128)(2,1)S(1)}, bf16[64,256]{1,0:T(8,128)(2,1)S(1)}, u32[]{:S(2)}, u32[]{:S(2)}) collective-permute-start(bf16[64,256]{1,0:T(8,128)(2,1)S(1)} %get-tuple-element.66), channel_id=1, source_target_pairs={{0,16},{8,24},{16,0},{24,8},{1,17},{9,25},{17,1},{25,9},{2,18},{10... | collective-permute-start | bytes 98312 | tf_op jit(solution)/shard_map/ppermute | solution.py:22
  57.0 5.3 %collective-permute-start.18 = (bf16[64,256]{1,0:T(8,128)(2,1)S(1)}, bf16[64,256]{1,0:T(8,128)(2,1)S(1)}, u32[]{:S(2)}, u32[]{:S(2)}) collective-permute-start(bf16[64,256]{1,0:T(8,128)(2,1)S(1)} %get-tuple-element.66), channel_id=1, source_target_pairs={{0,8},{8,0},{16,24},{24,16},{1,9},{9,1},{17,25},{25,17},{2,10},{10... | collective-permute-start | bytes 98312 | tf_op jit(solution)/shard_map/ppermute | solution.py:22
  62.4 6.0 %collective-permute-start.23 = (bf16[256,256]{1,0:T(8,128)(2,1)S(1)}, bf16[256,256]{1,0:T(8,128)(2,1)S(1)}, u32[]{:S(2)}, u32[]{:S(2)}) collective-permute-start(bf16[256,256]{1,0:T(8,128)(2,1)S(1)} %constant_dynamic-update-slice_fusion.3.refs_0_), channel_id=1, source_target_pairs={{0,6},{2,4},{4,2},{6,0},{1,7},{3,5},{5,3},{7,1},{8,14},{10,12},{12... | collective-permute-start | bytes 393224 | tf_op jit(solution)/shard_map/ppermute | solution.py:22
  65.0 13.3 %collective-permute-start.34 = (bf16[256,512]{1,0:T(8,128)(2,1)S(1)}, bf16[256,512]{1,0:T(8,128)(2,1)S(1)}, u32[]{:S(2)}, u32[]{:S(2)}) collective-permute-start(bf16[256,512]{1,0:T(8,128)(2,1)S(1)} %slice.23), channel_id=1, source_target_pairs={{0,8},{8,0},{16,24},{24,16},{1,9},{9,1},{17,25},{25,17},{2,10},{10... | collective-permute-start | bytes 786440 | tf_op jit(solution)/shard_map/ppermute | solution.py:22
  68.4 5.9 %collective-permute-start.21 = (bf16[256,256]{1,0:T(8,128)(2,1)S(1)}, bf16[256,256]{1,0:T(8,128)(2,1)S(1)}, u32[]{:S(2)}, u32[]{:S(2)}) collective-permute-start(bf16[256,256]{1,0:T(8,128)(2,1)S(1)} %constant_dynamic-update-slice_fusion.3.refs_0_), channel_id=1, source_target_pairs={{0,2},{2,0},{4,6},{6,4},{1,3},{3,1},{5,7},{7,5},{8,10},{10,8},{12,... | collective-permute-start | bytes 393224 | tf_op jit(solution)/shard_map/ppermute | solution.py:22
  71.9 6.4 %collective-permute-start.32 = (bf16[256,512]{1,0:T(8,128)(2,1)S(1)}, bf16[256,512]{1,0:T(8,128)(2,1)S(1)}, u32[]{:S(2)}, u32[]{:S(2)}) collective-permute-start(bf16[256,512]{1,0:T(8,128)(2,1)S(1)} %get-tuple-element.92), channel_id=1, source_target_pairs={{0,4},{2,6},{4,0},{6,2},{1,5},{3,7},{5,1},{7,3},{8,12},{10,14},{12... | collective-permute-start | bytes 786440 | tf_op jit(solution)/shard_map/ppermute | solution.py:22
  74.3 7.5 %collective-permute-start.28 = (bf16[256,512]{1,0:T(8,128)(2,1)S(1)}, bf16[256,512]{1,0:T(8,128)(2,1)S(1)}, u32[]{:S(2)}, u32[]{:S(2)}) collective-permute-start(bf16[256,512]{1,0:T(8,128)(2,1)S(1)} %get-tuple-element.93), channel_id=1, source_target_pairs={{0,2},{2,0},{4,6},{6,4},{1,3},{3,1},{5,7},{7,5},{8,10},{10,8},{12,... | collective-permute-start | bytes 786440 | tf_op jit(solution)/shard_map/ppermute | solution.py:22
  75.6 10.0 %collective-permute-start.29 = (bf16[256,512]{1,0:T(8,128)(2,1)S(1)}, bf16[256,512]{1,0:T(8,128)(2,1)S(1)}, u32[]{:S(2)}, u32[]{:S(2)}) collective-permute-start(bf16[256,512]{1,0:T(8,128)(2,1)S(1)} %get-tuple-element.91), channel_id=1, source_target_pairs={{0,2},{2,0},{4,6},{6,4},{1,3},{3,1},{5,7},{7,5},{8,10},{10,8},{12,... | collective-permute-start | bytes 786440 | tf_op jit(solution)/shard_map/ppermute | solution.py:22
  78.3 12.0 %collective-permute-start.24 = (bf16[336,512]{1,0:T(8,128)(2,1)S(1)}, bf16[336,512]{1,0:T(8,128)(2,1)S(1)}, u32[]{:S(2)}, u32[]{:S(2)}) collective-permute-start(bf16[336,512]{1,0:T(8,128)(2,1)S(1)} %get-tuple-element.70), channel_id=1, source_target_pairs={{0,1},{1,0},{2,3},{3,2},{4,5},{5,4},{6,7},{7,6},{8,9},{9,8},{10,11... | collective-permute-start | bytes 1032200 | tf_op jit(solution)/shard_map/ppermute | solution.py:22
  78.4 11.1 %collective-permute-start.33 = (bf16[256,512]{1,0:T(8,128)(2,1)S(1)}, bf16[256,512]{1,0:T(8,128)(2,1)S(1)}, u32[]{:S(2)}, u32[]{:S(2)}) collective-permute-start(bf16[256,512]{1,0:T(8,128)(2,1)S(1)} %get-tuple-element.90), channel_id=1, source_target_pairs={{0,4},{2,6},{4,0},{6,2},{1,5},{3,7},{5,1},{7,3},{8,12},{10,14},{12... | collective-permute-start | bytes 786440 | tf_op jit(solution)/shard_map/ppermute | solution.py:22
  81.8 8.4 %collective-permute-start.31 = (bf16[256,512]{1,0:T(8,128)(2,1)S(1)}, bf16[256,512]{1,0:T(8,128)(2,1)S(1)}, u32[]{:S(2)}, u32[]{:S(2)}) collective-permute-start(bf16[256,512]{1,0:T(8,128)(2,1)S(1)} %collective-permute-done.30.refs_4_), channel_id=1, source_target_pairs={{0,2},{2,0},{4,6},{6,4},{1,3},{3,1},{5,7},{7,5},{8,10},{10,8},{12,... | collective-permute-start | bytes 786440 | tf_op jit(solution)/shard_map/ppermute | solution.py:22
  85.6 7.9 %collective-permute-start.35 = (bf16[256,512]{1,0:T(8,128)(2,1)S(1)}, bf16[256,512]{1,0:T(8,128)(2,1)S(1)}, u32[]{:S(2)}, u32[]{:S(2)}) collective-permute-start(bf16[256,512]{1,0:T(8,128)(2,1)S(1)} %collective-permute-done.34.refs_10_), channel_id=1, source_target_pairs={{0,4},{2,6},{4,0},{6,2},{1,5},{3,7},{5,1},{7,3},{8,12},{10,14},{12... | collective-permute-start | bytes 786440 | tf_op jit(solution)/shard_map/ppermute | solution.py:22
  (17 other events, 133.5 us)
